TPU v7x, 512 devices: a whole 4x8x8 slice. The times are simulated.
512 devices in a mesh: rep: 2 (over z_hi), fs: 32 (over z_lo, y), tp: 8 (over x, core).
Axes of the slice: x: 4, y: 8, z: 8 (z_hi: 2, z_lo: 4; z = z_hi * 4 + z_lo), core: 2. Of those that a mesh axis runs over, the one named last changes fastest.
Arguments:
- tokens: bfloat16 [64, 192, 2048], P(('rep', 'fs'), 'tp'), may hold values from -6 to 6
- mix_gain: float32 [2048], replicated, may hold values from 0.1 to 1.9
- w_query: float32 [2048, 2048], P('fs', 'tp'), may hold values from -0.125 to 0.125
- w_key: float32 [2048, 2048], P('fs', 'tp'), may hold values from -0.125 to 0.125
- w_value: float32 [2048, 2048], P('fs', 'tp'), may hold values from -0.125 to 0.125
- w_out: float32 [2048, 2048], P('tp', 'fs'), may hold values from -0.125 to 0.125
- scale_query: float32 [2048], P('tp'), may hold values from 0.1 to 1.9
- scale_key: float32 [2048], P('tp'), may hold values from 0.1 to 1.9
- scale_value: float32 [2048], P('tp'), may hold values from 0.1 to 1.9
- scale_out: float32 [2048], replicated, may hold values from 0.1 to 1.9
- decay_rate: float32 [8], P('tp'), may hold values from 0.003 to 0.08
- mlp_gain: float32 [2048], replicated, may hold values from 0.1 to 1.9
- w_gate: float32 [2048, 3072], P('fs', 'tp'), may hold values from -0.125 to 0.125
- w_up: float32 [2048, 3072], P('fs', 'tp'), may hold values from -0.125 to 0.125
- w_down: float32 [3072, 2048], P('tp', 'fs'), may hold values from -0.109375 to 0.109375
- scale_gate: float32 [3072], P('tp'), may hold values from 0.1 to 1.9
- scale_up: float32 [3072], P('tp'), may hold values from 0.1 to 1.9
- scale_down: float32 [2048], replicated, may hold values from 0.1 to 1.9
Outputs:
- layer_out: bfloat16 [64, 192, 2048], P(('rep', 'fs'), 'tp')
All inputs are finite; a program needn't handle non-finite values.
Results may differ from a plain program's by a relative error of at most 0.015.
Values may be sent and summed in bfloat16 or wider, within the bound.
No kernel may reach another device: no remote copies, remote signals or barrier semaphores. Data moves between devices by JAX's collectives and lax.ppermute only.
A program may use at most 64 MiB of HBM per device.

v0:
```python
import jax
import jax.numpy as jnp
from jax import lax
from jax.sharding import Mesh, PartitionSpec as P


HEAD_DIM = 256
EPS = 1e-06
ROPE_BASE = 10000.0
RING = ("rep", "z")
TP = ("x", "core")


def inv_rms(values):
    return lax.rsqrt(jnp.mean(values * values, axis=-1, keepdims=True) + EPS)


def exchange_y(array):
    peers = lax.axis_size("y")
    return lax.all_to_all(
        jnp.broadcast_to(array[None], (peers, *array.shape)), "y", 0, 0, tiled=True
    )


def pairs(offset, n=8):
    out = []
    for a in range(offset, n + offset, 2):
        b = (a + 1) % n
        out += [(a % n, b), (b, a % n)]
    return out


def ring_pieces(block):
    half = block.shape[0] // 2
    even = lax.ppermute(block, RING, pairs(0))
    odd = lax.ppermute(block, RING, pairs(1))
    far_a = lax.ppermute(even[:half], RING, pairs(1))
    far_b = lax.ppermute(odd[half:], RING, pairs(0))
    return block, even, odd, far_a, far_b


def ring_labels():
    z = lax.axis_index("z")
    odd = z % 2
    return z, z + 1 - 2 * odd, (z + 3 + 2 * odd) % 4, (z + 2) % 4


def ring_slots():
    z, even, odd, _ = ring_labels()
    return [jnp.where(z == j, 0, jnp.where(even == j, 1, jnp.where(odd == j, 2, 3))) for j in range(4)]


def ring_dot(x, pieces):
    own, even, odd, far_a, far_b = pieces
    size = own.shape[0]
    half = size // 2
    own_at, even_at, odd_at, far_at = ring_labels()

    def term(label, start, piece):
        cut = lax.dynamic_slice_in_dim(x, label * size + start, piece.shape[0], 1)
        return jnp.dot(cut, piece, preferred_element_type=jnp.float32)

    total = term(own_at, 0, own) + term(even_at, 0, even) + term(odd_at, 0, odd)
    return total + term(far_at, 0, far_a) + term(far_at, half, far_b)


def dot_t(a, b):
    return lax.dot_general(a, b, (((1,), (1,)), ((), ())), preferred_element_type=jnp.float32)


def sum_at_owner(partial):
    chips = lax.axis_size("x")
    core, chip = lax.axis_index("core"), lax.axis_index("x")
    blocks = partial.reshape(chips, 2, -1, partial.shape[1])
    sent = lax.dynamic_index_in_dim(blocks, 1 - core, 1, keepdims=False)
    got = lax.ppermute(sent, "core", [(0, 1), (1, 0)])
    kept = lax.dynamic_index_in_dim(blocks, core, 1, keepdims=False)
    both = kept.astype(jnp.float32) + got.astype(jnp.float32)
    total = lax.dynamic_index_in_dim(both, chip, 0, keepdims=False)
    both = both.astype(jnp.bfloat16)
    for step in (1, 3, 2):
        block = lax.dynamic_index_in_dim(both, (chip + step) % chips, 0, keepdims=False)
        got = lax.ppermute(block, "x", [(i, (i + step) % chips) for i in range(chips)])
        total = total + got.astype(jnp.float32)
    return total


def rotary(values, cosine, sine):
    half = values.shape[-1] // 2
    first = values[:, :half]
    second = values[:, half:]
    return jnp.concatenate(
        [first * cosine - second * sine, first * sine + second * cosine], axis=-1
    )


def per_device(
    tokens,
    mix_gain,
    w_query,
    w_key,
    w_value,
    w_out,
    scale_query,
    scale_key,
    scale_value,
    scale_out,
    decay_rate,
    mlp_gain,
    w_gate,
    w_up,
    w_down,
    scale_gate,
    scale_up,
    scale_down,
):
    bf16, f32 = jnp.bfloat16, jnp.float32
    own_rows = tokens[0]
    rows, width = own_rows.shape
    length = rows * lax.axis_size(TP)
    cols = HEAD_DIM + HEAD_DIM // 2

    qkv = jnp.concatenate([w_query, w_key, w_value], axis=1).astype(bf16)
    first = exchange_y(qkv[:, :cols]).reshape(-1, cols)
    second = exchange_y(jnp.concatenate([qkv[:, cols:], w_out.T.astype(bf16)], axis=1))
    second = second.reshape(-1, cols + HEAD_DIM)
    first = ring_pieces(first)
    out_own = second[:, cols:]
    second = ring_pieces(second[:, :cols])
    out_pieces = ring_pieces(out_own)
    units = w_gate.shape[1]
    mlp = jnp.concatenate([w_gate, w_up], axis=1).astype(bf16)
    mlp = exchange_y(mlp).reshape(-1, mlp.shape[1])
    mlp = ring_pieces(mlp)
    own, even, odd, far_a, far_b = ring_pieces(w_down.T.astype(bf16))
    down = jnp.stack([own, even, odd, jnp.concatenate([far_a, far_b], axis=0)])
    down = exchange_y(down)
    down = jnp.moveaxis(down, 0, 1).reshape(width, -1)
    all_rows = lax.all_gather(own_rows, TP, axis=0, tiled=True)

    values = all_rows.astype(f32)
    normed = (values * inv_rms(values) * mix_gain).astype(bf16)
    first = ring_dot(normed, first)
    second = ring_dot(normed, second)
    positions = jnp.arange(length, dtype=f32)
    inv_freq = 1.0 / ROPE_BASE ** (jnp.arange(0, HEAD_DIM, 2, dtype=f32) / HEAD_DIM)
    angles = positions[:, None] * inv_freq[None, :]
    cosine, sine = jnp.cos(angles), jnp.sin(angles)
    key_raw = jnp.concatenate([first[:, HEAD_DIM:], second[:, : HEAD_DIM // 2]], axis=1)
    query = rotary(first[:, :HEAD_DIM] * scale_query, cosine, sine).astype(bf16)
    keyed = rotary(key_raw * scale_key, cosine, sine).astype(bf16)
    valued = (second[:, HEAD_DIM // 2 :] * scale_value).astype(bf16)
    distance = positions[:, None] - positions[None, :]
    decay = jnp.where(distance >= 0.0, jnp.exp(-decay_rate[0] * jnp.maximum(distance, 0.0)), 0.0)
    weights = (dot_t(query, keyed) * decay).astype(bf16)
    retained = jnp.dot(weights, valued, preferred_element_type=f32)
    attended = (retained * inv_rms(retained)).astype(bf16)
    partial = jnp.concatenate([dot_t(attended, piece) for piece in out_pieces], axis=1).astype(bf16)

    slots = ring_slots()

    def in_order(values):
        size = width // 4
        return jnp.concatenate(
            [lax.dynamic_slice_in_dim(values, slot * size, size, 1) for slot in slots], axis=1
        )

    mixed = sum_at_owner(partial)
    mixed = in_order(mixed) * scale_out
    hidden = (own_rows.astype(f32) + mixed).astype(bf16)
    values = hidden.astype(f32)
    mlp_in = (values * inv_rms(values) * mlp_gain).astype(bf16)
    mlp_in = lax.all_gather(mlp_in, TP, axis=0, tiled=True)

    both = ring_dot(mlp_in, mlp)
    inner = (jax.nn.silu(both[:, :units] * scale_gate) * (both[:, units:] * scale_up)).astype(bf16)
    channel = sum_at_owner(dot_t(inner, down).astype(bf16))
    channel = in_order(channel) * scale_down
    return (hidden.astype(f32) + channel).astype(bf16)[None]


def solution(mesh):
    grid = Mesh(mesh.devices.reshape(2, 4, 8, 4, 2), ("rep", "z", "y", "x", "core"))
    seqs, fs = ("rep", "z", "y"), ("z", "y")
    by_rows, by_cols = P(fs, TP), P(TP, fs)
    in_specs = (
        P(seqs, TP, None), P(), by_rows, by_rows, by_rows, by_cols,
        P(TP), P(TP), P(TP), P(), P(TP), P(),
        by_rows, by_rows, by_cols, P(TP), P(TP), P(),
    )

    return jax.shard_map(
        per_device, mesh=grid, in_specs=in_specs, out_specs=P(seqs, TP, None), check_vma=False
    )
```

profile of v0, /device:TPU:1, one launch (start us, length us, event | category | flops | bytes accessed | tf_op | source)
XLA Modules:
  0.0 211.2 jit_solution(5129365910789973397)
XLA Ops:
  2.5 7.6 %all-to-all-start = ((bf16[8,64,384]{2,1,0:T(8,128)(2,1)}), bf16[8,64,384]{2,1,0:T(8,128)(2,1)S(1)}, u32[]{:S(2)}, u32[]{:S(2)}) async-start(bf16[8,64,384]{2,1,0:T(8,128)(2,1)} %broadcast_in_dim.9), calls=%async_computation | async-start | bytes 786432 | tf_op jit(solution)/shard_map/all_to_all | solution.py:20
  10.3 15.9 %all-gather = bf16[1,192,2048]{2,1,0:T(8,128)(2,1)S(1)} all-gather(bf16[1,24,2048]{2,1,0:T(8,128)(2,1)S(1)} %copy-done.2), channel_id=2, replica_groups=mesh['rep'=2,'z'=4,'y'=8,'x'=4,'core'=2] {'x','core'}, dimensions={1}, use_global_device_ids=true | all-gather | bytes 884736 | tf_op jit(solution)/shard_map/all_gather | solution.py:139
  27.3 6.8 %all-to-all-start.1 = ((bf16[8,64,640]{2,1,0:T(8,128)(2,1)}), bf16[8,64,640]{2,1,0:T(8,128)(2,1)S(1)}, u32[]{:S(2)}, u32[]{:S(2)}) async-start(bf16[8,64,640]{2,1,0:T(8,128)(2,1)} %broadcast_in_dim.10), calls=%async_computation.1 | async-start | bytes 1310720 | tf_op jit(solution)/shard_map/all_to_all | solution.py:20
  37.1 8.8 %collective-permute-start.1 = (bf16[512,384]{1,0:T(8,128)(2,1)S(1)}, bf16[512,384]{1,0:T(8,128)(2,1)S(1)}, u32[]{:S(2)}, u32[]{:S(2)}) collective-permute-start(bf16[512,384]{1,0:T(8,128)(2,1)S(1)} %bitcast.116), channel_id=1, source_target_pairs={{64,128},{128,64},{192,256},{256,192},{320,384},{384,320},{448,0},... | collective-permute-start | bytes 1179656 | tf_op jit(solution)/shard_map/ppermute | solution.py:36
  48.8 6.0 %collective-permute-done.1 = bf16[512,384]{1,0:T(8,128)(2,1)S(1)} collective-permute-done((bf16[512,384]{1,0:T(8,128)(2,1)S(1)}, bf16[512,384]{1,0:T(8,128)(2,1)S(1)}, u32[]{:S(2)}, u32[]{:S(2)}) %collective-permute-start.1) | collective-permute-done | bytes 393248 | tf_op jit(solution)/shard_map/ppermute | solution.py:36
  58.1 4.3 %collective-permute-start.2 = (bf16[256,384]{1,0:T(8,128)(2,1)}, bf16[256,384]{1,0:T(8,128)(2,1)}, u32[]{:S(2)}, u32[]{:S(2)}) collective-permute-start(bf16[256,384]{1,0:T(8,128)(2,1)} %slice.98), channel_id=1, source_target_pairs={{64,128},{128,64},{192,256},{256,192},{320,384},{384,320},{448,0},... | collective-permute-start | bytes 589832 | tf_op jit(solution)/shard_map/ppermute | solution.py:37
  63.6 6.4 %all-to-all-start.2 = ((bf16[8,64,768]{2,1,0:T(8,128)(2,1)}), bf16[8,64,768]{2,1,0:T(8,128)(2,1)S(1)}, u32[]{:S(2)}, u32[]{:S(2)}) async-start(bf16[8,64,768]{2,1,0:T(8,128)(2,1)} %broadcast_in_dim.11), calls=%async_computation.2 | async-start | bytes 1572864 | tf_op jit(solution)/shard_map/all_to_all | solution.py:20
  71.9 3.6 %collective-permute-start.5 = (bf16[512,384]{1,0:T(8,128)(2,1)S(1)}, bf16[512,384]{1,0:T(8,128)(2,1)S(1)}, u32[]{:S(2)}, u32[]{:S(2)}) collective-permute-start(bf16[512,384]{1,0:T(8,128)(2,1)S(1)} %slice.104), channel_id=1, source_target_pairs={{64,128},{128,64},{192,256},{256,192},{320,384},{384,320},{448,0},... | collective-permute-start | bytes 1179656 | tf_op jit(solution)/shard_map/ppermute | solution.py:36
  77.8 3.1 %collective-permute-start.9 = (bf16[512,256]{1,0:T(8,128)(2,1)S(1)}, bf16[512,256]{1,0:T(8,128)(2,1)S(1)}, u32[]{:S(2)}, u32[]{:S(2)}) collective-permute-start(bf16[512,256]{1,0:T(8,128)(2,1)S(1)} %slice.111), channel_id=1, source_target_pairs={{64,128},{128,64},{192,256},{256,192},{320,384},{384,320},{448,0},... | collective-permute-start | bytes 786440 | tf_op jit(solution)/shard_map/ppermute | solution.py:36
  92.3 3.1 %collective-permute-start.7 = (bf16[256,384]{1,0:T(8,128)(2,1)S(1)}, bf16[256,384]{1,0:T(8,128)(2,1)S(1)}, u32[]{:S(2)}, u32[]{:S(2)}) collective-permute-start(bf16[256,384]{1,0:T(8,128)(2,1)S(1)} %slice.106), channel_id=1, source_target_pairs={{0,64},{64,0},{128,192},{192,128},{256,320},{320,256},{384,448},{4... | collective-permute-start | bytes 589832 | tf_op jit(solution)/shard_map/ppermute | solution.py:38
  95.5 3.6 %collective-permute-start.6 = (bf16[256,384]{1,0:T(8,128)(2,1)S(1)}, bf16[256,384]{1,0:T(8,128)(2,1)S(1)}, u32[]{:S(2)}, u32[]{:S(2)}) collective-permute-start(bf16[256,384]{1,0:T(8,128)(2,1)S(1)} %slice.105), channel_id=1, source_target_pairs={{64,128},{128,64},{192,256},{256,192},{320,384},{384,320},{448,0},... | collective-permute-start | bytes 589832 | tf_op jit(solution)/shard_map/ppermute | solution.py:37
  100.0 3.1 %collective-permute-done.6 = bf16[256,384]{1,0:T(8,128)(2,1)S(1)} collective-permute-done((bf16[256,384]{1,0:T(8,128)(2,1)S(1)}, bf16[256,384]{1,0:T(8,128)(2,1)S(1)}, u32[]{:S(2)}, u32[]{:S(2)}) %collective-permute-start.6) | collective-permute-done | bytes 196640 | tf_op jit(solution)/shard_map/ppermute | solution.py:37
  107.4 6.5 %collective-permute-start.12 = (bf16[4,24,2048]{2,1,0:T(8,128)(2,1)S(1)}, bf16[4,24,2048]{2,1,0:T(8,128)(2,1)S(1)}, u32[]{:S(2)}, u32[]{:S(2)}) collective-permute-start(bf16[4,24,2048]{2,1,0:T(8,128)(2,1)S(1)} %dynamic-slice_bitcast_fusion.1), channel_id=1, source_target_pairs={{0,1},{1,0},{2,3},{3,2},{4,5},{5,4},{6,7},{7,6},{8,9},{9,8},{10,11... | collective-permute-start | bytes 1179656 | tf_op jit(solution)/shard_map/ppermute | solution.py:76
  115.9 4.3 %collective-permute-start.21 = (bf16[64,384]{1,0:T(8,128)(2,1)S(1)}, bf16[64,384]{1,0:T(8,128)(2,1)S(1)}, u32[]{:S(2)}, u32[]{:S(2)}) collective-permute-start(bf16[64,384]{1,0:T(8,128)(2,1)S(1)} %get-tuple-element.30), channel_id=1, source_target_pairs={{64,128},{128,64},{192,256},{256,192},{320,384},{384,320},{448,0},... | collective-permute-start | bytes 147464 | tf_op jit(solution)/shard_map/ppermute | solution.py:36
  120.2 3.2 %collective-permute-start.22 = (bf16[32,384]{1,0:T(8,128)(2,1)S(1)}, bf16[32,384]{1,0:T(8,128)(2,1)S(1)}, u32[]{:S(2)}, u32[]{:S(2)}) collective-permute-start(bf16[32,384]{1,0:T(8,128)(2,1)S(1)} %slice.118), channel_id=1, source_target_pairs={{64,128},{128,64},{192,256},{256,192},{320,384},{384,320},{448,0},... | collective-permute-start | bytes 73736 | tf_op jit(solution)/shard_map/ppermute | solution.py:37
  130.0 3.5 %collective-permute-start.17 = (bf16[512,768]{1,0:T(8,128)(2,1)S(1)}, bf16[512,768]{1,0:T(8,128)(2,1)}, u32[]{:S(2)}, u32[]{:S(2)}) collective-permute-start(bf16[512,768]{1,0:T(8,128)(2,1)S(1)} %bitcast.112), channel_id=1, source_target_pairs={{64,128},{128,64},{192,256},{256,192},{320,384},{384,320},{448,0},... | collective-permute-start | bytes 2359304 | tf_op jit(solution)/shard_map/ppermute | solution.py:36
  137.4 3.7 %collective-permute-start.14 = (bf16[24,2048]{1,0:T(8,128)(2,1)S(1)}, bf16[24,2048]{1,0:T(8,128)(2,1)S(1)}, u32[]{:S(2)}, u32[]{:S(2)}) collective-permute-start(bf16[24,2048]{1,0:T(8,128)(2,1)S(1)} %get-tuple-element.16), channel_id=1, source_target_pairs={{0,6},{2,0},{4,2},{6,4},{1,7},{3,1},{5,3},{7,5},{8,14},{10,8},{12,... | collective-permute-start | bytes 294920 | tf_op jit(solution)/shard_map/ppermute | solution.py:83
  145.1 6.7 %all-to-all-start.3 = ((bf16[8,4,64,384]{3,2,1,0:T(8,128)(2,1)}), bf16[8,4,64,384]{3,2,1,0:T(8,128)(2,1)S(1)}, u32[]{:S(2)}, u32[]{:S(2)}) async-start(bf16[8,4,64,384]{3,2,1,0:T(8,128)(2,1)} %broadcast_in_dim.12), calls=%async_computation.3 | async-start | bytes 3145728 | tf_op jit(solution)/shard_map/all_to_all | solution.py:20
  160.3 17.7 %all_gather.7 = bf16[192,2048]{1,0:T(8,128)(2,1)S(1)} all-gather(bf16[24,2048]{1,0:T(8,128)(2,1)S(1)} %fusion.18), channel_id=1, replica_groups=mesh['rep'=2,'z'=4,'y'=8,'x'=4,'core'=2] {'x','core'}, dimensions={0}, use_global_device_ids=true | all-gather | bytes 884736 | tf_op jit(solution)/shard_map/all_gather | solution.py:173
  181.8 8.1 %all-to-all-done.3 = bf16[8,4,64,384]{3,2,1,0:T(8,128)(2,1)S(1)} async-done(((bf16[8,4,64,384]{3,2,1,0:T(8,128)(2,1)}), bf16[8,4,64,384]{3,2,1,0:T(8,128)(2,1)S(1)}, u32[]{:S(2)}, u32[]{:S(2)}) %all-to-all-start.3) | async-done | bytes 1572896 | tf_op jit(solution)/shard_map/all_to_all | solution.py:20
  190.9 4.6 %collective-permute-start.24 = (bf16[4,24,2048]{2,1,0:T(8,128)(2,1)S(1)}, bf16[4,24,2048]{2,1,0:T(8,128)(2,1)S(1)}, u32[]{:S(2)}, u32[]{:S(2)}) collective-permute-start(bf16[4,24,2048]{2,1,0:T(8,128)(2,1)S(1)} %dynamic-slice_bitcast_fusion), channel_id=1, source_target_pairs={{0,1},{1,0},{2,3},{3,2},{4,5},{5,4},{6,7},{7,6},{8,9},{9,8},{10,11... | collective-permute-start | bytes 1179656 | tf_op jit(solution)/shard_map/ppermute | solution.py:76
  199.8 3.7 %collective-permute-start.26 = (bf16[24,2048]{1,0:T(8,128)(2,1)S(1)}, bf16[24,2048]{1,0:T(8,128)(2,1)S(1)}, u32[]{:S(2)}, u32[]{:S(2)}) collective-permute-start(bf16[24,2048]{1,0:T(8,128)(2,1)S(1)} %get-tuple-element.13), channel_id=1, source_target_pairs={{0,6},{2,0},{4,2},{6,4},{1,7},{3,1},{5,3},{7,5},{8,14},{10,8},{12,... | collective-permute-start | bytes 294920 | tf_op jit(solution)/shard_map/ppermute | solution.py:83
  203.5 3.0 %collective-permute-start.27 = (bf16[24,2048]{1,0:T(8,128)(2,1)S(1)}, bf16[24,2048]{1,0:T(8,128)(2,1)S(1)}, u32[]{:S(2)}, u32[]{:S(2)}) collective-permute-start(bf16[24,2048]{1,0:T(8,128)(2,1)S(1)} %get-tuple-element.12), channel_id=1, source_target_pairs={{0,4},{2,6},{4,0},{6,2},{1,5},{3,7},{5,1},{7,3},{8,12},{10,14},{12... | collective-permute-start | bytes 294920 | tf_op jit(solution)/shard_map/ppermute | solution.py:83
  206.6 3.8 %collective-permute-done.27 = bf16[24,2048]{1,0:T(8,128)(2,1)S(1)} collective-permute-done((bf16[24,2048]{1,0:T(8,128)(2,1)S(1)}, bf16[24,2048]{1,0:T(8,128)(2,1)S(1)}, u32[]{:S(2)}, u32[]{:S(2)}) %collective-permute-start.27) | collective-permute-done | bytes 98336 | tf_op jit(solution)/shard_map/ppermute | solution.py:83
  (161 shorter events, 68.2 us)
Async XLA Ops:
  2.5 23.9 %all-to-all-start = ((bf16[8,64,384]{2,1,0:T(8,128)(2,1)}), bf16[8,64,384]{2,1,0:T(8,128)(2,1)S(1)}, u32[]{:S(2)}, u32[]{:S(2)}) async-start(bf16[8,64,384]{2,1,0:T(8,128)(2,1)} %broadcast_in_dim.9), calls=%async_computation | async-start | bytes 786432 | tf_op jit(solution)/shard_map/all_to_all | solution.py:20
  27.3 35.3 %all-to-all-start.1 = ((bf16[8,64,640]{2,1,0:T(8,128)(2,1)}), bf16[8,64,640]{2,1,0:T(8,128)(2,1)S(1)}, u32[]{:S(2)}, u32[]{:S(2)}) async-start(bf16[8,64,640]{2,1,0:T(8,128)(2,1)} %broadcast_in_dim.10), calls=%async_computation.1 | async-start | bytes 1310720 | tf_op jit(solution)/shard_map/all_to_all | solution.py:20
  34.4 22.9 %collective-permute-start = (bf16[512,384]{1,0:T(8,128)(2,1)S(1)}, bf16[512,384]{1,0:T(8,128)(2,1)S(1)}, u32[]{:S(2)}, u32[]{:S(2)}) collective-permute-start(bf16[512,384]{1,0:T(8,128)(2,1)S(1)} %bitcast.115), channel_id=1, source_target_pairs={{0,64},{64,0},{128,192},{192,128},{256,320},{320,256},{384,448},{4... | collective-permute-start | bytes 1179656 | tf_op jit(solution)/shard_map/ppermute | solution.py:35
  37.1 17.6 %collective-permute-start.1 = (bf16[512,384]{1,0:T(8,128)(2,1)S(1)}, bf16[512,384]{1,0:T(8,128)(2,1)S(1)}, u32[]{:S(2)}, u32[]{:S(2)}) collective-permute-start(bf16[512,384]{1,0:T(8,128)(2,1)S(1)} %bitcast.116), channel_id=1, source_target_pairs={{64,128},{128,64},{192,256},{256,192},{320,384},{384,320},{448,0},... | collective-permute-start | bytes 1179656 | tf_op jit(solution)/shard_map/ppermute | solution.py:36
  55.4 22.4 %collective-permute-start.3 = (bf16[256,384]{1,0:T(8,128)(2,1)}, bf16[256,384]{1,0:T(8,128)(2,1)}, u32[]{:S(2)}, u32[]{:S(2)}) collective-permute-start(bf16[256,384]{1,0:T(8,128)(2,1)} %slice.99), channel_id=1, source_target_pairs={{0,64},{64,0},{128,192},{192,128},{256,320},{320,256},{384,448},{4... | collective-permute-start | bytes 589832 | tf_op jit(solution)/shard_map/ppermute | solution.py:38
  58.1 24.0 %collective-permute-start.2 = (bf16[256,384]{1,0:T(8,128)(2,1)}, bf16[256,384]{1,0:T(8,128)(2,1)}, u32[]{:S(2)}, u32[]{:S(2)}) collective-permute-start(bf16[256,384]{1,0:T(8,128)(2,1)} %slice.98), channel_id=1, source_target_pairs={{64,128},{128,64},{192,256},{256,192},{320,384},{384,320},{448,0},... | collective-permute-start | bytes 589832 | tf_op jit(solution)/shard_map/ppermute | solution.py:37
  63.6 64.4 %all-to-all-start.2 = ((bf16[8,64,768]{2,1,0:T(8,128)(2,1)}), bf16[8,64,768]{2,1,0:T(8,128)(2,1)S(1)}, u32[]{:S(2)}, u32[]{:S(2)}) async-start(bf16[8,64,768]{2,1,0:T(8,128)(2,1)} %broadcast_in_dim.11), calls=%async_computation.2 | async-start | bytes 1572864 | tf_op jit(solution)/shard_map/all_to_all | solution.py:20
  70.0 25.4 %collective-permute-start.4 = (bf16[512,384]{1,0:T(8,128)(2,1)S(1)}, bf16[512,384]{1,0:T(8,128)(2,1)S(1)}, u32[]{:S(2)}, u32[]{:S(2)}) collective-permute-start(bf16[512,384]{1,0:T(8,128)(2,1)S(1)} %slice.104), channel_id=1, source_target_pairs={{0,64},{64,0},{128,192},{192,128},{256,320},{320,256},{384,448},{4... | collective-permute-start | bytes 1179656 | tf_op jit(solution)/shard_map/ppermute | solution.py:35
  71.9 20.3 %collective-permute-start.5 = (bf16[512,384]{1,0:T(8,128)(2,1)S(1)}, bf16[512,384]{1,0:T(8,128)(2,1)S(1)}, u32[]{:S(2)}, u32[]{:S(2)}) collective-permute-start(bf16[512,384]{1,0:T(8,128)(2,1)S(1)} %slice.104), channel_id=1, source_target_pairs={{64,128},{128,64},{192,256},{256,192},{320,384},{384,320},{448,0},... | collective-permute-start | bytes 1179656 | tf_op jit(solution)/shard_map/ppermute | solution.py:36
  75.6 10.2 %collective-permute-start.8 = (bf16[512,256]{1,0:T(8,128)(2,1)S(1)}, bf16[512,256]{1,0:T(8,128)(2,1)S(1)}, u32[]{:S(2)}, u32[]{:S(2)}) collective-permute-start(bf16[512,256]{1,0:T(8,128)(2,1)S(1)} %slice.111), channel_id=1, source_target_pairs={{0,64},{64,0},{128,192},{192,128},{256,320},{320,256},{384,448},{4... | collective-permute-start | bytes 786440 | tf_op jit(solution)/shard_map/ppermute | solution.py:35
  77.8 11.6 %collective-permute-start.9 = (bf16[512,256]{1,0:T(8,128)(2,1)S(1)}, bf16[512,256]{1,0:T(8,128)(2,1)S(1)}, u32[]{:S(2)}, u32[]{:S(2)}) collective-permute-start(bf16[512,256]{1,0:T(8,128)(2,1)S(1)} %slice.111), channel_id=1, source_target_pairs={{64,128},{128,64},{192,256},{256,192},{320,384},{384,320},{448,0},... | collective-permute-start | bytes 786440 | tf_op jit(solution)/shard_map/ppermute | solution.py:36
  86.5 19.4 %collective-permute-start.10 = (bf16[256,256]{1,0:T(8,128)(2,1)}, bf16[256,256]{1,0:T(8,128)(2,1)}, u32[]{:S(2)}, u32[]{:S(2)}) collective-permute-start(bf16[256,256]{1,0:T(8,128)(2,1)} %slice.112), channel_id=1, source_target_pairs={{64,128},{128,64},{192,256},{256,192},{320,384},{384,320},{448,0},... | collective-permute-start | bytes 393224 | tf_op jit(solution)/shard_map/ppermute | solution.py:37
  90.1 17.1 %collective-permute-start.11 = (bf16[256,256]{1,0:T(8,128)(2,1)}, bf16[256,256]{1,0:T(8,128)(2,1)S(1)}, u32[]{:S(2)}, u32[]{:S(2)}) collective-permute-start(bf16[256,256]{1,0:T(8,128)(2,1)} %slice.113), channel_id=1, source_target_pairs={{0,64},{64,0},{128,192},{192,128},{256,320},{320,256},{384,448},{4... | collective-permute-start | bytes 393224 | tf_op jit(solution)/shard_map/ppermute | solution.py:38
  95.5 7.6 %collective-permute-start.6 = (bf16[256,384]{1,0:T(8,128)(2,1)S(1)}, bf16[256,384]{1,0:T(8,128)(2,1)S(1)}, u32[]{:S(2)}, u32[]{:S(2)}) collective-permute-start(bf16[256,384]{1,0:T(8,128)(2,1)S(1)} %slice.105), channel_id=1, source_target_pairs={{64,128},{128,64},{192,256},{256,192},{320,384},{384,320},{448,0},... | collective-permute-start | bytes 589832 | tf_op jit(solution)/shard_map/ppermute | solution.py:37
  107.4 26.0 %collective-permute-start.12 = (bf16[4,24,2048]{2,1,0:T(8,128)(2,1)S(1)}, bf16[4,24,2048]{2,1,0:T(8,128)(2,1)S(1)}, u32[]{:S(2)}, u32[]{:S(2)}) collective-permute-start(bf16[4,24,2048]{2,1,0:T(8,128)(2,1)S(1)} %dynamic-slice_bitcast_fusion.1), channel_id=1, source_target_pairs={{0,1},{1,0},{2,3},{3,2},{4,5},{5,4},{6,7},{7,6},{8,9},{9,8},{10,11... | collective-permute-start | bytes 1179656 | tf_op jit(solution)/shard_map/ppermute | solution.py:76
  128.0 23.7 %collective-permute-start.16 = (bf16[512,768]{1,0:T(8,128)(2,1)S(1)}, bf16[512,768]{1,0:T(8,128)(2,1)}, u32[]{:S(2)}, u32[]{:S(2)}) collective-permute-start(bf16[512,768]{1,0:T(8,128)(2,1)S(1)} %bitcast.111), channel_id=1, source_target_pairs={{0,64},{64,0},{128,192},{192,128},{256,320},{320,256},{384,448},{4... | collective-permute-start | bytes 2359304 | tf_op jit(solution)/shard_map/ppermute | solution.py:35
  130.0 25.8 %collective-permute-start.17 = (bf16[512,768]{1,0:T(8,128)(2,1)S(1)}, bf16[512,768]{1,0:T(8,128)(2,1)}, u32[]{:S(2)}, u32[]{:S(2)}) collective-permute-start(bf16[512,768]{1,0:T(8,128)(2,1)S(1)} %bitcast.112), channel_id=1, source_target_pairs={{64,128},{128,64},{192,256},{256,192},{320,384},{384,320},{448,0},... | collective-permute-start | bytes 2359304 | tf_op jit(solution)/shard_map/ppermute | solution.py:36
  134.5 24.4 %collective-permute-start.13 = (bf16[24,2048]{1,0:T(8,128)(2,1)S(1)}, bf16[24,2048]{1,0:T(8,128)(2,1)S(1)}, u32[]{:S(2)}, u32[]{:S(2)}) collective-permute-start(bf16[24,2048]{1,0:T(8,128)(2,1)S(1)} %get-tuple-element.14), channel_id=1, source_target_pairs={{0,2},{2,4},{4,6},{6,0},{1,3},{3,5},{5,7},{7,1},{8,10},{10,12},{12... | collective-permute-start | bytes 294920 | tf_op jit(solution)/shard_map/ppermute | solution.py:83
  137.4 21.6 %collective-permute-start.14 = (bf16[24,2048]{1,0:T(8,128)(2,1)S(1)}, bf16[24,2048]{1,0:T(8,128)(2,1)S(1)}, u32[]{:S(2)}, u32[]{:S(2)}) collective-permute-start(bf16[24,2048]{1,0:T(8,128)(2,1)S(1)} %get-tuple-element.16), channel_id=1, source_target_pairs={{0,6},{2,0},{4,2},{6,4},{1,7},{3,1},{5,3},{7,5},{8,14},{10,8},{12,... | collective-permute-start | bytes 294920 | tf_op jit(solution)/shard_map/ppermute | solution.py:83
  141.0 17.9 %collective-permute-start.15 = (bf16[24,2048]{1,0:T(8,128)(2,1)S(1)}, bf16[24,2048]{1,0:T(8,128)(2,1)S(1)}, u32[]{:S(2)}, u32[]{:S(2)}) collective-permute-start(bf16[24,2048]{1,0:T(8,128)(2,1)S(1)} %get-tuple-element.15), channel_id=1, source_target_pairs={{0,4},{2,6},{4,0},{6,2},{1,5},{3,7},{5,1},{7,3},{8,12},{10,14},{12... | collective-permute-start | bytes 294920 | tf_op jit(solution)/shard_map/ppermute | solution.py:83
  145.1 44.9 %all-to-all-start.3 = ((bf16[8,4,64,384]{3,2,1,0:T(8,128)(2,1)}), bf16[8,4,64,384]{3,2,1,0:T(8,128)(2,1)S(1)}, u32[]{:S(2)}, u32[]{:S(2)}) async-start(bf16[8,4,64,384]{3,2,1,0:T(8,128)(2,1)} %broadcast_in_dim.12), calls=%async_computation.3 | async-start | bytes 3145728 | tf_op jit(solution)/shard_map/all_to_all | solution.py:20
  152.8 27.0 %collective-permute-start.18 = (bf16[256,768]{1,0:T(8,128)(2,1)S(1)}, bf16[256,768]{1,0:T(8,128)(2,1)S(1)}, u32[]{:S(2)}, u32[]{:S(2)}) collective-permute-start(bf16[256,768]{1,0:T(8,128)(2,1)S(1)} %slice.114), channel_id=1, source_target_pairs={{64,128},{128,64},{192,256},{256,192},{320,384},{384,320},{448,0},... | collective-permute-start | bytes 1179656 | tf_op jit(solution)/shard_map/ppermute | solution.py:37
  156.8 23.2 %collective-permute-start.19 = (bf16[256,768]{1,0:T(8,128)(2,1)S(1)}, bf16[256,768]{1,0:T(8,128)(2,1)S(1)}, u32[]{:S(2)}, u32[]{:S(2)}) collective-permute-start(bf16[256,768]{1,0:T(8,128)(2,1)S(1)} %slice.115), channel_id=1, source_target_pairs={{0,64},{64,0},{128,192},{192,128},{256,320},{320,256},{384,448},{4... | collective-permute-start | bytes 1179656 | tf_op jit(solution)/shard_map/ppermute | solution.py:38
  197.0 9.5 %collective-permute-start.25 = (bf16[24,2048]{1,0:T(8,128)(2,1)S(1)}, bf16[24,2048]{1,0:T(8,128)(2,1)S(1)}, u32[]{:S(2)}, u32[]{:S(2)}) collective-permute-start(bf16[24,2048]{1,0:T(8,128)(2,1)S(1)} %get-tuple-element.11), channel_id=1, source_target_pairs={{0,2},{2,4},{4,6},{6,0},{1,3},{3,5},{5,7},{7,1},{8,10},{10,12},{12... | collective-permute-start | bytes 294920 | tf_op jit(solution)/shard_map/ppermute | solution.py:83
  (28 other events, 205.4 us)
where the time goes:
time: 213 us; the launch traced here: 211 us
  starting transfers between devices  119 us (56%)
  blocking collectives  33.6 us (16%)
  waiting for transfers between devices  27.7 us (13%)
  matrix products  11.2 us (5%)
  local copies, waits for them, and re-layouts  9.97 us (5%)
  other arithmetic  7.79 us (4%)
    all_to_all x4, starting transfers between devices, exchange_y(): lax.all_to_all(jnp.broadcast_to(array[None], (peers, *array.shape)), 'y',...  27.5 us
    ppermute x5, starting transfers between devices, ring_pieces(): odd = lax.ppermute(block, RING, pairs(1))  23.4 us
    ppermute x6, starting transfers between devices, sum_at_owner(): lax.ppermute(block, 'x', [(i, (i + step) % chips) for i in range(chips)])  18.6 us
    all_gather x1, blocking collectives, per_device(): mlp_in = lax.all_gather(mlp_in, TP, axis=0, tiled=True)  17.7 us
    ppermute x5, starting transfers between devices, ring_pieces(): far_a = lax.ppermute(even[:half], RING, pairs(1))  17 us
    all_gather x1, blocking collectives, per_device(): all_rows = lax.all_gather(own_rows, TP, axis=0, tiled=True)  15.9 us
    ppermute x5, starting transfers between devices, ring_pieces(): far_b = lax.ppermute(odd[half:], RING, pairs(0))  11.3 us
    ppermute x2, starting transfers between devices, sum_at_owner(): got = lax.ppermute(sent, 'core', [(0, 1), (1, 0)])  11.1 us
  transfers between devices with their start and end apart: 32, of which 9 were waited for; matrix products, arithmetic and copies ran while one was open for 11% of the time, Pallas kernels for 0%

commit v1 on v0

--- a/solution.py
+++ b/solution.py
@@ -1,6 +1,8 @@
 import jax
 import jax.numpy as jnp
 from jax import lax
+from jax.experimental import pallas as pl
+from jax.experimental.pallas import tpu as pltpu
 from jax.sharding import Mesh, PartitionSpec as P
 
 
@@ -69,20 +71,56 @@
 
 
 def sum_at_owner(partial):
-    chips = lax.axis_size("x")
-    core, chip = lax.axis_index("core"), lax.axis_index("x")
-    blocks = partial.reshape(chips, 2, -1, partial.shape[1])
-    sent = lax.dynamic_index_in_dim(blocks, 1 - core, 1, keepdims=False)
-    got = lax.ppermute(sent, "core", [(0, 1), (1, 0)])
-    kept = lax.dynamic_index_in_dim(blocks, core, 1, keepdims=False)
-    both = kept.astype(jnp.float32) + got.astype(jnp.float32)
-    total = lax.dynamic_index_in_dim(both, chip, 0, keepdims=False)
-    both = both.astype(jnp.bfloat16)
-    for step in (1, 3, 2):
-        block = lax.dynamic_index_in_dim(both, (chip + step) % chips, 0, keepdims=False)
-        got = lax.ppermute(block, "x", [(i, (i + step) % chips) for i in range(chips)])
-        total = total + got.astype(jnp.float32)
-    return total
+    blocks = partial.reshape(lax.axis_size(TP), -1, partial.shape[1])
+    return jnp.sum(lax.all_to_all(blocks, TP, 0, 0, tiled=True).astype(jnp.float32), axis=0)
+
+
+def mlp_kernel(labels, x, weights, scale_gate, scale_up, out, held, sems):
+    units = scale_gate.shape[1]
+    copies = [
+        pltpu.make_async_copy(weights.at[:, p], held.at[p], sems.at[p]) for p in range(4)
+    ]
+    for copy in copies:
+        copy.start()
+    size = x.shape[1] // 4
+    both = jnp.zeros((x.shape[0], 2 * units), jnp.float32)
+    places = [pl.ds(pl.multiple_of(labels[p] * size, size), size) for p in range(4)]
+    for p in range(4):
+        copies[p].wait()
+        piece = held[p, :, :, : 2 * units].reshape(size, 2 * units)
+        both += jnp.dot(x[:, places[p]], piece, preferred_element_type=jnp.float32)
+    gate = both[:, :units] * scale_gate[...]
+    up = both[:, units:] * scale_up[...]
+    inner = (gate / (1.0 + jnp.exp(-gate)) * up).astype(jnp.bfloat16)
+    for p in range(4):
+        piece = held[p, :, :, 2 * units :].reshape(size, units)
+        out[:, places[p]] = dot_t(inner, piece).astype(jnp.bfloat16)
+
+
+def mlp(labels, x, weights, scale_gate, scale_up):
+    vmem = pl.BlockSpec(memory_space=pltpu.VMEM)
+    flops = 2 * x.shape[0] * x.shape[1] * weights.shape[-1]
+    return pl.pallas_call(
+        mlp_kernel,
+        out_shape=jax.ShapeDtypeStruct(x.shape, jnp.bfloat16),
+        in_specs=[
+            pl.BlockSpec(memory_space=pltpu.SMEM),
+            vmem,
+            pl.BlockSpec(memory_space=pl.ANY),
+            vmem,
+            vmem,
+        ],
+        out_specs=vmem,
+        scratch_shapes=[
+            pltpu.VMEM((4, weights.shape[0], *weights.shape[2:]), jnp.bfloat16),
+            pltpu.SemaphoreType.DMA((4,)),
+        ],
+        compiler_params=pltpu.CompilerParams(vmem_limit_bytes=20 * 2**20),
+        cost_estimate=pl.CostEstimate(
+            flops=flops, bytes_accessed=2 * weights.size, transcendentals=0
+        ),
+        name="mlp",
+    )(labels, x, weights, scale_gate[None], scale_up[None])
 
 
 def rotary(values, cosine, sine):
@@ -118,38 +156,29 @@
     own_rows = tokens[0]
     rows, width = own_rows.shape
     length = rows * lax.axis_size(TP)
-    cols = HEAD_DIM + HEAD_DIM // 2
-
-    qkv = jnp.concatenate([w_query, w_key, w_value], axis=1).astype(bf16)
-    first = exchange_y(qkv[:, :cols]).reshape(-1, cols)
-    second = exchange_y(jnp.concatenate([qkv[:, cols:], w_out.T.astype(bf16)], axis=1))
-    second = second.reshape(-1, cols + HEAD_DIM)
-    first = ring_pieces(first)
-    out_own = second[:, cols:]
-    second = ring_pieces(second[:, :cols])
-    out_pieces = ring_pieces(out_own)
-    units = w_gate.shape[1]
-    mlp = jnp.concatenate([w_gate, w_up], axis=1).astype(bf16)
-    mlp = exchange_y(mlp).reshape(-1, mlp.shape[1])
-    mlp = ring_pieces(mlp)
-    own, even, odd, far_a, far_b = ring_pieces(w_down.T.astype(bf16))
-    down = jnp.stack([own, even, odd, jnp.concatenate([far_a, far_b], axis=0)])
-    down = exchange_y(down)
-    down = jnp.moveaxis(down, 0, 1).reshape(width, -1)
+    heads = 3 * HEAD_DIM
+
+    own = jnp.concatenate([w_query, w_key, w_value, w_out.T], axis=1).astype(bf16)
+    both = exchange_y(own).reshape(-1, own.shape[1])
+    own = jnp.concatenate([w_gate, w_up, w_down.T], axis=1).astype(bf16)
+    own, even, odd, far_a, far_b = ring_pieces(own)
+    own = jnp.concatenate([own, even, odd, far_a, far_b], axis=0)
+    own = own.reshape(4, -1, own.shape[1])
+    mlp_weights = lax.all_gather(own, "y", axis=0)
+    qkv = ring_pieces(both[:, :heads])
+    out_pieces = ring_pieces(both[:, heads:])
     all_rows = lax.all_gather(own_rows, TP, axis=0, tiled=True)
 
     values = all_rows.astype(f32)
     normed = (values * inv_rms(values) * mix_gain).astype(bf16)
-    first = ring_dot(normed, first)
-    second = ring_dot(normed, second)
+    product = ring_dot(normed, qkv)
     positions = jnp.arange(length, dtype=f32)
     inv_freq = 1.0 / ROPE_BASE ** (jnp.arange(0, HEAD_DIM, 2, dtype=f32) / HEAD_DIM)
     angles = positions[:, None] * inv_freq[None, :]
     cosine, sine = jnp.cos(angles), jnp.sin(angles)
-    key_raw = jnp.concatenate([first[:, HEAD_DIM:], second[:, : HEAD_DIM // 2]], axis=1)
-    query = rotary(first[:, :HEAD_DIM] * scale_query, cosine, sine).astype(bf16)
-    keyed = rotary(key_raw * scale_key, cosine, sine).astype(bf16)
-    valued = (second[:, HEAD_DIM // 2 :] * scale_value).astype(bf16)
+    query = rotary(product[:, :HEAD_DIM] * scale_query, cosine, sine).astype(bf16)
+    keyed = rotary(product[:, HEAD_DIM : 2 * HEAD_DIM] * scale_key, cosine, sine).astype(bf16)
+    valued = (product[:, 2 * HEAD_DIM :] * scale_value).astype(bf16)
     distance = positions[:, None] - positions[None, :]
     decay = jnp.where(distance >= 0.0, jnp.exp(-decay_rate[0] * jnp.maximum(distance, 0.0)), 0.0)
     weights = (dot_t(query, keyed) * decay).astype(bf16)
@@ -172,10 +201,8 @@
     mlp_in = (values * inv_rms(values) * mlp_gain).astype(bf16)
     mlp_in = lax.all_gather(mlp_in, TP, axis=0, tiled=True)
 
-    both = ring_dot(mlp_in, mlp)
-    inner = (jax.nn.silu(both[:, :units] * scale_gate) * (both[:, units:] * scale_up)).astype(bf16)
-    channel = sum_at_owner(dot_t(inner, down).astype(bf16))
-    channel = in_order(channel) * scale_down
+    labels = jnp.stack(ring_labels()).astype(jnp.int32)
+    channel = sum_at_owner(mlp(labels, mlp_in, mlp_weights, scale_gate, scale_up)) * scale_down
     return (hidden.astype(f32) + channel).astype(bf16)[None]
 
 

time: 213 us -> 184 us (0.86)
  starting transfers between devices: 119 us -> 50.9 us
  between operations: 1.8 us -> 14.6 us
  waiting for transfers between devices: 27.7 us -> 40.4 us
  blocking collectives: 33.6 us -> 45 us
  matrix products: 11.2 us -> 7.01 us
  local copies, waits for them, and re-layouts: 9.97 us -> 13.8 us
  Pallas kernels: 0 us -> 2.88 us
    ppermute x8 -> x0, starting transfers between devices: 29.6 us -> none  [the longest x6 18.6 us: sum_at_owner(): lax.ppermute(block, 'x', [(i, (i + step) % chips) for i in range(chips)])]
    all_to_all x4 -> x1, starting transfers between devices: 27.5 us -> 6.95 us  [exchange_y(): lax.all_to_all(jnp.broadcast_to(array[None], (peers, *array.shape)), 'y',...]
    all_to_all x0 -> x1, blocking collectives: none -> 14.8 us  [sum_at_owner(): lax.all_to_all(blocks, TP, 0, 0, tiled=True).astype(jnp.float32)]
    all_to_all x0 -> x1, waiting for transfers between devices: none -> 12 us  [sum_at_owner(): lax.all_to_all(blocks, TP, 0, 0, tiled=True).astype(jnp.float32)]
    ppermute x5 -> x3, starting transfers between devices: 17 us -> 5.97 us  [ring_pieces(): far_a = lax.ppermute(even[:half], RING, pairs(1))]
    ppermute x5 -> x3, waiting for transfers between devices: 2.34 us -> 11.8 us  [ring_pieces(): even = lax.ppermute(block, RING, pairs(0))]
    ppermute x5 -> x3, starting transfers between devices: 23.4 us -> 14.8 us  [ring_pieces(): odd = lax.ppermute(block, RING, pairs(1))]
    ppermute x5 -> x3, waiting for transfers between devices: 2.42 us -> 9.43 us  [ring_pieces(): far_b = lax.ppermute(odd[half:], RING, pairs(0))]
  transfers between devices with their start and end apart: 32 -> 15, of which waited for: 9 -> 7; matrix products, arithmetic and copies ran while one was open for 11% -> 12% of each run, Pallas kernels for 0% -> 0%
where the time goes in v1:
time: 184 us; the launch traced here: 183 us
  starting transfers between devices  50.9 us (28%)
  blocking collectives  45 us (24%)
  waiting for transfers between devices  40.4 us (22%)
  between operations  14.6 us (8%)
  local copies, waits for them, and re-layouts  13.8 us (8%)
  other arithmetic  8.44 us (5%)
  matrix products  7.01 us (4%)
  Pallas kernels  2.88 us (2%)
    all_gather x1, blocking collectives, per_device(): all_rows = lax.all_gather(own_rows, TP, axis=0, tiled=True)  16 us
    ppermute x3, starting transfers between devices, ring_pieces(): odd = lax.ppermute(block, RING, pairs(1))  14.8 us
    all_to_all x1, blocking collectives, sum_at_owner(): lax.all_to_all(blocks, TP, 0, 0, tiled=True).astype(jnp.float32)  14.8 us
    all_gather x1, blocking collectives, per_device(): mlp_in = lax.all_gather(mlp_in, TP, axis=0, tiled=True)  14.2 us
    all_to_all x1, waiting for transfers between devices, sum_at_owner(): lax.all_to_all(blocks, TP, 0, 0, tiled=True).astype(jnp.float32)  12 us
    ppermute x3, waiting for transfers between devices, ring_pieces(): even = lax.ppermute(block, RING, pairs(0))  11.8 us
    ppermute x3, waiting for transfers between devices, ring_pieces(): far_b = lax.ppermute(odd[half:], RING, pairs(0))  9.43 us
    ppermute x3, starting transfers between devices, ring_pieces(): even = lax.ppermute(block, RING, pairs(0))  9.16 us
  transfers between devices with their start and end apart: 15, of which 7 were waited for; matrix products, arithmetic and copies ran while one was open for 12% of the time, Pallas kernels for 0%

profile of v1, /device:TPU:1, one launch (start us, length us, event | category | flops | bytes accessed | tf_op | source)
XLA Modules:
  0.0 183.1 jit_solution(3173375902409717412)
XLA Ops:
  9.3 4.8 %collective-permute-start.8 = (bf16[64,1152]{1,0:T(8,128)(2,1)S(1)}, bf16[64,1152]{1,0:T(8,128)(2,1)S(1)}, u32[]{:S(2)}, u32[]{:S(2)}) collective-permute-start(bf16[64,1152]{1,0:T(8,128)(2,1)S(1)} %get-tuple-element.17), channel_id=1, source_target_pairs={{0,64},{64,0},{128,192},{192,128},{256,320},{320,256},{384,448},{4... | collective-permute-start | bytes 442376 | tf_op jit(solution)/shard_map/ppermute | solution.py:37
  14.1 8.8 %collective-permute-start.9 = (bf16[64,1152]{1,0:T(8,128)(2,1)S(1)}, bf16[64,1152]{1,0:T(8,128)(2,1)S(1)}, u32[]{:S(2)}, u32[]{:S(2)}) collective-permute-start(bf16[64,1152]{1,0:T(8,128)(2,1)S(1)} %get-tuple-element.17), channel_id=1, source_target_pairs={{64,128},{128,64},{192,256},{256,192},{320,384},{384,320},{448,0},... | collective-permute-start | bytes 442376 | tf_op jit(solution)/shard_map/ppermute | solution.py:38
  27.5 7.0 %all-to-all-start = ((bf16[8,64,1024]{2,1,0:T(8,128)(2,1)}), bf16[8,64,1024]{2,1,0:T(8,128)(2,1)S(1)}, u32[]{:S(2)}, u32[]{:S(2)}) async-start(bf16[8,64,1024]{2,1,0:T(8,128)(2,1)} %broadcast_in_dim.7), calls=%async_computation | async-start | bytes 2097152 | tf_op jit(solution)/shard_map/all_to_all | solution.py:22
  34.5 1.9 %collective-permute-start.10 = (bf16[32,1152]{1,0:T(8,128)(2,1)S(1)}, bf16[32,1152]{1,0:T(8,128)(2,1)S(1)}, u32[]{:S(2)}, u32[]{:S(2)}) collective-permute-start(bf16[32,1152]{1,0:T(8,128)(2,1)S(1)} %slice.73), channel_id=1, source_target_pairs={{64,128},{128,64},{192,256},{256,192},{320,384},{384,320},{448,0},... | collective-permute-start | bytes 221192 | tf_op jit(solution)/shard_map/ppermute | solution.py:39
  36.4 1.9 %collective-permute-start.11 = (bf16[32,1152]{1,0:T(8,128)(2,1)S(1)}, bf16[32,1152]{1,0:T(8,128)(2,1)S(1)}, u32[]{:S(2)}, u32[]{:S(2)}) collective-permute-start(bf16[32,1152]{1,0:T(8,128)(2,1)S(1)} %slice.74), channel_id=1, source_target_pairs={{0,64},{64,0},{128,192},{192,128},{256,320},{320,256},{384,448},{4... | collective-permute-start | bytes 221192 | tf_op jit(solution)/shard_map/ppermute | solution.py:40
  38.4 2.4 %collective-permute-done.10 = bf16[32,1152]{1,0:T(8,128)(2,1)S(1)} collective-permute-done((bf16[32,1152]{1,0:T(8,128)(2,1)S(1)}, bf16[32,1152]{1,0:T(8,128)(2,1)S(1)}, u32[]{:S(2)}, u32[]{:S(2)}) %collective-permute-start.10) | collective-permute-done | bytes 73760 | tf_op jit(solution)/shard_map/ppermute | solution.py:39
  42.7 16.0 %all-gather = bf16[1,192,2048]{2,1,0:T(8,128)(2,1)S(1)} all-gather(bf16[1,24,2048]{2,1,0:T(8,128)(2,1)S(1)} %copy-done.2), channel_id=2, replica_groups=mesh['rep'=2,'z'=4,'y'=8,'x'=4,'core'=2] {'x','core'}, dimensions={1}, use_global_device_ids=true | all-gather | bytes 884736 | tf_op jit(solution)/shard_map/all_gather | solution.py:170
  58.9 4.7 %all-to-all-done = bf16[8,64,1024]{2,1,0:T(8,128)(2,1)S(1)} async-done(((bf16[8,64,1024]{2,1,0:T(8,128)(2,1)}), bf16[8,64,1024]{2,1,0:T(8,128)(2,1)S(1)}, u32[]{:S(2)}, u32[]{:S(2)}) %all-to-all-start) | async-done | bytes 1048608 | tf_op jit(solution)/shard_map/all_to_all | solution.py:22
  66.5 3.1 %collective-permute-start.1 = (bf16[512,768]{1,0:T(8,128)(2,1)}, bf16[512,768]{1,0:T(8,128)(2,1)}, u32[]{:S(2)}, u32[]{:S(2)}) collective-permute-start(bf16[512,768]{1,0:T(8,128)(2,1)} %slice.60), channel_id=1, source_target_pairs={{64,128},{128,64},{192,256},{256,192},{320,384},{384,320},{448,0},... | collective-permute-start | bytes 2359304 | tf_op jit(solution)/shard_map/ppermute | solution.py:38
  70.6 2.4 %collective-permute-start.4 = (bf16[512,256]{1,0:T(8,128)(2,1)}, bf16[512,256]{1,0:T(8,128)(2,1)}, u32[]{:S(2)}, u32[]{:S(2)}) collective-permute-start(bf16[512,256]{1,0:T(8,128)(2,1)} %slice.70), channel_id=1, source_target_pairs={{0,64},{64,0},{128,192},{192,128},{256,320},{320,256},{384,448},{4... | collective-permute-start | bytes 786440 | tf_op jit(solution)/shard_map/ppermute | solution.py:37
  73.1 2.9 %collective-permute-start.5 = (bf16[512,256]{1,0:T(8,128)(2,1)}, bf16[512,256]{1,0:T(8,128)(2,1)}, u32[]{:S(2)}, u32[]{:S(2)}) collective-permute-start(bf16[512,256]{1,0:T(8,128)(2,1)} %slice.70), channel_id=1, source_target_pairs={{64,128},{128,64},{192,256},{256,192},{320,384},{384,320},{448,0},... | collective-permute-start | bytes 786440 | tf_op jit(solution)/shard_map/ppermute | solution.py:38
  76.7 8.6 %collective-permute-done = bf16[512,768]{1,0:T(8,128)(2,1)S(1)} collective-permute-done((bf16[512,768]{1,0:T(8,128)(2,1)}, bf16[512,768]{1,0:T(8,128)(2,1)S(1)}, u32[]{:S(2)}, u32[]{:S(2)}) %collective-permute-start) | collective-permute-done | bytes 786464 | tf_op jit(solution)/shard_map/ppermute | solution.py:37
  85.3 2.0 %collective-permute-start.2 = (bf16[256,768]{1,0:T(8,128)(2,1)S(1)}, bf16[256,768]{1,0:T(8,128)(2,1)S(1)}, u32[]{:S(2)}, u32[]{:S(2)}) collective-permute-start(bf16[256,768]{1,0:T(8,128)(2,1)S(1)} %slice.61), channel_id=1, source_target_pairs={{64,128},{128,64},{192,256},{256,192},{320,384},{384,320},{448,0},... | collective-permute-start | bytes 1179656 | tf_op jit(solution)/shard_map/ppermute | solution.py:39
  87.7 3.2 %collective-permute-done.4 = bf16[512,256]{1,0:T(8,128)(2,1)} collective-permute-done((bf16[512,256]{1,0:T(8,128)(2,1)}, bf16[512,256]{1,0:T(8,128)(2,1)}, u32[]{:S(2)}, u32[]{:S(2)}) %collective-permute-start.4) | collective-permute-done | bytes 262176 | tf_op jit(solution)/shard_map/ppermute | solution.py:37
  92.5 2.0 %collective-permute-start.6 = (bf16[256,256]{1,0:T(8,128)(2,1)}, bf16[256,256]{1,0:T(8,128)(2,1)}, u32[]{:S(2)}, u32[]{:S(2)}) collective-permute-start(bf16[256,256]{1,0:T(8,128)(2,1)} %slice.71), channel_id=1, source_target_pairs={{64,128},{128,64},{192,256},{256,192},{320,384},{384,320},{448,0},... | collective-permute-start | bytes 393224 | tf_op jit(solution)/shard_map/ppermute | solution.py:39
  96.1 2.5 %collective-permute-start.7 = (bf16[256,256]{1,0:T(8,128)(2,1)}, bf16[256,256]{1,0:T(8,128)(2,1)S(1)}, u32[]{:S(2)}, u32[]{:S(2)}) collective-permute-start(bf16[256,256]{1,0:T(8,128)(2,1)} %slice.72), channel_id=1, source_target_pairs={{0,64},{64,0},{128,192},{192,128},{256,320},{320,256},{384,448},{4... | collective-permute-start | bytes 393224 | tf_op jit(solution)/shard_map/ppermute | solution.py:40
  99.6 2.8 %collective-permute-start.3 = (bf16[256,768]{1,0:T(8,128)(2,1)S(1)}, bf16[256,768]{1,0:T(8,128)(2,1)S(1)}, u32[]{:S(2)}, u32[]{:S(2)}) collective-permute-start(bf16[256,768]{1,0:T(8,128)(2,1)S(1)} %slice.62), channel_id=1, source_target_pairs={{0,64},{64,0},{128,192},{192,128},{256,320},{320,256},{384,448},{4... | collective-permute-start | bytes 1179656 | tf_op jit(solution)/shard_map/ppermute | solution.py:40
  103.0 8.4 %collective-permute-done.3 = bf16[256,768]{1,0:T(8,128)(2,1)S(1)} collective-permute-done((bf16[256,768]{1,0:T(8,128)(2,1)S(1)}, bf16[256,768]{1,0:T(8,128)(2,1)S(1)}, u32[]{:S(2)}, u32[]{:S(2)}) %collective-permute-start.3) | collective-permute-done | bytes 393248 | tf_op jit(solution)/shard_map/ppermute | solution.py:40
  121.7 6.8 %all-to-all-start.1 = ((bf16[8,24,2048]{2,1,0:T(8,128)(2,1)}), bf16[8,24,2048]{2,1,0:T(8,128)(2,1)S(1)}, u32[]{:S(2)}, u32[]{:S(2)}) async-start(bf16[8,24,2048]{2,1,0:T(8,128)(2,1)} %constant_dynamic-update-slice_fusion), calls=%async_computation.1 | async-start | bytes 1572864 | tf_op jit(solution)/shard_map/all_to_all | solution.py:75
  128.7 12.0 %all-to-all-done.1 = bf16[8,24,2048]{2,1,0:T(8,128)(2,1)S(1)} async-done(((bf16[8,24,2048]{2,1,0:T(8,128)(2,1)}), bf16[8,24,2048]{2,1,0:T(8,128)(2,1)S(1)}, u32[]{:S(2)}, u32[]{:S(2)}) %all-to-all-start.1) | async-done | bytes 786464 | tf_op jit(solution)/shard_map/all_to_all | solution.py:75
  141.1 14.2 %all_gather.10.x = bf16[192,2048]{1,0:T(8,128)(2,1)S(1)} all-gather(bf16[24,2048]{1,0:T(8,128)(2,1)S(1)} %fusion.12), channel_id=1, replica_groups=mesh['rep'=2,'z'=4,'y'=8,'x'=4,'core'=2] {'x','core'}, dimensions={0}, use_global_device_ids=true | all-gather | bytes 884736 | tf_op jit(solution)/shard_map/all_gather | solution.py:202
  155.4 2.3 %copy-done = bf16[8,4,64,1152]{3,2,1,0:T(8,128)(2,1)S(1)} copy-done((bf16[8,4,64,1152]{3,2,1,0:T(8,128)(2,1)S(1)}, bf16[8,4,64,1152]{3,2,1,0:T(8,128)(2,1)}, u32[]{:S(2)}) %copy-start) | copy-done | bytes 4718616
  157.7 2.9 %mlp.1 = bf16[192,2048]{1,0:T(8,128)(2,1)S(1)} custom-call(s32[4]{0:T(128)S(1)} %pad_add_fusion.labels, bf16[192,2048]{1,0:T(8,128)(2,1)S(1)} %all_gather.10.x, bf16[8,4,64,1152]{3,2,1,0:T(8,128)(2,1)S(1)} %copy-done, f32[1,384]{1,0:T(1,128)S(1)} %broadcast_in_dim.8.scale_gate, f32[1,384]{1,0:T(1,128)S(1)} %broadcast_in_dim.9.scale_up), custom_call_target="tpu_custom_call" | custom-call | flops 905969664 | bytes 4718592 | tf_op jit(solution)/shard_map/mlp/pallas_call | solution.py:103
  160.6 14.8 %all_to_all.15 = bf16[8,24,2048]{2,1,0:T(8,128)(2,1)S(1)} all-to-all(bf16[8,24,2048]{2,1,0:T(8,128)(2,1)S(1)} %bitcast.51), channel_id=1, replica_groups=mesh['rep'=2,'z'=4,'y'=8,'x'=4,'core'=2] {'x','core'}, dimensions={0} | all-to-all | bytes 1572864 | tf_op jit(solution)/shard_map/all_to_all | solution.py:75
  (91 shorter events, 30.0 us)
Async XLA Ops:
  9.3 25.2 %collective-permute-start.8 = (bf16[64,1152]{1,0:T(8,128)(2,1)S(1)}, bf16[64,1152]{1,0:T(8,128)(2,1)S(1)}, u32[]{:S(2)}, u32[]{:S(2)}) collective-permute-start(bf16[64,1152]{1,0:T(8,128)(2,1)S(1)} %get-tuple-element.17), channel_id=1, source_target_pairs={{0,64},{64,0},{128,192},{192,128},{256,320},{320,256},{384,448},{4... | collective-permute-start | bytes 442376 | tf_op jit(solution)/shard_map/ppermute | solution.py:37
  14.1 22.3 %collective-permute-start.9 = (bf16[64,1152]{1,0:T(8,128)(2,1)S(1)}, bf16[64,1152]{1,0:T(8,128)(2,1)S(1)}, u32[]{:S(2)}, u32[]{:S(2)}) collective-permute-start(bf16[64,1152]{1,0:T(8,128)(2,1)S(1)} %get-tuple-element.17), channel_id=1, source_target_pairs={{64,128},{128,64},{192,256},{256,192},{320,384},{384,320},{448,0},... | collective-permute-start | bytes 442376 | tf_op jit(solution)/shard_map/ppermute | solution.py:38
  27.5 15.2 %copy-start.2 = (bf16[1,24,2048]{2,1,0:T(8,128)(2,1)S(1)}, bf16[1,24,2048]{2,1,0:T(8,128)(2,1)}, u32[]{:S(2)}) copy-start(bf16[1,24,2048]{2,1,0:T(8,128)(2,1)} %param.18) | copy-start | bytes 294916
  27.5 36.1 %all-to-all-start = ((bf16[8,64,1024]{2,1,0:T(8,128)(2,1)}), bf16[8,64,1024]{2,1,0:T(8,128)(2,1)S(1)}, u32[]{:S(2)}, u32[]{:S(2)}) async-start(bf16[8,64,1024]{2,1,0:T(8,128)(2,1)} %broadcast_in_dim.7), calls=%async_computation | async-start | bytes 2097152 | tf_op jit(solution)/shard_map/all_to_all | solution.py:22
  34.4 120.9 %all-gather.3.cloned.1.call-start = ((), (), s32[]{:S(2)}) async-start(), calls=%async_computation.3 | async-start | bytes 5308416 | tf_op jit(solution)/shard_map/all_gather | solution.py:167
  34.5 6.3 %collective-permute-start.10 = (bf16[32,1152]{1,0:T(8,128)(2,1)S(1)}, bf16[32,1152]{1,0:T(8,128)(2,1)S(1)}, u32[]{:S(2)}, u32[]{:S(2)}) collective-permute-start(bf16[32,1152]{1,0:T(8,128)(2,1)S(1)} %slice.73), channel_id=1, source_target_pairs={{64,128},{128,64},{192,256},{256,192},{320,384},{384,320},{448,0},... | collective-permute-start | bytes 221192 | tf_op jit(solution)/shard_map/ppermute | solution.py:39
  36.4 5.4 %collective-permute-start.11 = (bf16[32,1152]{1,0:T(8,128)(2,1)S(1)}, bf16[32,1152]{1,0:T(8,128)(2,1)S(1)}, u32[]{:S(2)}, u32[]{:S(2)}) collective-permute-start(bf16[32,1152]{1,0:T(8,128)(2,1)S(1)} %slice.74), channel_id=1, source_target_pairs={{0,64},{64,0},{128,192},{192,128},{256,320},{320,256},{384,448},{4... | collective-permute-start | bytes 221192 | tf_op jit(solution)/shard_map/ppermute | solution.py:40
  42.7 26.9 %copy-start.4 = (f32[2048]{0:T(1024)S(1)}, f32[2048]{0:T(1024)}, u32[]{:S(2)}) copy-start(f32[2048]{0:T(1024)} %param.19) | copy-start | bytes 24580
  64.6 20.7 %collective-permute-start = (bf16[512,768]{1,0:T(8,128)(2,1)}, bf16[512,768]{1,0:T(8,128)(2,1)S(1)}, u32[]{:S(2)}, u32[]{:S(2)}) collective-permute-start(bf16[512,768]{1,0:T(8,128)(2,1)} %slice.60), channel_id=1, source_target_pairs={{0,64},{64,0},{128,192},{192,128},{256,320},{320,256},{384,448},{4... | collective-permute-start | bytes 2359304 | tf_op jit(solution)/shard_map/ppermute | solution.py:37
  66.5 32.0 %collective-permute-start.1 = (bf16[512,768]{1,0:T(8,128)(2,1)}, bf16[512,768]{1,0:T(8,128)(2,1)}, u32[]{:S(2)}, u32[]{:S(2)}) collective-permute-start(bf16[512,768]{1,0:T(8,128)(2,1)} %slice.60), channel_id=1, source_target_pairs={{64,128},{128,64},{192,256},{256,192},{320,384},{384,320},{448,0},... | collective-permute-start | bytes 2359304 | tf_op jit(solution)/shard_map/ppermute | solution.py:38
  70.6 20.2 %collective-permute-start.4 = (bf16[512,256]{1,0:T(8,128)(2,1)}, bf16[512,256]{1,0:T(8,128)(2,1)}, u32[]{:S(2)}, u32[]{:S(2)}) collective-permute-start(bf16[512,256]{1,0:T(8,128)(2,1)} %slice.70), channel_id=1, source_target_pairs={{0,64},{64,0},{128,192},{192,128},{256,320},{320,256},{384,448},{4... | collective-permute-start | bytes 786440 | tf_op jit(solution)/shard_map/ppermute | solution.py:37
  73.1 21.4 %collective-permute-start.5 = (bf16[512,256]{1,0:T(8,128)(2,1)}, bf16[512,256]{1,0:T(8,128)(2,1)}, u32[]{:S(2)}, u32[]{:S(2)}) collective-permute-start(bf16[512,256]{1,0:T(8,128)(2,1)} %slice.70), channel_id=1, source_target_pairs={{64,128},{128,64},{192,256},{256,192},{320,384},{384,320},{448,0},... | collective-permute-start | bytes 786440 | tf_op jit(solution)/shard_map/ppermute | solution.py:38
  85.3 17.4 %collective-permute-start.2 = (bf16[256,768]{1,0:T(8,128)(2,1)S(1)}, bf16[256,768]{1,0:T(8,128)(2,1)S(1)}, u32[]{:S(2)}, u32[]{:S(2)}) collective-permute-start(bf16[256,768]{1,0:T(8,128)(2,1)S(1)} %slice.61), channel_id=1, source_target_pairs={{64,128},{128,64},{192,256},{256,192},{320,384},{384,320},{448,0},... | collective-permute-start | bytes 1179656 | tf_op jit(solution)/shard_map/ppermute | solution.py:39
  92.5 24.7 %collective-permute-start.6 = (bf16[256,256]{1,0:T(8,128)(2,1)}, bf16[256,256]{1,0:T(8,128)(2,1)}, u32[]{:S(2)}, u32[]{:S(2)}) collective-permute-start(bf16[256,256]{1,0:T(8,128)(2,1)} %slice.71), channel_id=1, source_target_pairs={{64,128},{128,64},{192,256},{256,192},{320,384},{384,320},{448,0},... | collective-permute-start | bytes 393224 | tf_op jit(solution)/shard_map/ppermute | solution.py:39
  96.1 24.8 %collective-permute-start.7 = (bf16[256,256]{1,0:T(8,128)(2,1)}, bf16[256,256]{1,0:T(8,128)(2,1)S(1)}, u32[]{:S(2)}, u32[]{:S(2)}) collective-permute-start(bf16[256,256]{1,0:T(8,128)(2,1)} %slice.72), channel_id=1, source_target_pairs={{0,64},{64,0},{128,192},{192,128},{256,320},{320,256},{384,448},{4... | collective-permute-start | bytes 393224 | tf_op jit(solution)/shard_map/ppermute | solution.py:40
  99.6 11.8 %collective-permute-start.3 = (bf16[256,768]{1,0:T(8,128)(2,1)S(1)}, bf16[256,768]{1,0:T(8,128)(2,1)S(1)}, u32[]{:S(2)}, u32[]{:S(2)}) collective-permute-start(bf16[256,768]{1,0:T(8,128)(2,1)S(1)} %slice.62), channel_id=1, source_target_pairs={{0,64},{64,0},{128,192},{192,128},{256,320},{320,256},{384,448},{4... | collective-permute-start | bytes 1179656 | tf_op jit(solution)/shard_map/ppermute | solution.py:40
  111.6 2.0 %copy-start.11 = (f32[256]{0:T(256)S(1)}, f32[256]{0:T(256)}, u32[]{:S(2)}) copy-start(f32[256]{0:T(256)} %param.26) | copy-start | bytes 3076
  118.3 10.3 %copy-start.7 = (f32[384]{0:T(512)S(1)}, f32[384]{0:T(512)}, u32[]{:S(2)}) copy-start(f32[384]{0:T(512)} %param.33) | copy-start | bytes 4612
  118.3 10.3 %copy-start.8 = (f32[384]{0:T(512)S(1)}, f32[384]{0:T(512)}, u32[]{:S(2)}) copy-start(f32[384]{0:T(512)} %param.34) | copy-start | bytes 4612
  121.7 19.1 %copy-start.3 = (f32[2048]{0:T(1024)S(1)}, f32[2048]{0:T(1024)}, u32[]{:S(2)}) copy-start(f32[2048]{0:T(1024)} %param.27) | copy-start | bytes 24580
  121.7 19.3 %copy-start.6 = (f32[2048]{0:T(1024)S(1)}, f32[2048]{0:T(1024)}, u32[]{:S(2)}) copy-start(f32[2048]{0:T(1024)} %param.29) | copy-start | bytes 24580
  121.7 19.0 %all-to-all-start.1 = ((bf16[8,24,2048]{2,1,0:T(8,128)(2,1)}), bf16[8,24,2048]{2,1,0:T(8,128)(2,1)S(1)}, u32[]{:S(2)}, u32[]{:S(2)}) async-start(bf16[8,24,2048]{2,1,0:T(8,128)(2,1)} %constant_dynamic-update-slice_fusion), calls=%async_computation.1 | async-start | bytes 1572864 | tf_op jit(solution)/shard_map/all_to_all | solution.py:75
  155.4 2.3 %copy-start = (bf16[8,4,64,1152]{3,2,1,0:T(8,128)(2,1)S(1)}, bf16[8,4,64,1152]{3,2,1,0:T(8,128)(2,1)}, u32[]{:S(2)}) copy-start(bf16[8,4,64,1152]{3,2,1,0:T(8,128)(2,1)} %all-gather.3.cloned.1.call-done.weights) | copy-start | bytes 14155780
  160.6 14.9 %copy-start.5 = (f32[2048]{0:T(1024)S(1)}, f32[2048]{0:T(1024)}, u32[]{:S(2)}) copy-start(f32[2048]{0:T(1024)} %param.35) | copy-start | bytes 24580
  (3 other events, 3.9 us)
Sparse Core Ops, SparseCore 0:
  42.8 63.4 all-gather.2

commit v2 on v1

--- a/solution.py
+++ b/solution.py
@@ -11,6 +11,7 @@
 ROPE_BASE = 10000.0
 RING = ("rep", "z")
 TP = ("x", "core")
+CHUNKS = 4
 
 
 def inv_rms(values):
@@ -75,52 +76,53 @@
     return jnp.sum(lax.all_to_all(blocks, TP, 0, 0, tiled=True).astype(jnp.float32), axis=0)
 
 
-def mlp_kernel(labels, x, weights, scale_gate, scale_up, out, held, sems):
+def mlp_kernel(x, weights, scale_gate, scale_up, out, held, sems):
     units = scale_gate.shape[1]
-    copies = [
-        pltpu.make_async_copy(weights.at[:, p], held.at[p], sems.at[p]) for p in range(4)
-    ]
-    for copy in copies:
-        copy.start()
-    size = x.shape[1] // 4
-    both = jnp.zeros((x.shape[0], 2 * units), jnp.float32)
-    places = [pl.ds(pl.multiple_of(labels[p] * size, size), size) for p in range(4)]
-    for p in range(4):
-        copies[p].wait()
-        piece = held[p, :, :, : 2 * units].reshape(size, 2 * units)
-        both += jnp.dot(x[:, places[p]], piece, preferred_element_type=jnp.float32)
-    gate = both[:, :units] * scale_gate[...]
-    up = both[:, units:] * scale_up[...]
-    inner = (gate / (1.0 + jnp.exp(-gate)) * up).astype(jnp.bfloat16)
-    for p in range(4):
-        piece = held[p, :, :, 2 * units :].reshape(size, units)
-        out[:, places[p]] = dot_t(inner, piece).astype(jnp.bfloat16)
-
-
-def mlp(labels, x, weights, scale_gate, scale_up):
+    size = x.shape[1] // CHUNKS
+    places = [pl.ds(p * size, size) for p in range(CHUNKS)]
+
+    def fetch(r, p):
+        at = (r, places[p])
+        return pltpu.make_async_copy(weights.at[at], held.at[at], sems.at[r, p])
+
+    copies = [[fetch(r, p) for p in range(CHUNKS)] for r in range(2)]
+    for r in range(2):
+        for copy in copies[r]:
+            copy.start()
+    inner = []
+    for r in range(2):
+        both = jnp.zeros((x.shape[0], 2 * units), jnp.float32)
+        for copy, at in zip(copies[r], places):
+            copy.wait()
+            both += jnp.dot(
+                x[:, at], held[r, at, : 2 * units], preferred_element_type=jnp.float32
+            )
+        gate = both[:, :units] * scale_gate[r : r + 1]
+        up = both[:, units:] * scale_up[r : r + 1]
+        inner.append((gate / (1.0 + jnp.exp(-gate)) * up).astype(jnp.bfloat16))
+    for at in places:
+        total = dot_t(inner[0], held[0, at, 2 * units :]) + dot_t(inner[1], held[1, at, 2 * units :])
+        out[:, at] = total.astype(jnp.bfloat16)
+
+
+def mlp(x, weights, scale_gate, scale_up):
     vmem = pl.BlockSpec(memory_space=pltpu.VMEM)
-    flops = 2 * x.shape[0] * x.shape[1] * weights.shape[-1]
+    flops = 2 * x.shape[0] * weights.size
     return pl.pallas_call(
         mlp_kernel,
         out_shape=jax.ShapeDtypeStruct(x.shape, jnp.bfloat16),
-        in_specs=[
-            pl.BlockSpec(memory_space=pltpu.SMEM),
-            vmem,
-            pl.BlockSpec(memory_space=pl.ANY),
-            vmem,
-            vmem,
-        ],
+        in_specs=[vmem, pl.BlockSpec(memory_space=pltpu.HBM), vmem, vmem],
         out_specs=vmem,
         scratch_shapes=[
-            pltpu.VMEM((4, weights.shape[0], *weights.shape[2:]), jnp.bfloat16),
-            pltpu.SemaphoreType.DMA((4,)),
+            pltpu.VMEM(weights.shape, jnp.bfloat16),
+            pltpu.SemaphoreType.DMA((2, CHUNKS)),
         ],
-        compiler_params=pltpu.CompilerParams(vmem_limit_bytes=20 * 2**20),
+        compiler_params=pltpu.CompilerParams(vmem_limit_bytes=60 * 2**20),
         cost_estimate=pl.CostEstimate(
             flops=flops, bytes_accessed=2 * weights.size, transcendentals=0
         ),
         name="mlp",
-    )(labels, x, weights, scale_gate[None], scale_up[None])
+    )(x, weights, scale_gate.reshape(2, -1), scale_up.reshape(2, -1))
 
 
 def rotary(values, cosine, sine):
@@ -160,11 +162,14 @@
 
     own = jnp.concatenate([w_query, w_key, w_value, w_out.T], axis=1).astype(bf16)
     both = exchange_y(own).reshape(-1, own.shape[1])
-    own = jnp.concatenate([w_gate, w_up, w_down.T], axis=1).astype(bf16)
-    own, even, odd, far_a, far_b = ring_pieces(own)
-    own = jnp.concatenate([own, even, odd, far_a, far_b], axis=0)
-    own = own.reshape(4, -1, own.shape[1])
-    mlp_weights = lax.all_gather(own, "y", axis=0)
+    half = w_gate.shape[1] // 2
+    low = lax.axis_index("rep") == 0
+    own = [
+        jnp.where(low, w[:, :half], w[:, half:]) for w in (w_gate, w_up, w_down.T)
+    ]
+    own = jnp.concatenate(own, axis=1).astype(bf16)
+    mlp_weights = lax.all_gather(own, ("rep", "z", "y"), axis=0, tiled=True)
+    mlp_weights = mlp_weights.reshape(2, width, -1)
     qkv = ring_pieces(both[:, :heads])
     out_pieces = ring_pieces(both[:, heads:])
     all_rows = lax.all_gather(own_rows, TP, axis=0, tiled=True)
@@ -201,8 +206,7 @@
     mlp_in = (values * inv_rms(values) * mlp_gain).astype(bf16)
     mlp_in = lax.all_gather(mlp_in, TP, axis=0, tiled=True)
 
-    labels = jnp.stack(ring_labels()).astype(jnp.int32)
-    channel = sum_at_owner(mlp(labels, mlp_in, mlp_weights, scale_gate, scale_up)) * scale_down
+    channel = sum_at_owner(mlp(mlp_in, mlp_weights, scale_gate, scale_up)) * scale_down
     return (hidden.astype(f32) + channel).astype(bf16)[None]
 
 

time: 184 us -> 201 us (1.092)
  starting transfers between devices: 50.9 us -> 67.2 us
  Pallas kernels: 2.88 us -> 5.99 us
  waiting for transfers between devices: 40.4 us -> 38.1 us
    ppermute x3 -> x2, starting transfers between devices: 5.97 us -> 25.8 us  [ring_pieces(): far_a = lax.ppermute(even[:half], RING, pairs(1))]
    ppermute x3 -> x2, waiting for transfers between devices: 11.8 us -> 1.55 us  [ring_pieces(): even = lax.ppermute(block, RING, pairs(0))]
    all_to_all x1, waiting for transfers between devices: 4.69 us -> 12.5 us  [exchange_y(): lax.all_to_all(jnp.broadcast_to(array[None], (peers, *array.shape)), 'y',...]
    ppermute x3 -> x2, waiting for transfers between devices: 2.38 us -> 8.5 us  [ring_pieces(): far_a = lax.ppermute(even[:half], RING, pairs(1))]
    ppermute x3 -> x2, waiting for transfers between devices: 9.43 us -> 3.8 us  [ring_pieces(): far_b = lax.ppermute(odd[half:], RING, pairs(0))]
    unnamed x31 -> x24, local copies, waits for them, and re-layouts: 6.1 us -> 2.87 us
    pallas_call x1, Pallas kernels: 2.88 us -> 5.99 us  [mlp(): pl.pallas_call(mlp_kernel, out_shape=jax.ShapeDtypeStruct(x.shape, jnp.bf...]
    ppermute x3 -> x2, starting transfers between devices: 14.8 us -> 12.6 us  [ring_pieces(): odd = lax.ppermute(block, RING, pairs(1))]
  transfers between devices with their start and end apart: 15 -> 11, of which waited for: 7 -> 6; matrix products, arithmetic and copies ran while one was open for 12% -> 12% of each run, Pallas kernels for 0% -> 0%
where the time goes in v2:
time: 201 us; the launch traced here: 200 us
  starting transfers between devices  67.2 us (33%)
  blocking collectives  47 us (23%)
  waiting for transfers between devices  38.1 us (19%)
  between operations  14.5 us (7%)
  local copies, waits for them, and re-layouts  11.9 us (6%)
  other arithmetic  8.36 us (4%)
  matrix products  7.03 us (3%)
  Pallas kernels  5.99 us (3%)
    ppermute x2, starting transfers between devices, ring_pieces(): far_a = lax.ppermute(even[:half], RING, pairs(1))  25.8 us
    all_gather x1, blocking collectives, per_device(): all_rows = lax.all_gather(own_rows, TP, axis=0, tiled=True)  16 us
    all_to_all x1, blocking collectives, sum_at_owner(): lax.all_to_all(blocks, TP, 0, 0, tiled=True).astype(jnp.float32)  15.8 us
    all_gather x1, blocking collectives, per_device(): mlp_in = lax.all_gather(mlp_in, TP, axis=0, tiled=True)  15.3 us
    ppermute x2, starting transfers between devices, ring_pieces(): odd = lax.ppermute(block, RING, pairs(1))  12.6 us
    all_to_all x1, waiting for transfers between devices, exchange_y(): lax.all_to_all(jnp.broadcast_to(array[None], (peers, *array.shape)), 'y',...  12.5 us
    all_to_all x1, waiting for transfers between devices, sum_at_owner(): lax.all_to_all(blocks, TP, 0, 0, tiled=True).astype(jnp.float32)  10.8 us
    ppermute x2, waiting for transfers between devices, ring_pieces(): far_a = lax.ppermute(even[:half], RING, pairs(1))  8.5 us
  transfers between devices with their start and end apart: 11, of which 6 were waited for; matrix products, arithmetic and copies ran while one was open for 12% of the time, Pallas kernels for 0%

profile of v2, /device:TPU:1, one launch (start us, length us, event | category | flops | bytes accessed | tf_op | source)
XLA Modules:
  0.0 200.1 jit_solution(11572099822107234757)
XLA Ops:
  13.9 7.6 %all-to-all-start = ((bf16[8,64,1024]{2,1,0:T(8,128)(2,1)}), bf16[8,64,1024]{2,1,0:T(8,128)(2,1)S(1)}, u32[]{:S(2)}, u32[]{:S(2)}) async-start(bf16[8,64,1024]{2,1,0:T(8,128)(2,1)} %broadcast_in_dim.3), calls=%async_computation | async-start | bytes 2097152 | tf_op jit(solution)/shard_map/all_to_all | solution.py:23
  21.5 16.0 %all-gather = bf16[1,192,2048]{2,1,0:T(8,128)(2,1)S(1)} all-gather(bf16[1,24,2048]{2,1,0:T(8,128)(2,1)S(1)} %copy-done), channel_id=2, replica_groups=mesh['rep'=2,'z'=4,'y'=8,'x'=4,'core'=2] {'x','core'}, dimensions={1}, use_global_device_ids=true | all-gather | bytes 884736 | tf_op jit(solution)/shard_map/all_gather | solution.py:175
  37.8 12.5 %all-to-all-done = bf16[8,64,1024]{2,1,0:T(8,128)(2,1)S(1)} async-done(((bf16[8,64,1024]{2,1,0:T(8,128)(2,1)}), bf16[8,64,1024]{2,1,0:T(8,128)(2,1)S(1)}, u32[]{:S(2)}, u32[]{:S(2)}) %all-to-all-start) | async-done | bytes 1048608 | tf_op jit(solution)/shard_map/all_to_all | solution.py:23
  51.3 6.3 %collective-permute-start = (bf16[512,768]{1,0:T(8,128)(2,1)}, bf16[512,768]{1,0:T(8,128)(2,1)S(1)}, u32[]{:S(2)}, u32[]{:S(2)}) collective-permute-start(bf16[512,768]{1,0:T(8,128)(2,1)} %slice.76), channel_id=1, source_target_pairs={{0,64},{64,0},{128,192},{192,128},{256,320},{320,256},{384,448},{4... | collective-permute-start | bytes 2359304 | tf_op jit(solution)/shard_map/ppermute | solution.py:38
  57.6 9.5 %collective-permute-start.1 = (bf16[512,768]{1,0:T(8,128)(2,1)}, bf16[512,768]{1,0:T(8,128)(2,1)}, u32[]{:S(2)}, u32[]{:S(2)}) collective-permute-start(bf16[512,768]{1,0:T(8,128)(2,1)} %slice.76), channel_id=1, source_target_pairs={{64,128},{128,64},{192,256},{256,192},{320,384},{384,320},{448,0},... | collective-permute-start | bytes 2359304 | tf_op jit(solution)/shard_map/ppermute | solution.py:39
  68.1 1.9 collective-permute-start.4
  70.0 3.1 %collective-permute-start.5 = (bf16[512,256]{1,0:T(8,128)(2,1)}, bf16[512,256]{1,0:T(8,128)(2,1)}, u32[]{:S(2)}, u32[]{:S(2)}) collective-permute-start(bf16[512,256]{1,0:T(8,128)(2,1)} %slice.86), channel_id=1, source_target_pairs={{64,128},{128,64},{192,256},{256,192},{320,384},{384,320},{448,0},... | collective-permute-start | bytes 786440 | tf_op jit(solution)/shard_map/ppermute | solution.py:39
  73.8 1.5 collective-permute-done
  75.4 15.0 %collective-permute-start.2 = (bf16[256,768]{1,0:T(8,128)(2,1)S(1)}, bf16[256,768]{1,0:T(8,128)(2,1)S(1)}, u32[]{:S(2)}, u32[]{:S(2)}) collective-permute-start(bf16[256,768]{1,0:T(8,128)(2,1)S(1)} %slice.77), channel_id=1, source_target_pairs={{64,128},{128,64},{192,256},{256,192},{320,384},{384,320},{448,0},... | collective-permute-start | bytes 1179656 | tf_op jit(solution)/shard_map/ppermute | solution.py:40
  90.8 1.6 slice.87
  92.3 10.8 %collective-permute-start.6 = (bf16[256,256]{1,0:T(8,128)(2,1)}, bf16[256,256]{1,0:T(8,128)(2,1)}, u32[]{:S(2)}, u32[]{:S(2)}) collective-permute-start(bf16[256,256]{1,0:T(8,128)(2,1)} %slice.87), channel_id=1, source_target_pairs={{64,128},{128,64},{192,256},{256,192},{320,384},{384,320},{448,0},... | collective-permute-start | bytes 393224 | tf_op jit(solution)/shard_map/ppermute | solution.py:40
  104.1 1.6 slice.88
  105.6 1.9 collective-permute-start.7
  108.6 3.4 %collective-permute-start.3 = (bf16[256,768]{1,0:T(8,128)(2,1)S(1)}, bf16[256,768]{1,0:T(8,128)(2,1)S(1)}, u32[]{:S(2)}, u32[]{:S(2)}) collective-permute-start(bf16[256,768]{1,0:T(8,128)(2,1)S(1)} %slice.78), channel_id=1, source_target_pairs={{0,64},{64,0},{128,192},{192,128},{256,320},{320,256},{384,448},{4... | collective-permute-start | bytes 1179656 | tf_op jit(solution)/shard_map/ppermute | solution.py:41
  112.3 8.5 %collective-permute-done.2 = bf16[256,768]{1,0:T(8,128)(2,1)S(1)} collective-permute-done((bf16[256,768]{1,0:T(8,128)(2,1)S(1)}, bf16[256,768]{1,0:T(8,128)(2,1)S(1)}, u32[]{:S(2)}, u32[]{:S(2)}) %collective-permute-start.2) | collective-permute-done | bytes 393248 | tf_op jit(solution)/shard_map/ppermute | solution.py:40
  121.1 3.8 %collective-permute-done.3 = bf16[256,768]{1,0:T(8,128)(2,1)S(1)} collective-permute-done((bf16[256,768]{1,0:T(8,128)(2,1)S(1)}, bf16[256,768]{1,0:T(8,128)(2,1)S(1)}, u32[]{:S(2)}, u32[]{:S(2)}) %collective-permute-start.3) | collective-permute-done | bytes 393248 | tf_op jit(solution)/shard_map/ppermute | solution.py:41
  125.1 1.5 fusion.4
  128.0 1.2 convolution_convert_fusion.1
  131.7 1.2 convolution_convert_fusion
  135.2 7.7 %all-to-all-start.1 = ((bf16[8,24,2048]{2,1,0:T(8,128)(2,1)}), bf16[8,24,2048]{2,1,0:T(8,128)(2,1)S(1)}, u32[]{:S(2)}, u32[]{:S(2)}) async-start(bf16[8,24,2048]{2,1,0:T(8,128)(2,1)} %constant_dynamic-update-slice_fusion), calls=%async_computation.1 | async-start | bytes 1572864 | tf_op jit(solution)/shard_map/all_to_all | solution.py:76
  144.2 10.8 %all-to-all-done.1 = bf16[8,24,2048]{2,1,0:T(8,128)(2,1)S(1)} async-done(((bf16[8,24,2048]{2,1,0:T(8,128)(2,1)}), bf16[8,24,2048]{2,1,0:T(8,128)(2,1)S(1)}, u32[]{:S(2)}, u32[]{:S(2)}) %all-to-all-start.1) | async-done | bytes 786464 | tf_op jit(solution)/shard_map/all_to_all | solution.py:76
  155.5 15.3 %all_gather.10.x = bf16[192,2048]{1,0:T(8,128)(2,1)} all-gather(bf16[24,2048]{1,0:T(8,128)(2,1)S(1)} %fusion.12), channel_id=1, replica_groups=mesh['rep'=2,'z'=4,'y'=8,'x'=4,'core'=2] {'x','core'}, dimensions={0}, use_global_device_ids=true | all-gather | bytes 884736 | tf_op jit(solution)/shard_map/all_gather | solution.py:207
  170.7 6.0 %mlp.1 = bf16[192,2048]{1,0:T(8,128)(2,1)} custom-call(bf16[192,2048]{1,0:T(8,128)(2,1)} %all_gather.10.x, bf16[2,2048,576]{2,1,0:T(8,128)(2,1)} %bitcast.50, f32[2,192]{1,0:T(2,128)} %reshape.199.scale_gate, f32[2,192]{1,0:T(2,128)} %reshape.200.scale_up), custom_call_target="tpu_custom_call" | custom-call | flops 905969664 | bytes 4718592 | tf_op jit(solution)/shard_map/mlp/pallas_call | solution.py:111
  176.7 15.8 %all_to_all.15 = bf16[8,24,2048]{2,1,0:T(8,128)(2,1)S(1)} all-to-all(bf16[8,24,2048]{2,1,0:T(8,128)(2,1)} %bitcast.51), channel_id=1, replica_groups=mesh['rep'=2,'z'=4,'y'=8,'x'=4,'core'=2] {'x','core'}, dimensions={0} | all-to-all | bytes 1572864 | tf_op jit(solution)/shard_map/all_to_all | solution.py:76
  (71 shorter events, 21.2 us)
Async XLA Ops:
  6.5 164.2 %all-gather.3.cloned.1.call-start = ((), (), s32[]{:S(2)}) async-start(), calls=%async_computation.3 | async-start | bytes 5324800 | tf_op jit(solution)/shard_map/all_gather | solution.py:171
  12.7 8.8 %copy-start = (bf16[1,24,2048]{2,1,0:T(8,128)(2,1)S(1)}, bf16[1,24,2048]{2,1,0:T(8,128)(2,1)}, u32[]{:S(2)}) copy-start(bf16[1,24,2048]{2,1,0:T(8,128)(2,1)} %param.18) | copy-start | bytes 294916
  13.9 36.4 %all-to-all-start = ((bf16[8,64,1024]{2,1,0:T(8,128)(2,1)}), bf16[8,64,1024]{2,1,0:T(8,128)(2,1)S(1)}, u32[]{:S(2)}, u32[]{:S(2)}) async-start(bf16[8,64,1024]{2,1,0:T(8,128)(2,1)} %broadcast_in_dim.3), calls=%async_computation | async-start | bytes 2097152 | tf_op jit(solution)/shard_map/all_to_all | solution.py:23
  21.5 45.6 %copy-start.2 = (f32[2048]{0:T(1024)S(1)}, f32[2048]{0:T(1024)}, u32[]{:S(2)}) copy-start(f32[2048]{0:T(1024)} %param.19) | copy-start | bytes 24580
  51.3 24.1 %collective-permute-start = (bf16[512,768]{1,0:T(8,128)(2,1)}, bf16[512,768]{1,0:T(8,128)(2,1)S(1)}, u32[]{:S(2)}, u32[]{:S(2)}) collective-permute-start(bf16[512,768]{1,0:T(8,128)(2,1)} %slice.76), channel_id=1, source_target_pairs={{0,64},{64,0},{128,192},{192,128},{256,320},{320,256},{384,448},{4... | collective-permute-start | bytes 2359304 | tf_op jit(solution)/shard_map/ppermute | solution.py:38
  57.6 50.0 %collective-permute-start.1 = (bf16[512,768]{1,0:T(8,128)(2,1)}, bf16[512,768]{1,0:T(8,128)(2,1)}, u32[]{:S(2)}, u32[]{:S(2)}) collective-permute-start(bf16[512,768]{1,0:T(8,128)(2,1)} %slice.76), channel_id=1, source_target_pairs={{64,128},{128,64},{192,256},{256,192},{320,384},{384,320},{448,0},... | collective-permute-start | bytes 2359304 | tf_op jit(solution)/shard_map/ppermute | solution.py:39
  68.1 22.7 %collective-permute-start.4 = (bf16[512,256]{1,0:T(8,128)(2,1)}, bf16[512,256]{1,0:T(8,128)(2,1)}, u32[]{:S(2)}, u32[]{:S(2)}) collective-permute-start(bf16[512,256]{1,0:T(8,128)(2,1)} %slice.86), channel_id=1, source_target_pairs={{0,64},{64,0},{128,192},{192,128},{256,320},{320,256},{384,448},{4... | collective-permute-start | bytes 786440 | tf_op jit(solution)/shard_map/ppermute | solution.py:38
  70.0 34.0 %collective-permute-start.5 = (bf16[512,256]{1,0:T(8,128)(2,1)}, bf16[512,256]{1,0:T(8,128)(2,1)}, u32[]{:S(2)}, u32[]{:S(2)}) collective-permute-start(bf16[512,256]{1,0:T(8,128)(2,1)} %slice.86), channel_id=1, source_target_pairs={{64,128},{128,64},{192,256},{256,192},{320,384},{384,320},{448,0},... | collective-permute-start | bytes 786440 | tf_op jit(solution)/shard_map/ppermute | solution.py:39
  75.4 45.4 %collective-permute-start.2 = (bf16[256,768]{1,0:T(8,128)(2,1)S(1)}, bf16[256,768]{1,0:T(8,128)(2,1)S(1)}, u32[]{:S(2)}, u32[]{:S(2)}) collective-permute-start(bf16[256,768]{1,0:T(8,128)(2,1)S(1)} %slice.77), channel_id=1, source_target_pairs={{64,128},{128,64},{192,256},{256,192},{320,384},{384,320},{448,0},... | collective-permute-start | bytes 1179656 | tf_op jit(solution)/shard_map/ppermute | solution.py:40
  92.3 38.3 %collective-permute-start.6 = (bf16[256,256]{1,0:T(8,128)(2,1)}, bf16[256,256]{1,0:T(8,128)(2,1)}, u32[]{:S(2)}, u32[]{:S(2)}) collective-permute-start(bf16[256,256]{1,0:T(8,128)(2,1)} %slice.87), channel_id=1, source_target_pairs={{64,128},{128,64},{192,256},{256,192},{320,384},{384,320},{448,0},... | collective-permute-start | bytes 393224 | tf_op jit(solution)/shard_map/ppermute | solution.py:40
  105.6 28.7 %collective-permute-start.7 = (bf16[256,256]{1,0:T(8,128)(2,1)}, bf16[256,256]{1,0:T(8,128)(2,1)S(1)}, u32[]{:S(2)}, u32[]{:S(2)}) collective-permute-start(bf16[256,256]{1,0:T(8,128)(2,1)} %slice.88), channel_id=1, source_target_pairs={{0,64},{64,0},{128,192},{192,128},{256,320},{320,256},{384,448},{4... | collective-permute-start | bytes 393224 | tf_op jit(solution)/shard_map/ppermute | solution.py:41
  108.6 16.3 %collective-permute-start.3 = (bf16[256,768]{1,0:T(8,128)(2,1)S(1)}, bf16[256,768]{1,0:T(8,128)(2,1)S(1)}, u32[]{:S(2)}, u32[]{:S(2)}) collective-permute-start(bf16[256,768]{1,0:T(8,128)(2,1)S(1)} %slice.78), channel_id=1, source_target_pairs={{0,64},{64,0},{128,192},{192,128},{256,320},{320,256},{384,448},{4... | collective-permute-start | bytes 1179656 | tf_op jit(solution)/shard_map/ppermute | solution.py:41
  125.1 1.5 copy-start.7
  125.1 1.5 copy-start.8
  125.1 2.0 copy-start.9
  131.7 11.2 %copy-start.5 = (f32[384]{0:T(512)S(1)}, f32[384]{0:T(512)}, u32[]{:S(2)}) copy-start(f32[384]{0:T(512)} %param.33) | copy-start | bytes 4612
  131.7 11.8 %copy-start.6 = (f32[384]{0:T(512)S(1)}, f32[384]{0:T(512)}, u32[]{:S(2)}) copy-start(f32[384]{0:T(512)} %param.34) | copy-start | bytes 4612
  134.5 20.7 %copy-start.1 = (f32[2048]{0:T(1024)S(1)}, f32[2048]{0:T(1024)}, u32[]{:S(2)}) copy-start(f32[2048]{0:T(1024)} %param.27) | copy-start | bytes 24580
  135.2 20.2 %copy-start.4 = (f32[2048]{0:T(1024)S(1)}, f32[2048]{0:T(1024)}, u32[]{:S(2)}) copy-start(f32[2048]{0:T(1024)} %param.29) | copy-start | bytes 24580
  135.2 19.8 %all-to-all-start.1 = ((bf16[8,24,2048]{2,1,0:T(8,128)(2,1)}), bf16[8,24,2048]{2,1,0:T(8,128)(2,1)S(1)}, u32[]{:S(2)}, u32[]{:S(2)}) async-start(bf16[8,24,2048]{2,1,0:T(8,128)(2,1)} %constant_dynamic-update-slice_fusion), calls=%async_computation.1 | async-start | bytes 1572864 | tf_op jit(solution)/shard_map/all_to_all | solution.py:76
  176.7 15.9 %copy-start.3 = (f32[2048]{0:T(1024)S(1)}, f32[2048]{0:T(1024)}, u32[]{:S(2)}) copy-start(f32[2048]{0:T(1024)} %param.35) | copy-start | bytes 24580
Sparse Core Ops, SparseCore 0:
  10.3 116.7 all-gather.2

commit v3 on v0

v3 whole, which is shorter than its diff:
```python
import jax
import jax.numpy as jnp
from jax import lax
from jax.experimental import pallas as pl
from jax.experimental.pallas import tpu as pltpu
from jax.sharding import Mesh, PartitionSpec as P


HEAD_DIM = 256
EPS = 1e-06
ROPE_BASE = 10000.0
RING = ("rep", "z")
TP = ("x", "core")


def inv_rms(values):
    return lax.rsqrt(jnp.mean(values * values, axis=-1, keepdims=True) + EPS)


def pairs(offset, n=8):
    out = []
    for a in range(offset, n + offset, 2):
        b = (a + 1) % n
        out += [(a % n, b), (b, a % n)]
    return out


def ring_pieces(block):
    half = block.shape[0] // 2
    even = lax.ppermute(block, RING, pairs(0))
    odd = lax.ppermute(block, RING, pairs(1))
    far_a = lax.ppermute(even[:half], RING, pairs(1))
    far_b = lax.ppermute(odd[half:], RING, pairs(0))
    return block, even, odd, far_a, far_b


def ring_labels():
    z = lax.axis_index("z")
    odd = z % 2
    return z, z + 1 - 2 * odd, (z + 3 + 2 * odd) % 4, (z + 2) % 4


def ring_slots():
    z, even, odd, _ = ring_labels()
    return [jnp.where(z == j, 0, jnp.where(even == j, 1, jnp.where(odd == j, 2, 3))) for j in range(4)]


def ring_blocks(block):
    even = lax.ppermute(block, RING, pairs(0))
    odd = lax.ppermute(block, RING, pairs(1))
    far = lax.ppermute(block, RING, [(i, (i + 2) % 8) for i in range(8)])
    return jnp.stack([block, even, odd, far])


def ring_dot(x, pieces, columns):
    size = pieces[0].shape[0]
    half = size // 2
    own_at, even_at, odd_at, far_at = ring_labels()
    starts = (own_at * size, even_at * size, odd_at * size, far_at * size, far_at * size + half)

    def term(start, piece):
        cut = lax.dynamic_slice_in_dim(x, start, piece.shape[0], 1)
        return jnp.dot(cut, piece[:, :columns], preferred_element_type=jnp.float32)

    return sum(term(start, piece) for start, piece in zip(starts, pieces))


def dot_t(a, b):
    return lax.dot_general(a, b, (((1,), (1,)), ((), ())), preferred_element_type=jnp.float32)


def sum_at_owner(partial):
    blocks = partial.reshape(lax.axis_size(TP), -1, partial.shape[1])
    return jnp.sum(lax.all_to_all(blocks, TP, 0, 0, tiled=True).astype(jnp.float32), axis=0)


def rotary(values, cosine, sine):
    half = values.shape[-1] // 2
    first = values[:, :half]
    second = values[:, half:]
    return jnp.concatenate(
        [first * cosine - second * sine, first * sine + second * cosine], axis=-1
    )


VMEM = pl.BlockSpec(memory_space=pltpu.VMEM)
SMEM = pl.BlockSpec(memory_space=pltpu.SMEM)


def local_call(kernel, out_shape, specs, flops=0, moved=0):
    return pl.pallas_call(
        kernel,
        out_shape=out_shape,
        in_specs=specs,
        out_specs=VMEM,
        compiler_params=pltpu.CompilerParams(vmem_limit_bytes=24 * 2**20),
        cost_estimate=pl.CostEstimate(flops=flops, bytes_accessed=moved, transcendentals=0),
    )


def heads_shard_kernel(query, keyed, valued, out_w, out):
    width = query.shape[1]
    parts = [ref[...].astype(jnp.bfloat16) for ref in (query, keyed, valued, out_w)]
    for peer in range(out.shape[0]):
        for i, part in enumerate(parts):
            out[peer, :, i * width : (i + 1) * width] = part


def heads_shard(w_query, w_key, w_value, w_out, peers):
    rows, width = w_query.shape
    shape = jax.ShapeDtypeStruct((peers, rows, 4 * width), jnp.bfloat16)
    return local_call(heads_shard_kernel, shape, [VMEM] * 4, 10**7, 2**21)(
        w_query, w_key, w_value, w_out.T
    )


def mlp_shard_kernel(gate, up, down, out):
    units = gate.shape[1]
    out[:, :units] = gate[...].astype(jnp.bfloat16)
    out[:, units : 2 * units] = up[...].astype(jnp.bfloat16)
    out[:, 2 * units :] = down[...].astype(jnp.bfloat16)


def mlp_shard(w_gate, w_up, w_down):
    rows, units = w_gate.shape
    shape = jax.ShapeDtypeStruct((rows, 3 * units), jnp.bfloat16)
    return local_call(mlp_shard_kernel, shape, [VMEM] * 3, 10**7, 2**20)(w_gate, w_up, w_down.T)


def retain_kernel(rate, product, cosine, sine, sq, sk, sv, own, even, odd, far_a, far_b, out):
    width = sq.shape[1]
    cos, sin = cosine[...], sine[...]
    query = rotary(product[:, :width] * sq[...], cos, sin).astype(jnp.bfloat16)
    keyed = rotary(product[:, width : 2 * width] * sk[...], cos, sin).astype(jnp.bfloat16)
    valued = (product[:, 2 * width :] * sv[...]).astype(jnp.bfloat16)
    length = product.shape[0]
    after = lax.broadcasted_iota(jnp.int32, (length, length), 0)
    before = lax.broadcasted_iota(jnp.int32, (length, length), 1)
    distance = (after - before).astype(jnp.float32)
    decay = jnp.exp(-rate[0] * jnp.maximum(distance, 0.0))
    weights = jnp.where(distance >= 0.0, dot_t(query, keyed) * decay, 0.0).astype(jnp.bfloat16)
    retained = jnp.dot(weights, valued, preferred_element_type=jnp.float32)
    attended = (retained * inv_rms(retained)).astype(jnp.bfloat16)
    at = 0
    for piece in (own, even, odd, far_a, far_b):
        to = at + piece.shape[0]
        out[:, at:to] = dot_t(attended, piece[:, 3 * width :]).astype(jnp.bfloat16)
        at = to


def retain(rate, product, cosine, sine, scales, pieces):
    columns = sum(piece.shape[0] for piece in pieces)
    shape = jax.ShapeDtypeStruct((product.shape[0], columns), jnp.bfloat16)
    specs = [SMEM] + [VMEM] * (6 + len(pieces))
    scales = [scale[None] for scale in scales]
    return local_call(retain_kernel, shape, specs, 3 * 10**8, 2**21)(
        rate, product, cosine, sine, *scales, *pieces
    )


def mlp_kernel(labels, x, weights, scale_gate, scale_up, out):
    units = scale_gate.shape[1]
    size = x.shape[1] // 4
    both = jnp.zeros((x.shape[0], 2 * units), jnp.float32)
    places = [pl.ds(pl.multiple_of(labels[p] * size, size), size) for p in range(4)]
    for p, at in enumerate(places):
        piece = weights[:, p, :, : 2 * units].reshape(size, 2 * units)
        both += jnp.dot(x[:, at], piece, preferred_element_type=jnp.float32)
    gate = both[:, :units] * scale_gate[...]
    up = both[:, units:] * scale_up[...]
    inner = (gate / (1.0 + jnp.exp(-gate)) * up).astype(jnp.bfloat16)
    for p, at in enumerate(places):
        piece = weights[:, p, :, 2 * units :].reshape(size, units)
        out[:, at] = dot_t(inner, piece).astype(jnp.bfloat16)


def mlp(labels, x, weights, scale_gate, scale_up):
    shape = jax.ShapeDtypeStruct(x.shape, jnp.bfloat16)
    flops = 2 * x.shape[0] * x.shape[1] * weights.shape[-1]
    return local_call(mlp_kernel, shape, [SMEM] + [VMEM] * 4, flops, 2 * weights.size)(
        labels, x, weights, scale_gate[None], scale_up[None]
    )


def per_device(
    tokens,
    mix_gain,
    w_query,
    w_key,
    w_value,
    w_out,
    scale_query,
    scale_key,
    scale_value,
    scale_out,
    decay_rate,
    mlp_gain,
    w_gate,
    w_up,
    w_down,
    scale_gate,
    scale_up,
    scale_down,
):
    bf16, f32 = jnp.bfloat16, jnp.float32
    own_rows = tokens[0]
    rows, width = own_rows.shape
    length = rows * lax.axis_size(TP)
    peers = lax.axis_size("y")
    heads = heads_shard(w_query, w_key, w_value, w_out, peers)
    heads = lax.all_to_all(heads, "y", 0, 0, tiled=True).reshape(-1, heads.shape[2])
    own = ring_blocks(mlp_shard(w_gate, w_up, w_down))
    mlp_weights = lax.all_gather(own, "y", axis=0)
    heads = ring_pieces(heads)
    all_rows = lax.all_gather(own_rows, TP, axis=0, tiled=True)

    values = all_rows.astype(f32)
    normed = (values * inv_rms(values) * mix_gain).astype(bf16)
    product = ring_dot(normed, heads, 3 * HEAD_DIM)
    positions = jnp.arange(length, dtype=f32)
    inv_freq = 1.0 / ROPE_BASE ** (jnp.arange(0, HEAD_DIM, 2, dtype=f32) / HEAD_DIM)
    angles = positions[:, None] * inv_freq[None, :]
    scales = (scale_query, scale_key, scale_value)
    partial = retain(decay_rate, product, jnp.cos(angles), jnp.sin(angles), scales, heads)

    slots = ring_slots()

    def in_order(values):
        size = width // 4
        return jnp.concatenate(
            [lax.dynamic_slice_in_dim(values, slot * size, size, 1) for slot in slots], axis=1
        )

    mixed = sum_at_owner(partial)
    mixed = in_order(mixed) * scale_out
    hidden = (own_rows.astype(f32) + mixed).astype(bf16)
    values = hidden.astype(f32)
    mlp_in = (values * inv_rms(values) * mlp_gain).astype(bf16)
    mlp_in = lax.all_gather(mlp_in, TP, axis=0, tiled=True)

    labels = jnp.stack(ring_labels()).astype(jnp.int32)
    channel = sum_at_owner(mlp(labels, mlp_in, mlp_weights, scale_gate, scale_up)) * scale_down
    return (hidden.astype(f32) + channel).astype(bf16)[None]


def solution(mesh):
    grid = Mesh(mesh.devices.reshape(2, 4, 8, 4, 2), ("rep", "z", "y", "x", "core"))
    seqs, fs = ("rep", "z", "y"), ("z", "y")
    by_rows, by_cols = P(fs, TP), P(TP, fs)
    in_specs = (
        P(seqs, TP, None), P(), by_rows, by_rows, by_rows, by_cols,
        P(TP), P(TP), P(TP), P(), P(TP), P(),
        by_rows, by_rows, by_cols, P(TP), P(TP), P(),
    )

    return jax.shard_map(
        per_device, mesh=grid, in_specs=in_specs, out_specs=P(seqs, TP, None), check_vma=False
    )
```

time: 213 us -> 187 us (0.88)
  starting transfers between devices: 119 us -> 55.9 us
  waiting for transfers between devices: 27.7 us -> 55.3 us
  between operations: 1.8 us -> 14.4 us
  blocking collectives: 33.6 us -> 45.8 us
  matrix products: 11.2 us -> 1.49 us
  Pallas kernels: 0 us -> 5.18 us
  other arithmetic: 7.79 us -> 3.04 us
  local copies, waits for them, and re-layouts: 9.97 us -> 5.5 us
    all_to_all x4 -> x2, waiting for transfers between devices: 8.13 us -> 28.3 us  [the longest x1 16.3 us: per_device(): lax.all_to_all(heads, 'y', 0, 0, tiled=True).reshape(-1, heads.shape[2])]
    all_to_all x0 -> x1, blocking collectives: none -> 14.8 us  [sum_at_owner(): lax.all_to_all(blocks, TP, 0, 0, tiled=True).astype(jnp.float32)]
    ppermute x5 -> x1, starting transfers between devices: 23.4 us -> 9.04 us  [ring_pieces(): odd = lax.ppermute(block, RING, pairs(1))]
    ppermute x8 -> x3, starting transfers between devices: 29.6 us -> 15.7 us  [the longest x1 8.85 us: ring_blocks(): odd = lax.ppermute(block, RING, pairs(1))]
    all_to_all x4 -> x2, starting transfers between devices: 27.5 us -> 14.2 us  [the longest x1 7.21 us: sum_at_owner(): lax.all_to_all(blocks, TP, 0, 0, tiled=True).astype(jnp.float32)]
    dot_general x22 -> x5, matrix products: 11.2 us -> 1.49 us  [term(): return jnp.dot(cut, piece[:, :columns], preferred_element_type=jnp.float32)]
    ppermute x5 -> x1, starting transfers between devices: 11.3 us -> 2.4 us  [ring_pieces(): far_b = lax.ppermute(odd[half:], RING, pairs(0))]
    ppermute x5 -> x1, starting transfers between devices: 10.4 us -> 1.91 us  [ring_pieces(): even = lax.ppermute(block, RING, pairs(0))]
  transfers between devices with their start and end apart: 32 -> 10, of which waited for: 9 -> 7; matrix products, arithmetic and copies ran while one was open for 11% -> 2% of each run, Pallas kernels for 0% -> 2%
where the time goes in v3:
time: 187 us
  starting transfers between devices  55.9 us (30%)
  waiting for transfers between devices  55.3 us (30%)
  blocking collectives  45.8 us (24%)
  between operations  14.4 us (8%)
  local copies, waits for them, and re-layouts  5.5 us (3%)
  Pallas kernels  5.18 us (3%)
  other arithmetic  3.04 us (2%)
    all_gather x1, blocking collectives, per_device(): all_rows = lax.all_gather(own_rows, TP, axis=0, tiled=True)  16.7 us
    all_to_all x1, waiting for transfers between devices, per_device(): lax.all_to_all(heads, 'y', 0, 0, tiled=True).reshape(-1, heads.shape[2])  16.3 us
    all_to_all x1, blocking collectives, sum_at_owner(): lax.all_to_all(blocks, TP, 0, 0, tiled=True).astype(jnp.float32)  14.8 us
    all_gather x1, blocking collectives, per_device(): mlp_in = lax.all_gather(mlp_in, TP, axis=0, tiled=True)  14.2 us
    ppermute x1, starting transfers between devices, ring_pieces(): far_a = lax.ppermute(even[:half], RING, pairs(1))  12.7 us
    all_to_all x1, waiting for transfers between devices, sum_at_owner(): lax.all_to_all(blocks, TP, 0, 0, tiled=True).astype(jnp.float32)  12 us
    ppermute x1, waiting for transfers between devices, ring_pieces(): even = lax.ppermute(block, RING, pairs(0))  10.6 us
    ppermute x1, starting transfers between devices, ring_pieces(): odd = lax.ppermute(block, RING, pairs(1))  9.04 us
  transfers between devices with their start and end apart: 10, of which 7 were waited for; matrix products, arithmetic and copies ran while one was open for 2% of the time, Pallas kernels for 2%

profile of v3, /device:TPU:1, one launch (start us, length us, event | category | flops | bytes accessed | tf_op | source)
XLA Modules:
  0.0 186.5 jit_solution(2143578401904365285)
XLA Ops:
  9.3 5.0 %collective-permute-start.4 = (bf16[64,1152]{1,0:T(8,128)(2,1)S(1)}, bf16[64,1152]{1,0:T(8,128)(2,1)S(1)}, u32[]{:S(2)}, u32[]{:S(2)}) collective-permute-start(bf16[64,1152]{1,0:T(8,128)(2,1)S(1)} %shard_map.174), channel_id=1, source_target_pairs={{0,64},{64,0},{128,192},{192,128},{256,320},{320,256},{384,448},{4... | collective-permute-start | bytes 442376 | tf_op jit(solution)/shard_map/ppermute | solution.py:49
  14.2 8.8 %collective-permute-start.5 = (bf16[64,1152]{1,0:T(8,128)(2,1)S(1)}, bf16[64,1152]{1,0:T(8,128)(2,1)S(1)}, u32[]{:S(2)}, u32[]{:S(2)}) collective-permute-start(bf16[64,1152]{1,0:T(8,128)(2,1)S(1)} %shard_map.174), channel_id=1, source_target_pairs={{64,128},{128,64},{192,256},{256,192},{320,384},{384,320},{448,0},... | collective-permute-start | bytes 442376 | tf_op jit(solution)/shard_map/ppermute | solution.py:50
  23.1 1.9 %collective-permute-start.6 = (bf16[64,1152]{1,0:T(8,128)(2,1)S(1)}, bf16[64,1152]{1,0:T(8,128)(2,1)S(1)}, u32[]{:S(2)}, u32[]{:S(2)}) collective-permute-start(bf16[64,1152]{1,0:T(8,128)(2,1)S(1)} %shard_map.174), channel_id=1, source_target_pairs={{0,128},{64,192},{128,256},{192,320},{256,384},{320,448},{384,0},{... | collective-permute-start | bytes 442376 | tf_op jit(solution)/shard_map/ppermute | solution.py:51
  25.0 1.3 collective-permute-done.5
  26.3 4.8 %collective-permute-done.6 = bf16[64,1152]{1,0:T(8,128)(2,1)S(1)} collective-permute-done((bf16[64,1152]{1,0:T(8,128)(2,1)S(1)}, bf16[64,1152]{1,0:T(8,128)(2,1)S(1)}, u32[]{:S(2)}, u32[]{:S(2)}) %collective-permute-start.6) | collective-permute-done | bytes 147488 | tf_op jit(solution)/shard_map/ppermute | solution.py:51
  31.2 0.9 pad_maximum_fusion
  32.2 1.1 shard_map.172
  33.3 7.0 %all-to-all-start = ((bf16[8,64,1024]{2,1,0:T(8,128)(2,1)}), bf16[8,64,1024]{2,1,0:T(8,128)(2,1)S(1)}, u32[]{:S(2)}, u32[]{:S(2)}) async-start(bf16[8,64,1024]{2,1,0:T(8,128)(2,1)} %shard_map.172), calls=%async_computation | async-start | bytes 2097152 | tf_op jit(solution)/shard_map/all_to_all | solution.py:211
  40.9 16.7 %all-gather = bf16[1,192,2048]{2,1,0:T(8,128)(2,1)S(1)} all-gather(bf16[1,24,2048]{2,1,0:T(8,128)(2,1)S(1)} %copy-done.11), channel_id=2, replica_groups=mesh['rep'=2,'z'=4,'y'=8,'x'=4,'core'=2] {'x','core'}, dimensions={1}, use_global_device_ids=true | all-gather | bytes 884736 | tf_op jit(solution)/shard_map/all_gather | solution.py:215
  57.9 16.3 %all-to-all-done = bf16[8,64,1024]{2,1,0:T(8,128)(2,1)S(1)} async-done(((bf16[8,64,1024]{2,1,0:T(8,128)(2,1)}), bf16[8,64,1024]{2,1,0:T(8,128)(2,1)S(1)}, u32[]{:S(2)}, u32[]{:S(2)}) %all-to-all-start) | async-done | bytes 1048608 | tf_op jit(solution)/shard_map/all_to_all | solution.py:211
  74.2 1.9 %collective-permute-start = (bf16[512,1024]{1,0:T(8,128)(2,1)S(1)}, bf16[512,1024]{1,0:T(8,128)(2,1)S(1)}, u32[]{:S(2)}, u32[]{:S(2)}) collective-permute-start(bf16[512,1024]{1,0:T(8,128)(2,1)S(1)} %bitcast.38), channel_id=1, source_target_pairs={{0,64},{64,0},{128,192},{192,128},{256,320},{320,256},{384,448},{4... | collective-permute-start | bytes 3145736 | tf_op jit(solution)/shard_map/ppermute | solution.py:30
  76.1 9.0 %collective-permute-start.1 = (bf16[512,1024]{1,0:T(8,128)(2,1)S(1)}, bf16[512,1024]{1,0:T(8,128)(2,1)S(1)}, u32[]{:S(2)}, u32[]{:S(2)}) collective-permute-start(bf16[512,1024]{1,0:T(8,128)(2,1)S(1)} %bitcast.39), channel_id=1, source_target_pairs={{64,128},{128,64},{192,256},{256,192},{320,384},{384,320},{448,0},... | collective-permute-start | bytes 3145736 | tf_op jit(solution)/shard_map/ppermute | solution.py:31
  85.8 10.6 %collective-permute-done.even = bf16[512,1024]{1,0:T(8,128)(2,1)S(1)} collective-permute-done((bf16[512,1024]{1,0:T(8,128)(2,1)S(1)}, bf16[512,1024]{1,0:T(8,128)(2,1)S(1)}, u32[]{:S(2)}, u32[]{:S(2)}) %collective-permute-start) | collective-permute-done | bytes 1048608 | tf_op jit(solution)/shard_map/ppermute | solution.py:30
  96.4 12.7 %collective-permute-start.2 = (bf16[256,1024]{1,0:T(8,128)(2,1)S(1)}, bf16[256,1024]{1,0:T(8,128)(2,1)S(1)}, u32[]{:S(2)}, u32[]{:S(2)}) collective-permute-start(bf16[256,1024]{1,0:T(8,128)(2,1)S(1)} %slice.31), channel_id=1, source_target_pairs={{64,128},{128,64},{192,256},{256,192},{320,384},{384,320},{448,0},... | collective-permute-start | bytes 1572872 | tf_op jit(solution)/shard_map/ppermute | solution.py:32
  109.2 2.4 %collective-permute-start.3 = (bf16[256,1024]{1,0:T(8,128)(2,1)S(1)}, bf16[256,1024]{1,0:T(8,128)(2,1)S(1)}, u32[]{:S(2)}, u32[]{:S(2)}) collective-permute-start(bf16[256,1024]{1,0:T(8,128)(2,1)S(1)} %slice.33), channel_id=1, source_target_pairs={{0,64},{64,0},{128,192},{192,128},{256,320},{320,256},{384,448},{4... | collective-permute-start | bytes 1572872 | tf_op jit(solution)/shard_map/ppermute | solution.py:33
  112.3 7.6 %collective-permute-done.2.far_a = bf16[256,1024]{1,0:T(8,128)(2,1)S(1)} collective-permute-done((bf16[256,1024]{1,0:T(8,128)(2,1)S(1)}, bf16[256,1024]{1,0:T(8,128)(2,1)S(1)}, u32[]{:S(2)}, u32[]{:S(2)}) %collective-permute-start.2) | collective-permute-done | bytes 524320 | tf_op jit(solution)/shard_map/ppermute | solution.py:32
  120.1 2.6 %collective-permute-done.3.far_b = bf16[256,1024]{1,0:T(8,128)(2,1)S(1)} collective-permute-done((bf16[256,1024]{1,0:T(8,128)(2,1)S(1)}, bf16[256,1024]{1,0:T(8,128)(2,1)S(1)}, u32[]{:S(2)}, u32[]{:S(2)}) %collective-permute-start.3) | collective-permute-done | bytes 524320 | tf_op jit(solution)/shard_map/ppermute | solution.py:33
  123.7 1.7 shard_map.173
  125.4 7.2 %all-to-all-start.1 = ((bf16[8,24,2048]{2,1,0:T(8,128)(2,1)}), bf16[8,24,2048]{2,1,0:T(8,128)(2,1)S(1)}, u32[]{:S(2)}, u32[]{:S(2)}) async-start(bf16[8,24,2048]{2,1,0:T(8,128)(2,1)} %bitcast.7), calls=%async_computation.1 | async-start | bytes 1572864 | tf_op jit(solution)/shard_map/all_to_all | solution.py:74
  132.7 12.0 %all-to-all-done.1 = bf16[8,24,2048]{2,1,0:T(8,128)(2,1)S(1)} async-done(((bf16[8,24,2048]{2,1,0:T(8,128)(2,1)}), bf16[8,24,2048]{2,1,0:T(8,128)(2,1)S(1)}, u32[]{:S(2)}, u32[]{:S(2)}) %all-to-all-start.1) | async-done | bytes 786464 | tf_op jit(solution)/shard_map/all_to_all | solution.py:74
  145.2 14.2 %all_gather.13.x = bf16[192,2048]{1,0:T(8,128)(2,1)S(1)} all-gather(bf16[24,2048]{1,0:T(8,128)(2,1)S(1)} %fusion.18), channel_id=1, replica_groups=mesh['rep'=2,'z'=4,'y'=8,'x'=4,'core'=2] {'x','core'}, dimensions={0}, use_global_device_ids=true | all-gather | bytes 884736 | tf_op jit(solution)/shard_map/all_gather | solution.py:239
  159.4 2.3 %copy-done = bf16[32,64,1152]{2,1,0:T(8,128)(2,1)S(1)} copy-done((bf16[32,64,1152]{2,1,0:T(8,128)(2,1)S(1)}, bf16[32,64,1152]{2,1,0:T(8,128)(2,1)}, u32[]{:S(2)}) %copy-start) | copy-done | bytes 4718616
  161.7 2.3 %shard_map.175 = bf16[192,2048]{1,0:T(8,128)(2,1)S(1)} custom-call(s32[4]{0:T(128)S(1)} %pad_add_fusion.labels, bf16[192,2048]{1,0:T(8,128)(2,1)S(1)} %all_gather.13.x, bf16[8,4,64,1152]{3,2,1,0:T(8,128)(2,1)S(1)} %bitcast.42, f32[1,384]{1,0:T(1,128)S(1)} %broadcast_in_dim.13.scale_gate, f32[1,384]{1,0:T(1,128)S(1)} %broadcast_in_dim.28.scale_up), custom_call_target="tpu_custom_call" | custom-call | flops 905969664 | bytes 4718592 | tf_op jit(solution)/shard_map/pallas_call | solution.py:180
  164.1 14.8 %all_to_all.15 = bf16[8,24,2048]{2,1,0:T(8,128)(2,1)S(1)} all-to-all(bf16[8,24,2048]{2,1,0:T(8,128)(2,1)S(1)} %bitcast.43), channel_id=1, replica_groups=mesh['rep'=2,'z'=4,'y'=8,'x'=4,'core'=2] {'x','core'}, dimensions={0} | all-to-all | bytes 1572864 | tf_op jit(solution)/shard_map/all_to_all | solution.py:74
  (63 shorter events, 6.8 us)
Async XLA Ops:
  6.5 152.9 %all-gather.4.cloned.1.call-start = ((), (), s32[]{:S(2)}) async-start(), calls=%async_computation.3 | async-start | bytes 5308416 | tf_op jit(solution)/shard_map/all_gather | solution.py:213
  6.5 0.9 copy-start.1
  8.3 0.9 copy-start.3
  9.2 22.9 %copy-start.4 = (f32[64,256]{1,0:T(8,128)S(1)}, f32[64,256]{1,0:T(8,128)}, u32[]{:S(2)}) copy-start(f32[64,256]{1,0:T(8,128)} %query.1) | copy-start | bytes 196612
  9.2 22.9 %copy-start.5 = (f32[64,256]{1,0:T(8,128)S(1)}, f32[64,256]{1,0:T(8,128)}, u32[]{:S(2)}) copy-start(f32[64,256]{1,0:T(8,128)} %keyed.1) | copy-start | bytes 196612
  9.2 22.9 %copy-start.6 = (f32[64,256]{1,0:T(8,128)S(1)}, f32[64,256]{1,0:T(8,128)}, u32[]{:S(2)}) copy-start(f32[64,256]{1,0:T(8,128)} %valued.1) | copy-start | bytes 196612
  9.2 22.9 %copy-start.7 = (f32[256,64]{0,1:T(8,128)S(1)}, f32[256,64]{0,1:T(8,128)}, u32[]{:S(2)}) copy-start(f32[256,64]{0,1:T(8,128)} %param.23) | copy-start | bytes 196612
  9.3 15.7 %collective-permute-start.4 = (bf16[64,1152]{1,0:T(8,128)(2,1)S(1)}, bf16[64,1152]{1,0:T(8,128)(2,1)S(1)}, u32[]{:S(2)}, u32[]{:S(2)}) collective-permute-start(bf16[64,1152]{1,0:T(8,128)(2,1)S(1)} %shard_map.174), channel_id=1, source_target_pairs={{0,64},{64,0},{128,192},{192,128},{256,320},{320,256},{384,448},{4... | collective-permute-start | bytes 442376 | tf_op jit(solution)/shard_map/ppermute | solution.py:49
  14.2 12.1 %collective-permute-start.5 = (bf16[64,1152]{1,0:T(8,128)(2,1)S(1)}, bf16[64,1152]{1,0:T(8,128)(2,1)S(1)}, u32[]{:S(2)}, u32[]{:S(2)}) collective-permute-start(bf16[64,1152]{1,0:T(8,128)(2,1)S(1)} %shard_map.174), channel_id=1, source_target_pairs={{64,128},{128,64},{192,256},{256,192},{320,384},{384,320},{448,0},... | collective-permute-start | bytes 442376 | tf_op jit(solution)/shard_map/ppermute | solution.py:50
  23.1 8.1 %collective-permute-start.6 = (bf16[64,1152]{1,0:T(8,128)(2,1)S(1)}, bf16[64,1152]{1,0:T(8,128)(2,1)S(1)}, u32[]{:S(2)}, u32[]{:S(2)}) collective-permute-start(bf16[64,1152]{1,0:T(8,128)(2,1)S(1)} %shard_map.174), channel_id=1, source_target_pairs={{0,128},{64,192},{128,256},{192,320},{256,384},{320,448},{384,0},{... | collective-permute-start | bytes 442376 | tf_op jit(solution)/shard_map/ppermute | solution.py:51
  32.1 8.8 %copy-start.11 = (bf16[1,24,2048]{2,1,0:T(8,128)(2,1)S(1)}, bf16[1,24,2048]{2,1,0:T(8,128)(2,1)}, u32[]{:S(2)}) copy-start(bf16[1,24,2048]{2,1,0:T(8,128)(2,1)} %param.18) | copy-start | bytes 294916
  33.3 52.3 %copy-start.13 = (f32[2048]{0:T(1024)S(1)}, f32[2048]{0:T(1024)}, u32[]{:S(2)}) copy-start(f32[2048]{0:T(1024)} %param.19) | copy-start | bytes 24580
  33.3 40.9 %all-to-all-start = ((bf16[8,64,1024]{2,1,0:T(8,128)(2,1)}), bf16[8,64,1024]{2,1,0:T(8,128)(2,1)S(1)}, u32[]{:S(2)}, u32[]{:S(2)}) async-start(bf16[8,64,1024]{2,1,0:T(8,128)(2,1)} %shard_map.172), calls=%async_computation | async-start | bytes 2097152 | tf_op jit(solution)/shard_map/all_to_all | solution.py:211
  74.2 22.2 %collective-permute-start = (bf16[512,1024]{1,0:T(8,128)(2,1)S(1)}, bf16[512,1024]{1,0:T(8,128)(2,1)S(1)}, u32[]{:S(2)}, u32[]{:S(2)}) collective-permute-start(bf16[512,1024]{1,0:T(8,128)(2,1)S(1)} %bitcast.38), channel_id=1, source_target_pairs={{0,64},{64,0},{128,192},{192,128},{256,320},{320,256},{384,448},{4... | collective-permute-start | bytes 3145736 | tf_op jit(solution)/shard_map/ppermute | solution.py:30
  76.1 33.0 %collective-permute-start.1 = (bf16[512,1024]{1,0:T(8,128)(2,1)S(1)}, bf16[512,1024]{1,0:T(8,128)(2,1)S(1)}, u32[]{:S(2)}, u32[]{:S(2)}) collective-permute-start(bf16[512,1024]{1,0:T(8,128)(2,1)S(1)} %bitcast.39), channel_id=1, source_target_pairs={{64,128},{128,64},{192,256},{256,192},{320,384},{384,320},{448,0},... | collective-permute-start | bytes 3145736 | tf_op jit(solution)/shard_map/ppermute | solution.py:31
  96.4 23.4 %collective-permute-start.2 = (bf16[256,1024]{1,0:T(8,128)(2,1)S(1)}, bf16[256,1024]{1,0:T(8,128)(2,1)S(1)}, u32[]{:S(2)}, u32[]{:S(2)}) collective-permute-start(bf16[256,1024]{1,0:T(8,128)(2,1)S(1)} %slice.31), channel_id=1, source_target_pairs={{64,128},{128,64},{192,256},{256,192},{320,384},{384,320},{448,0},... | collective-permute-start | bytes 1572872 | tf_op jit(solution)/shard_map/ppermute | solution.py:32
  109.2 13.5 %collective-permute-start.3 = (bf16[256,1024]{1,0:T(8,128)(2,1)S(1)}, bf16[256,1024]{1,0:T(8,128)(2,1)S(1)}, u32[]{:S(2)}, u32[]{:S(2)}) collective-permute-start(bf16[256,1024]{1,0:T(8,128)(2,1)S(1)} %slice.33), channel_id=1, source_target_pairs={{0,64},{64,0},{128,192},{192,128},{256,320},{320,256},{384,448},{4... | collective-permute-start | bytes 1572872 | tf_op jit(solution)/shard_map/ppermute | solution.py:33
  125.4 7.2 %copy-start.16 = (f32[384]{0:T(512)S(1)}, f32[384]{0:T(512)}, u32[]{:S(2)}) copy-start(f32[384]{0:T(512)} %param.33) | copy-start | bytes 4612
  125.4 7.2 %copy-start.17 = (f32[384]{0:T(512)S(1)}, f32[384]{0:T(512)}, u32[]{:S(2)}) copy-start(f32[384]{0:T(512)} %param.34) | copy-start | bytes 4612
  125.4 19.5 %copy-start.12 = (f32[2048]{0:T(1024)S(1)}, f32[2048]{0:T(1024)}, u32[]{:S(2)}) copy-start(f32[2048]{0:T(1024)} %param.27) | copy-start | bytes 24580
  125.4 19.7 %copy-start.15 = (f32[2048]{0:T(1024)S(1)}, f32[2048]{0:T(1024)}, u32[]{:S(2)}) copy-start(f32[2048]{0:T(1024)} %param.29) | copy-start | bytes 24580
  125.4 19.4 %all-to-all-start.1 = ((bf16[8,24,2048]{2,1,0:T(8,128)(2,1)}), bf16[8,24,2048]{2,1,0:T(8,128)(2,1)S(1)}, u32[]{:S(2)}, u32[]{:S(2)}) async-start(bf16[8,24,2048]{2,1,0:T(8,128)(2,1)} %bitcast.7), calls=%async_computation.1 | async-start | bytes 1572864 | tf_op jit(solution)/shard_map/all_to_all | solution.py:74
  159.4 2.3 %copy-start = (bf16[32,64,1152]{2,1,0:T(8,128)(2,1)S(1)}, bf16[32,64,1152]{2,1,0:T(8,128)(2,1)}, u32[]{:S(2)}) copy-start(bf16[32,64,1152]{2,1,0:T(8,128)(2,1)} %all-gather.4.cloned.1.call-done) | copy-start | bytes 14155780
  164.1 14.9 %copy-start.14 = (f32[2048]{0:T(1024)S(1)}, f32[2048]{0:T(1024)}, u32[]{:S(2)}) copy-start(f32[2048]{0:T(1024)} %param.35) | copy-start | bytes 24580
  (4 other events, 2.9 us)
Sparse Core Ops, SparseCore 0:
  32.2 79.3 all-gather.3

commit v4 on v3

--- a/solution.py
+++ b/solution.py
@@ -69,9 +69,13 @@
     return lax.dot_general(a, b, (((1,), (1,)), ((), ())), preferred_element_type=jnp.float32)
 
 
-def sum_at_owner(partial):
-    blocks = partial.reshape(lax.axis_size(TP), -1, partial.shape[1])
-    return jnp.sum(lax.all_to_all(blocks, TP, 0, 0, tiled=True).astype(jnp.float32), axis=0)
+def sum_over_chips(partial):
+    blocks = partial.reshape(lax.axis_size("x"), -1, partial.shape[1])
+    return jnp.sum(lax.all_to_all(blocks, "x", 0, 0, tiled=True).astype(jnp.float32), axis=0)
+
+
+def swap_cores(array):
+    return lax.ppermute(array, "core", [(0, 1), (1, 0)])
 
 
 def rotary(values, cosine, sine):
@@ -87,31 +91,45 @@
 SMEM = pl.BlockSpec(memory_space=pltpu.SMEM)
 
 
-def local_call(kernel, out_shape, specs, flops=0, moved=0):
+def local_call(kernel, out_shape, specs, flops, moved, out_specs=VMEM):
     return pl.pallas_call(
         kernel,
         out_shape=out_shape,
         in_specs=specs,
-        out_specs=VMEM,
+        out_specs=out_specs,
         compiler_params=pltpu.CompilerParams(vmem_limit_bytes=24 * 2**20),
         cost_estimate=pl.CostEstimate(flops=flops, bytes_accessed=moved, transcendentals=0),
     )
 
 
-def heads_shard_kernel(query, keyed, valued, out_w, out):
+def heads_shard_kernel(query, keyed, valued, out_w, out, held, sems):
     width = query.shape[1]
-    parts = [ref[...].astype(jnp.bfloat16) for ref in (query, keyed, valued, out_w)]
-    for peer in range(out.shape[0]):
-        for i, part in enumerate(parts):
+    parts = (query, keyed, valued, out_w)
+    copies = [pltpu.make_async_copy(w, held.at[i], sems.at[i]) for i, w in enumerate(parts)]
+    for copy in copies:
+        copy.start()
+    for i, copy in enumerate(copies):
+        copy.wait()
+        part = held[i].astype(jnp.bfloat16)
+        for peer in range(out.shape[0]):
             out[peer, :, i * width : (i + 1) * width] = part
 
 
 def heads_shard(w_query, w_key, w_value, w_out, peers):
     rows, width = w_query.shape
-    shape = jax.ShapeDtypeStruct((peers, rows, 4 * width), jnp.bfloat16)
-    return local_call(heads_shard_kernel, shape, [VMEM] * 4, 10**7, 2**21)(
-        w_query, w_key, w_value, w_out.T
-    )
+    return pl.pallas_call(
+        heads_shard_kernel,
+        out_shape=jax.ShapeDtypeStruct((peers, rows, 4 * width), jnp.bfloat16),
+        in_specs=[pl.BlockSpec(memory_space=pltpu.HBM)] * 4,
+        out_specs=VMEM,
+        scratch_shapes=[
+            pltpu.VMEM((4, rows, width), jnp.float32),
+            pltpu.SemaphoreType.DMA((4,)),
+        ],
+        compiler_params=pltpu.CompilerParams(vmem_limit_bytes=60 * 2**20),
+        cost_estimate=pl.CostEstimate(flops=10**7, bytes_accessed=2**21, transcendentals=0),
+        name="heads_shard",
+    )(w_query, w_key, w_value, w_out.T)
 
 
 def mlp_shard_kernel(gate, up, down, out):
@@ -127,7 +145,7 @@
     return local_call(mlp_shard_kernel, shape, [VMEM] * 3, 10**7, 2**20)(w_gate, w_up, w_down.T)
 
 
-def retain_kernel(rate, product, cosine, sine, sq, sk, sv, own, even, odd, far_a, far_b, out):
+def retain_kernel(rate, core, product, cosine, sine, sq, sk, sv, own, even, odd, far_a, far_b, kept, sent):
     width = sq.shape[1]
     cos, sin = cosine[...], sine[...]
     query = rotary(product[:, :width] * sq[...], cos, sin).astype(jnp.bfloat16)
@@ -140,45 +158,69 @@
     decay = jnp.exp(-rate[0] * jnp.maximum(distance, 0.0))
     weights = jnp.where(distance >= 0.0, dot_t(query, keyed) * decay, 0.0).astype(jnp.bfloat16)
     retained = jnp.dot(weights, valued, preferred_element_type=jnp.float32)
-    attended = (retained * inv_rms(retained)).astype(jnp.bfloat16)
+    attended = retained * inv_rms(retained)
+    rows = length // 8
+    first = [attended[i * rows : (i + 1) * rows] for i in range(0, 8, 2)]
+    second = [attended[i * rows : (i + 1) * rows] for i in range(1, 8, 2)]
+    low = core[0] == 0
+    mine = [jnp.where(low, a, b) for a, b in zip(first, second)]
+    other = [jnp.where(low, b, a) for a, b in zip(first, second)]
+    attended = jnp.concatenate(mine + other, axis=0).astype(jnp.bfloat16)
+    half = length // 2
     at = 0
     for piece in (own, even, odd, far_a, far_b):
         to = at + piece.shape[0]
-        out[:, at:to] = dot_t(attended, piece[:, 3 * width :]).astype(jnp.bfloat16)
+        term = dot_t(attended, piece[:, 3 * width :])
+        kept[:, at:to] = term[:half]
+        sent[:, at:to] = term[half:].astype(jnp.bfloat16)
         at = to
 
 
-def retain(rate, product, cosine, sine, scales, pieces):
+def retain(rate, core, product, cosine, sine, scales, pieces):
     columns = sum(piece.shape[0] for piece in pieces)
-    shape = jax.ShapeDtypeStruct((product.shape[0], columns), jnp.bfloat16)
-    specs = [SMEM] + [VMEM] * (6 + len(pieces))
+    half = product.shape[0] // 2
+    shapes = [jax.ShapeDtypeStruct((half, columns), kind) for kind in (jnp.float32, jnp.bfloat16)]
+    specs = [SMEM] * 2 + [VMEM] * (6 + len(pieces))
     scales = [scale[None] for scale in scales]
-    return local_call(retain_kernel, shape, specs, 3 * 10**8, 2**21)(
-        rate, product, cosine, sine, *scales, *pieces
-    )
-
-
-def mlp_kernel(labels, x, weights, scale_gate, scale_up, out):
-    units = scale_gate.shape[1]
+    return local_call(retain_kernel, shapes, specs, 3 * 10**8, 2**21, [VMEM] * 2)(
+        rate, core, product, cosine, sine, *scales, *pieces
+    )
+
+
+def hold_kernel(weights, out):
+    out[...] = weights[...]
+
+
+def hold(weights):
+    shape = jax.ShapeDtypeStruct(weights.shape, weights.dtype)
+    return local_call(hold_kernel, shape, [VMEM], 10**7, 4 * weights.size)(weights)
+
+
+def mlp_kernel(labels, x, weights, others, scales, other_scales, out):
+    units = scales.shape[1]
     size = x.shape[1] // 4
-    both = jnp.zeros((x.shape[0], 2 * units), jnp.float32)
     places = [pl.ds(pl.multiple_of(labels[p] * size, size), size) for p in range(4)]
+    inner = []
+    for held, scale in ((weights, scales), (others, other_scales)):
+        both = jnp.zeros((x.shape[0], 2 * units), jnp.float32)
+        for p, at in enumerate(places):
+            piece = held[:, p, :, : 2 * units].reshape(size, 2 * units)
+            both += jnp.dot(x[:, at], piece, preferred_element_type=jnp.float32)
+        gate = both[:, :units] * scale[0:1]
+        up = both[:, units:] * scale[1:2]
+        inner.append((gate / (1.0 + jnp.exp(-gate)) * up).astype(jnp.bfloat16))
     for p, at in enumerate(places):
-        piece = weights[:, p, :, : 2 * units].reshape(size, 2 * units)
-        both += jnp.dot(x[:, at], piece, preferred_element_type=jnp.float32)
-    gate = both[:, :units] * scale_gate[...]
-    up = both[:, units:] * scale_up[...]
-    inner = (gate / (1.0 + jnp.exp(-gate)) * up).astype(jnp.bfloat16)
-    for p, at in enumerate(places):
-        piece = weights[:, p, :, 2 * units :].reshape(size, units)
-        out[:, at] = dot_t(inner, piece).astype(jnp.bfloat16)
-
-
-def mlp(labels, x, weights, scale_gate, scale_up):
+        total = 0.0
+        for held, part in zip((weights, others), inner):
+            total += dot_t(part, held[:, p, :, 2 * units :].reshape(size, units))
+        out[:, at] = total.astype(jnp.bfloat16)
+
+
+def mlp(labels, x, weights, others, scales, other_scales):
     shape = jax.ShapeDtypeStruct(x.shape, jnp.bfloat16)
-    flops = 2 * x.shape[0] * x.shape[1] * weights.shape[-1]
-    return local_call(mlp_kernel, shape, [SMEM] + [VMEM] * 4, flops, 2 * weights.size)(
-        labels, x, weights, scale_gate[None], scale_up[None]
+    flops = 4 * x.shape[0] * x.shape[1] * weights.shape[-1]
+    return local_call(mlp_kernel, shape, [SMEM] + [VMEM] * 5, flops, 4 * weights.size)(
+        labels, x, weights, others, scales, other_scales
     )
 
 
@@ -211,6 +253,10 @@
     heads = lax.all_to_all(heads, "y", 0, 0, tiled=True).reshape(-1, heads.shape[2])
     own = ring_blocks(mlp_shard(w_gate, w_up, w_down))
     mlp_weights = lax.all_gather(own, "y", axis=0)
+    mlp_weights = hold(mlp_weights)
+    mlp_others = swap_cores(mlp_weights)
+    mlp_scales = jnp.stack([scale_gate, scale_up])
+    other_scales = swap_cores(mlp_scales)
     heads = ring_pieces(heads)
     all_rows = lax.all_gather(own_rows, TP, axis=0, tiled=True)
 
@@ -221,7 +267,10 @@
     inv_freq = 1.0 / ROPE_BASE ** (jnp.arange(0, HEAD_DIM, 2, dtype=f32) / HEAD_DIM)
     angles = positions[:, None] * inv_freq[None, :]
     scales = (scale_query, scale_key, scale_value)
-    partial = retain(decay_rate, product, jnp.cos(angles), jnp.sin(angles), scales, heads)
+    core = lax.axis_index("core").astype(jnp.int32)[None]
+    kept, sent = retain(
+        decay_rate, core, product, jnp.cos(angles), jnp.sin(angles), scales, heads
+    )
 
     slots = ring_slots()
 
@@ -231,15 +280,18 @@
             [lax.dynamic_slice_in_dim(values, slot * size, size, 1) for slot in slots], axis=1
         )
 
-    mixed = sum_at_owner(partial)
+    got = swap_cores(sent)
+    mixed = sum_over_chips((kept + got.astype(f32)).astype(bf16))
     mixed = in_order(mixed) * scale_out
     hidden = (own_rows.astype(f32) + mixed).astype(bf16)
     values = hidden.astype(f32)
     mlp_in = (values * inv_rms(values) * mlp_gain).astype(bf16)
-    mlp_in = lax.all_gather(mlp_in, TP, axis=0, tiled=True)
+    copies = jnp.broadcast_to(mlp_in[None], (lax.axis_size("x"), rows, width))
+    mlp_in = lax.all_to_all(copies, "x", 0, 0, tiled=True).reshape(-1, width)
 
     labels = jnp.stack(ring_labels()).astype(jnp.int32)
-    channel = sum_at_owner(mlp(labels, mlp_in, mlp_weights, scale_gate, scale_up)) * scale_down
+    partial = mlp(labels, mlp_in, mlp_weights, mlp_others, mlp_scales, other_scales)
+    channel = sum_over_chips(partial) * scale_down
     return (hidden.astype(f32) + channel).astype(bf16)[None]
 
 

time: 187 us -> 195 us (1.043)
  the two profiles are of different devices: /device:TPU:1 before, /device:TPU:24 now
where the time goes in v4:
time: 195 us; the launch traced here: 194 us
  waiting for transfers between devices  82.9 us (43%)
  starting transfers between devices  48.9 us (25%)
  blocking collectives  23.5 us (12%)
  between operations  14.4 us (7%)
  Pallas kernels  11.7 us (6%)
  local copies, waits for them, and re-layouts  7.15 us (4%)
  other arithmetic  3.78 us (2%)
    all_gather x1, waiting for transfers between devices, per_device(): mlp_weights = lax.all_gather(own, 'y', axis=0)  30.4 us
    all_to_all x1, waiting for transfers between devices, per_device(): lax.all_to_all(heads, 'y', 0, 0, tiled=True).reshape(-1, heads.shape[2])  19.3 us
    all_gather x1, blocking collectives, per_device(): all_rows = lax.all_gather(own_rows, TP, axis=0, tiled=True)  13.7 us
    all_to_all x1, blocking collectives, sum_over_chips(): lax.all_to_all(blocks, 'x', 0, 0, tiled=True).astype(jnp.float32)  9.77 us
    ppermute x1, waiting for transfers between devices, ring_pieces(): far_b = lax.ppermute(odd[half:], RING, pairs(0))  8.48 us
    all_to_all x1, waiting for transfers between devices, sum_over_chips(): lax.all_to_all(blocks, 'x', 0, 0, tiled=True).astype(jnp.float32)  8.37 us
    all_to_all x1, starting transfers between devices, per_device(): lax.all_to_all(heads, 'y', 0, 0, tiled=True).reshape(-1, heads.shape[2])  7.33 us
    ppermute x1, starting transfers between devices, ring_blocks(): odd = lax.ppermute(block, RING, pairs(1))  6.78 us
  transfers between devices with their start and end apart: 14, of which 9 were waited for; matrix products, arithmetic and copies ran while one was open for 2% of the time, Pallas kernels for 3%

profile of v4, /device:TPU:24, one launch (start us, length us, event | category | flops | bytes accessed | tf_op | source)
XLA Modules:
  0.0 193.8 jit_solution(3409163842432504193)
XLA Ops:
  9.2 6.1 %collective-permute-start.7 = (bf16[64,1152]{1,0:T(8,128)(2,1)S(1)}, bf16[64,1152]{1,0:T(8,128)(2,1)S(1)}, u32[]{:S(2)}, u32[]{:S(2)}) collective-permute-start(bf16[64,1152]{1,0:T(8,128)(2,1)S(1)} %shard_map.173), channel_id=1, source_target_pairs={{0,128},{64,192},{128,256},{192,320},{256,384},{320,448},{384,0},{... | collective-permute-start | bytes 442376 | tf_op jit(solution)/shard_map/ppermute | solution.py:51
  15.3 6.8 %collective-permute-start.6 = (bf16[64,1152]{1,0:T(8,128)(2,1)S(1)}, bf16[64,1152]{1,0:T(8,128)(2,1)S(1)}, u32[]{:S(2)}, u32[]{:S(2)}) collective-permute-start(bf16[64,1152]{1,0:T(8,128)(2,1)S(1)} %shard_map.173), channel_id=1, source_target_pairs={{64,128},{128,64},{192,256},{256,192},{320,384},{384,320},{448,0},... | collective-permute-start | bytes 442376 | tf_op jit(solution)/shard_map/ppermute | solution.py:50
  22.1 3.0 %collective-permute-start.5 = (bf16[64,1152]{1,0:T(8,128)(2,1)S(1)}, bf16[64,1152]{1,0:T(8,128)(2,1)S(1)}, u32[]{:S(2)}, u32[]{:S(2)}) collective-permute-start(bf16[64,1152]{1,0:T(8,128)(2,1)S(1)} %shard_map.173), channel_id=1, source_target_pairs={{0,64},{64,0},{128,192},{192,128},{256,320},{320,256},{384,448},{4... | collective-permute-start | bytes 442376 | tf_op jit(solution)/shard_map/ppermute | solution.py:49
  25.1 5.2 %collective-permute-done.6 = bf16[64,1152]{1,0:T(8,128)(2,1)S(1)} collective-permute-done((bf16[64,1152]{1,0:T(8,128)(2,1)S(1)}, bf16[64,1152]{1,0:T(8,128)(2,1)S(1)}, u32[]{:S(2)}, u32[]{:S(2)}) %collective-permute-start.6) | collective-permute-done | bytes 147488 | tf_op jit(solution)/shard_map/ppermute | solution.py:50
  31.3 2.0 %heads_shard.1 = bf16[8,64,1024]{2,1,0:T(8,128)(2,1)} custom-call(f32[64,256]{1,0:T(8,128)} %query.1, f32[64,256]{1,0:T(8,128)} %keyed.1, f32[64,256]{1,0:T(8,128)} %valued.1, f32[64,256]{1,0:T(8,128)} %bitcast.60), custom_call_target="tpu_custom_call" | custom-call | flops 10000000 | bytes 2097152 | tf_op jit(solution)/shard_map/heads_shard/pallas_call | solution.py:120
  33.4 7.3 %all-to-all-start = ((bf16[8,64,1024]{2,1,0:T(8,128)(2,1)}), bf16[8,64,1024]{2,1,0:T(8,128)(2,1)S(1)}, u32[]{:S(2)}, u32[]{:S(2)}) async-start(bf16[8,64,1024]{2,1,0:T(8,128)(2,1)} %heads_shard.1), calls=%async_computation | async-start | bytes 2097152 | tf_op jit(solution)/shard_map/all_to_all | solution.py:253
  41.4 13.7 %all-gather = bf16[1,192,2048]{2,1,0:T(8,128)(2,1)S(1)} all-gather(bf16[1,24,2048]{2,1,0:T(8,128)(2,1)S(1)} %copy-done.9), channel_id=2, replica_groups=mesh['rep'=2,'z'=4,'y'=8,'x'=4,'core'=2] {'x','core'}, dimensions={1}, use_global_device_ids=true | all-gather | bytes 884736 | tf_op jit(solution)/shard_map/all_gather | solution.py:261
  56.2 19.3 %all-to-all-done = bf16[8,64,1024]{2,1,0:T(8,128)(2,1)S(1)} async-done(((bf16[8,64,1024]{2,1,0:T(8,128)(2,1)}), bf16[8,64,1024]{2,1,0:T(8,128)(2,1)S(1)}, u32[]{:S(2)}, u32[]{:S(2)}) %all-to-all-start) | async-done | bytes 1048608 | tf_op jit(solution)/shard_map/all_to_all | solution.py:253
  77.4 3.3 %collective-permute-start = (bf16[512,1024]{1,0:T(8,128)(2,1)S(1)}, bf16[512,1024]{1,0:T(8,128)(2,1)S(1)}, u32[]{:S(2)}, u32[]{:S(2)}) collective-permute-start(bf16[512,1024]{1,0:T(8,128)(2,1)S(1)} %bitcast.42), channel_id=1, source_target_pairs={{0,64},{64,0},{128,192},{192,128},{256,320},{320,256},{384,448},{4... | collective-permute-start | bytes 3145736 | tf_op jit(solution)/shard_map/ppermute | solution.py:30
  80.7 30.4 %all-gather.4.cloned.1.call-done = bf16[32,64,1152]{2,1,0:T(8,128)(2,1)} async-done(((bf16[4,64,1152]{2,1,0:T(8,128)(2,1)}), bf16[32,64,1152]{2,1,0:T(8,128)(2,1)}) %all-gather.4.cloned.1.call-update) | async-done | bytes 4718608 | tf_op jit(solution)/shard_map/all_gather | solution.py:255
  111.2 2.3 %copy-done = bf16[32,64,1152]{2,1,0:T(8,128)(2,1)S(1)} copy-done((bf16[32,64,1152]{2,1,0:T(8,128)(2,1)S(1)}, bf16[32,64,1152]{2,1,0:T(8,128)(2,1)}, u32[]{:S(2)}) %copy-start) | copy-done | bytes 4718616
  113.5 2.5 %shard_map.174.weights = bf16[8,4,64,1152]{3,2,1,0:T(8,128)(2,1)} custom-call(bf16[8,4,64,1152]{3,2,1,0:T(8,128)(2,1)S(1)} %bitcast.45), custom_call_target="tpu_custom_call" | custom-call | flops 10000000 | bytes 9437184 | tf_op jit(solution)/shard_map/pallas_call | solution.py:196
  118.6 3.4 %collective-permute-start.3 = (bf16[256,1024]{1,0:T(8,128)(2,1)S(1)}, bf16[256,1024]{1,0:T(8,128)(2,1)S(1)}, u32[]{:S(2)}, u32[]{:S(2)}) collective-permute-start(bf16[256,1024]{1,0:T(8,128)(2,1)S(1)} %slice.33), channel_id=1, source_target_pairs={{0,64},{64,0},{128,192},{192,128},{256,320},{320,256},{384,448},{4... | collective-permute-start | bytes 1572872 | tf_op jit(solution)/shard_map/ppermute | solution.py:33
  122.0 3.6 %collective-permute-start.2 = (bf16[256,1024]{1,0:T(8,128)(2,1)S(1)}, bf16[256,1024]{1,0:T(8,128)(2,1)S(1)}, u32[]{:S(2)}, u32[]{:S(2)}) collective-permute-start(bf16[256,1024]{1,0:T(8,128)(2,1)S(1)} %slice.31), channel_id=1, source_target_pairs={{64,128},{128,64},{192,256},{256,192},{320,384},{384,320},{448,0},... | collective-permute-start | bytes 1572872 | tf_op jit(solution)/shard_map/ppermute | solution.py:32
  126.4 8.5 %collective-permute-done.3.far_b = bf16[256,1024]{1,0:T(8,128)(2,1)S(1)} collective-permute-done((bf16[256,1024]{1,0:T(8,128)(2,1)S(1)}, bf16[256,1024]{1,0:T(8,128)(2,1)S(1)}, u32[]{:S(2)}, u32[]{:S(2)}) %collective-permute-start.3) | collective-permute-done | bytes 524320 | tf_op jit(solution)/shard_map/ppermute | solution.py:33
  135.1 4.1 %collective-permute-done.2.far_a = bf16[256,1024]{1,0:T(8,128)(2,1)S(1)} collective-permute-done((bf16[256,1024]{1,0:T(8,128)(2,1)S(1)}, bf16[256,1024]{1,0:T(8,128)(2,1)S(1)}, u32[]{:S(2)}, u32[]{:S(2)}) %collective-permute-start.2) | collective-permute-done | bytes 524320 | tf_op jit(solution)/shard_map/ppermute | solution.py:32
  141.0 1.9 collective-permute-start.4
  145.5 4.3 %all-to-all-start.1 = ((bf16[4,24,2048]{2,1,0:T(8,128)(2,1)}), bf16[4,24,2048]{2,1,0:T(8,128)(2,1)S(1)}, u32[]{:S(2)}, u32[]{:S(2)}) async-start(bf16[4,24,2048]{2,1,0:T(8,128)(2,1)} %bitcast.8), calls=%async_computation.1 | async-start | bytes 786432 | tf_op jit(solution)/shard_map/all_to_all | solution.py:74
  149.8 8.4 %all-to-all-done.1 = bf16[4,24,2048]{2,1,0:T(8,128)(2,1)S(1)} async-done(((bf16[4,24,2048]{2,1,0:T(8,128)(2,1)}), bf16[4,24,2048]{2,1,0:T(8,128)(2,1)S(1)}, u32[]{:S(2)}, u32[]{:S(2)}) %all-to-all-start.1) | async-done | bytes 393248 | tf_op jit(solution)/shard_map/all_to_all | solution.py:74
  159.3 3.5 %all-to-all-start.2 = ((bf16[4,24,2048]{2,1,0:T(8,128)(2,1)}), bf16[4,24,2048]{2,1,0:T(8,128)(2,1)S(1)}, u32[]{:S(2)}, u32[]{:S(2)}) async-start(bf16[4,24,2048]{2,1,0:T(8,128)(2,1)} %broadcast_in_dim.34), calls=%async_computation.2 | async-start | bytes 786432 | tf_op jit(solution)/shard_map/all_to_all | solution.py:290
  162.8 1.9 collective-permute-start.9
  165.9 4.2 %all-to-all-done.2 = bf16[4,24,2048]{2,1,0:T(8,128)(2,1)S(1)} async-done(((bf16[4,24,2048]{2,1,0:T(8,128)(2,1)}), bf16[4,24,2048]{2,1,0:T(8,128)(2,1)S(1)}, u32[]{:S(2)}, u32[]{:S(2)}) %all-to-all-start.2) | async-done | bytes 393248 | tf_op jit(solution)/shard_map/all_to_all | solution.py:290
  170.1 6.4 %shard_map.175 = bf16[96,2048]{1,0:T(8,128)(2,1)S(1)} custom-call(s32[4]{0:T(128)S(1)} %pad_add_fusion.labels, bf16[96,2048]{1,0:T(8,128)(2,1)S(1)} %bitcast.46, bf16[8,4,64,1152]{3,2,1,0:T(8,128)(2,1)} %shard_map.174.weights, bf16[8,4,64,1152]{3,2,1,0:T(8,128)(2,1)} %collective-permute-done.8.others, f32[2,384]{1,0:T(2,128)S(1)} %pad_maximum_fusion.1.scales, ...), custom_call_target="tpu_custom_call" | custom-call | flops 905969664 | bytes 9437184 | tf_op jit(solution)/shard_map/pallas_call | solution.py:222
  176.5 9.8 %all_to_all.20 = bf16[4,24,2048]{2,1,0:T(8,128)(2,1)S(1)} all-to-all(bf16[4,24,2048]{2,1,0:T(8,128)(2,1)S(1)} %bitcast.47), channel_id=1, replica_groups=mesh['rep'=2,'z'=4,'y'=8,'x'=4,'core'=2] {'x'}, dimensions={0} | all-to-all | bytes 786432 | tf_op jit(solution)/shard_map/all_to_all | solution.py:74
  (70 shorter events, 17.5 us)
Async XLA Ops:
  6.5 104.6 %all-gather.4.cloned.1.call-start = ((), (), s32[]{:S(2)}) async-start(), calls=%async_computation.4 | async-start | bytes 5308416 | tf_op jit(solution)/shard_map/all_gather | solution.py:255
  6.5 0.9 copy-start.1
  9.2 15.9 %collective-permute-start.7 = (bf16[64,1152]{1,0:T(8,128)(2,1)S(1)}, bf16[64,1152]{1,0:T(8,128)(2,1)S(1)}, u32[]{:S(2)}, u32[]{:S(2)}) collective-permute-start(bf16[64,1152]{1,0:T(8,128)(2,1)S(1)} %shard_map.173), channel_id=1, source_target_pairs={{0,128},{64,192},{128,256},{192,320},{256,384},{320,448},{384,0},{... | collective-permute-start | bytes 442376 | tf_op jit(solution)/shard_map/ppermute | solution.py:51
  15.3 15.0 %collective-permute-start.6 = (bf16[64,1152]{1,0:T(8,128)(2,1)S(1)}, bf16[64,1152]{1,0:T(8,128)(2,1)S(1)}, u32[]{:S(2)}, u32[]{:S(2)}) collective-permute-start(bf16[64,1152]{1,0:T(8,128)(2,1)S(1)} %shard_map.173), channel_id=1, source_target_pairs={{64,128},{128,64},{192,256},{256,192},{320,384},{384,320},{448,0},... | collective-permute-start | bytes 442376 | tf_op jit(solution)/shard_map/ppermute | solution.py:50
  22.1 8.2 %collective-permute-start.5 = (bf16[64,1152]{1,0:T(8,128)(2,1)S(1)}, bf16[64,1152]{1,0:T(8,128)(2,1)S(1)}, u32[]{:S(2)}, u32[]{:S(2)}) collective-permute-start(bf16[64,1152]{1,0:T(8,128)(2,1)S(1)} %shard_map.173), channel_id=1, source_target_pairs={{0,64},{64,0},{128,192},{192,128},{256,320},{320,256},{384,448},{4... | collective-permute-start | bytes 442376 | tf_op jit(solution)/shard_map/ppermute | solution.py:49
  31.3 10.1 %copy-start.9 = (bf16[1,24,2048]{2,1,0:T(8,128)(2,1)S(1)}, bf16[1,24,2048]{2,1,0:T(8,128)(2,1)}, u32[]{:S(2)}) copy-start(bf16[1,24,2048]{2,1,0:T(8,128)(2,1)} %param.18) | copy-start | bytes 294916
  33.4 42.2 %all-to-all-start = ((bf16[8,64,1024]{2,1,0:T(8,128)(2,1)}), bf16[8,64,1024]{2,1,0:T(8,128)(2,1)S(1)}, u32[]{:S(2)}, u32[]{:S(2)}) async-start(bf16[8,64,1024]{2,1,0:T(8,128)(2,1)} %heads_shard.1), calls=%async_computation | async-start | bytes 2097152 | tf_op jit(solution)/shard_map/all_to_all | solution.py:253
  75.5 43.0 %collective-permute-start.1 = (bf16[512,1024]{1,0:T(8,128)(2,1)S(1)}, bf16[512,1024]{1,0:T(8,128)(2,1)S(1)}, u32[]{:S(2)}, u32[]{:S(2)}) collective-permute-start(bf16[512,1024]{1,0:T(8,128)(2,1)S(1)} %bitcast.41), channel_id=1, source_target_pairs={{64,128},{128,64},{192,256},{256,192},{320,384},{384,320},{448,0},... | collective-permute-start | bytes 3145736 | tf_op jit(solution)/shard_map/ppermute | solution.py:31
  77.4 44.5 %collective-permute-start = (bf16[512,1024]{1,0:T(8,128)(2,1)S(1)}, bf16[512,1024]{1,0:T(8,128)(2,1)S(1)}, u32[]{:S(2)}, u32[]{:S(2)}) collective-permute-start(bf16[512,1024]{1,0:T(8,128)(2,1)S(1)} %bitcast.42), channel_id=1, source_target_pairs={{0,64},{64,0},{128,192},{192,128},{256,320},{320,256},{384,448},{4... | collective-permute-start | bytes 3145736 | tf_op jit(solution)/shard_map/ppermute | solution.py:30
  111.2 2.3 %copy-start = (bf16[32,64,1152]{2,1,0:T(8,128)(2,1)S(1)}, bf16[32,64,1152]{2,1,0:T(8,128)(2,1)}, u32[]{:S(2)}) copy-start(bf16[32,64,1152]{2,1,0:T(8,128)(2,1)} %all-gather.4.cloned.1.call-done) | copy-start | bytes 14155780
  113.5 4.8 %copy-start.8 = (bf16[1,192,2048]{2,1,0:T(8,128)(2,1)S(1)}, bf16[1,192,2048]{2,1,0:T(8,128)(2,1)}, u32[]{:S(2)}) copy-start(bf16[1,192,2048]{2,1,0:T(8,128)(2,1)} %copy-done.7) | copy-start | bytes 2359300
  113.5 4.8 %copy-start.11 = (f32[2048]{0:T(1024)S(1)}, f32[2048]{0:T(1024)}, u32[]{:S(2)}) copy-start(f32[2048]{0:T(1024)} %param.19) | copy-start | bytes 24580
  116.0 54.1 %collective-permute-start.8 = (bf16[8,4,64,1152]{3,2,1,0:T(8,128)(2,1)}, bf16[8,4,64,1152]{3,2,1,0:T(8,128)(2,1)}, u32[]{:S(2)}, u32[]{:S(2)}) collective-permute-start(bf16[8,4,64,1152]{3,2,1,0:T(8,128)(2,1)} %shard_map.174.weights), channel_id=1, source_target_pairs={{0,1},{1,0},{2,3},{3,2},{4,5},{5,4},{6,7},{7,6},{8,9},{9,8},{10,11... | collective-permute-start | bytes 14155784 | tf_op jit(solution)/shard_map/ppermute | solution.py:78
  118.6 16.2 %collective-permute-start.3 = (bf16[256,1024]{1,0:T(8,128)(2,1)S(1)}, bf16[256,1024]{1,0:T(8,128)(2,1)S(1)}, u32[]{:S(2)}, u32[]{:S(2)}) collective-permute-start(bf16[256,1024]{1,0:T(8,128)(2,1)S(1)} %slice.33), channel_id=1, source_target_pairs={{0,64},{64,0},{128,192},{192,128},{256,320},{320,256},{384,448},{4... | collective-permute-start | bytes 1572872 | tf_op jit(solution)/shard_map/ppermute | solution.py:33
  122.0 17.2 %collective-permute-start.2 = (bf16[256,1024]{1,0:T(8,128)(2,1)S(1)}, bf16[256,1024]{1,0:T(8,128)(2,1)S(1)}, u32[]{:S(2)}, u32[]{:S(2)}) collective-permute-start(bf16[256,1024]{1,0:T(8,128)(2,1)S(1)} %slice.31), channel_id=1, source_target_pairs={{64,128},{128,64},{192,256},{256,192},{320,384},{384,320},{448,0},... | collective-permute-start | bytes 1572872 | tf_op jit(solution)/shard_map/ppermute | solution.py:32
  141.0 3.6 %collective-permute-start.4 = (bf16[96,2048]{1,0:T(8,128)(2,1)S(1)}, bf16[96,2048]{1,0:T(8,128)(2,1)S(1)}, u32[]{:S(2)}, u32[]{:S(2)}) collective-permute-start(bf16[96,2048]{1,0:T(8,128)(2,1)S(1)} %get-tuple-element.8), channel_id=1, source_target_pairs={{0,1},{1,0},{2,3},{3,2},{4,5},{5,4},{6,7},{7,6},{8,9},{9,8},{10,11... | collective-permute-start | bytes 1179656 | tf_op jit(solution)/shard_map/ppermute | solution.py:78
  144.6 13.6 %copy-start.10 = (f32[2048]{0:T(1024)S(1)}, f32[2048]{0:T(1024)}, u32[]{:S(2)}) copy-start(f32[2048]{0:T(1024)} %param.27) | copy-start | bytes 24580
  144.6 13.8 %copy-start.12 = (f32[2048]{0:T(1024)S(1)}, f32[2048]{0:T(1024)}, u32[]{:S(2)}) copy-start(f32[2048]{0:T(1024)} %param.29) | copy-start | bytes 24580
  145.5 12.7 %all-to-all-start.1 = ((bf16[4,24,2048]{2,1,0:T(8,128)(2,1)}), bf16[4,24,2048]{2,1,0:T(8,128)(2,1)S(1)}, u32[]{:S(2)}, u32[]{:S(2)}) async-start(bf16[4,24,2048]{2,1,0:T(8,128)(2,1)} %bitcast.8), calls=%async_computation.1 | async-start | bytes 786432 | tf_op jit(solution)/shard_map/all_to_all | solution.py:74
  149.8 13.0 %copy-start.14 = (f32[384]{0:T(512)S(1)}, f32[384]{0:T(512)}, u32[]{:S(2)}) copy-start(f32[384]{0:T(512)} %param.34) | copy-start | bytes 4612
  149.8 13.0 %copy-start.15 = (f32[384]{0:T(512)S(1)}, f32[384]{0:T(512)}, u32[]{:S(2)}) copy-start(f32[384]{0:T(512)} %param.33) | copy-start | bytes 4612
  159.3 10.8 %all-to-all-start.2 = ((bf16[4,24,2048]{2,1,0:T(8,128)(2,1)}), bf16[4,24,2048]{2,1,0:T(8,128)(2,1)S(1)}, u32[]{:S(2)}, u32[]{:S(2)}) async-start(bf16[4,24,2048]{2,1,0:T(8,128)(2,1)} %broadcast_in_dim.34), calls=%async_computation.2 | async-start | bytes 786432 | tf_op jit(solution)/shard_map/all_to_all | solution.py:290
  162.8 3.1 %collective-permute-start.9 = (f32[2,384]{1,0:T(2,128)S(1)}, f32[2,384]{1,0:T(2,128)S(1)}, u32[]{:S(2)}, u32[]{:S(2)}) collective-permute-start(f32[2,384]{1,0:T(2,128)S(1)} %pad_maximum_fusion.1.scales), channel_id=1, source_target_pairs={{0,1},{1,0},{2,3},{3,2},{4,5},{5,4},{6,7},{7,6},{8,9},{9,8},{10,11... | collective-permute-start | bytes 9224 | tf_op jit(solution)/shard_map/ppermute | solution.py:78
  170.1 16.2 %copy-start.13 = (f32[2048]{0:T(1024)S(1)}, f32[2048]{0:T(1024)}, u32[]{:S(2)}) copy-start(f32[2048]{0:T(1024)} %param.35) | copy-start | bytes 24580
  (6 other events, 4.7 us)
Sparse Core Ops, SparseCore 0:
  31.4 79.6 all-gather.3

commit v5 on v4

--- a/solution.py
+++ b/solution.py
@@ -34,6 +34,18 @@
     return block, even, odd, far_a, far_b
 
 
+def ring_halves(block):
+    half = block.shape[0] // 2
+    low, high = block[:half], block[half:]
+    even1 = lax.ppermute(low, RING, pairs(0))
+    odd2 = lax.ppermute(high, RING, pairs(1))
+    even2 = lax.ppermute(high, RING, pairs(0))
+    odd1 = lax.ppermute(low, RING, pairs(1))
+    far_a = lax.ppermute(even1, RING, pairs(1))
+    far_b = lax.ppermute(odd2, RING, pairs(0))
+    return block, even1, even2, odd1, odd2, far_a, far_b
+
+
 def ring_labels():
     z = lax.axis_index("z")
     odd = z % 2
@@ -55,8 +67,8 @@
 def ring_dot(x, pieces, columns):
     size = pieces[0].shape[0]
     half = size // 2
-    own_at, even_at, odd_at, far_at = ring_labels()
-    starts = (own_at * size, even_at * size, odd_at * size, far_at * size, far_at * size + half)
+    own_at, even_at, odd_at, far_at = [label * size for label in ring_labels()]
+    starts = (own_at, even_at, even_at + half, odd_at, odd_at + half, far_at, far_at + half)
 
     def term(start, piece):
         cut = lax.dynamic_slice_in_dim(x, start, piece.shape[0], 1)
@@ -67,11 +79,6 @@
 
 def dot_t(a, b):
     return lax.dot_general(a, b, (((1,), (1,)), ((), ())), preferred_element_type=jnp.float32)
-
-
-def sum_over_chips(partial):
-    blocks = partial.reshape(lax.axis_size("x"), -1, partial.shape[1])
-    return jnp.sum(lax.all_to_all(blocks, "x", 0, 0, tiled=True).astype(jnp.float32), axis=0)
 
 
 def swap_cores(array):
@@ -132,20 +139,25 @@
     )(w_query, w_key, w_value, w_out.T)
 
 
-def mlp_shard_kernel(gate, up, down, out):
+def mlp_shard_kernel(gate, up, down, both, downs):
     units = gate.shape[1]
-    out[:, :units] = gate[...].astype(jnp.bfloat16)
-    out[:, units : 2 * units] = up[...].astype(jnp.bfloat16)
-    out[:, 2 * units :] = down[...].astype(jnp.bfloat16)
-
-
-def mlp_shard(w_gate, w_up, w_down):
+    both[:, :units] = gate[...].astype(jnp.bfloat16)
+    both[:, units:] = up[...].astype(jnp.bfloat16)
+    part = down[...].astype(jnp.bfloat16)
+    for peer in range(downs.shape[0]):
+        downs[peer] = part
+
+
+def mlp_shard(w_gate, w_up, w_down, peers):
     rows, units = w_gate.shape
-    shape = jax.ShapeDtypeStruct((rows, 3 * units), jnp.bfloat16)
-    return local_call(mlp_shard_kernel, shape, [VMEM] * 3, 10**7, 2**20)(w_gate, w_up, w_down.T)
-
-
-def retain_kernel(rate, core, product, cosine, sine, sq, sk, sv, own, even, odd, far_a, far_b, kept, sent):
+    shapes = [(rows, 2 * units), (peers, rows, units)]
+    shapes = [jax.ShapeDtypeStruct(shape, jnp.bfloat16) for shape in shapes]
+    call = local_call(mlp_shard_kernel, shapes, [VMEM] * 3, 10**7, 2**20, [VMEM] * 2)
+    return call(w_gate, w_up, w_down.T)
+
+
+def retain_kernel(rate, core, product, cosine, sine, sq, sk, sv, *refs):
+    pieces, (kept, sent) = refs[:-2], refs[-2:]
     width = sq.shape[1]
     cos, sin = cosine[...], sine[...]
     query = rotary(product[:, :width] * sq[...], cos, sin).astype(jnp.bfloat16)
@@ -168,7 +180,7 @@
     attended = jnp.concatenate(mine + other, axis=0).astype(jnp.bfloat16)
     half = length // 2
     at = 0
-    for piece in (own, even, odd, far_a, far_b):
+    for piece in pieces:
         to = at + piece.shape[0]
         term = dot_t(attended, piece[:, 3 * width :])
         kept[:, at:to] = term[:half]
@@ -187,16 +199,64 @@
     )
 
 
-def hold_kernel(weights, out):
-    out[...] = weights[...]
+def hold_kernel(weights, out, sem):
+    copy = pltpu.make_async_copy(weights, out, sem)
+    copy.start()
+    copy.wait()
 
 
 def hold(weights):
-    shape = jax.ShapeDtypeStruct(weights.shape, weights.dtype)
-    return local_call(hold_kernel, shape, [VMEM], 10**7, 4 * weights.size)(weights)
-
-
-def mlp_kernel(labels, x, weights, others, scales, other_scales, out):
+    return pl.pallas_call(
+        hold_kernel,
+        out_shape=jax.ShapeDtypeStruct(weights.shape, weights.dtype),
+        in_specs=[pl.BlockSpec(memory_space=pltpu.HBM)],
+        out_specs=VMEM,
+        scratch_shapes=[pltpu.SemaphoreType.DMA],
+        compiler_params=pltpu.CompilerParams(vmem_limit_bytes=16 * 2**20),
+        cost_estimate=pl.CostEstimate(flops=10**7, bytes_accessed=2**22, transcendentals=0),
+        name="hold",
+    )(weights)
+
+
+def settle_kernel(slots, terms, own, scale, gain, hidden, copies):
+    size = own.shape[1] // 4
+    total = 0.0
+    for j in range(4):
+        at = slice(j * size, (j + 1) * size)
+        there = pl.ds(pl.multiple_of(slots[j] * size, size), size)
+        mixed = jnp.sum(terms[:, :, there].astype(jnp.float32), axis=0) * scale[:, at]
+        block = (own[:, at].astype(jnp.float32) + mixed).astype(jnp.bfloat16)
+        hidden[:, at] = block
+        block = block.astype(jnp.float32)
+        total += jnp.sum(block * block, axis=-1, keepdims=True)
+    factor = lax.rsqrt(total / own.shape[1] + EPS)
+    for j in range(4):
+        at = slice(j * size, (j + 1) * size)
+        block = (hidden[:, at].astype(jnp.float32) * factor * gain[:, at]).astype(jnp.bfloat16)
+        for peer in range(copies.shape[0]):
+            copies[peer, :, at] = block
+
+
+def settle(slots, terms, own, scale, gain):
+    shapes = [jax.ShapeDtypeStruct(a.shape, jnp.bfloat16) for a in (own, terms)]
+    call = local_call(settle_kernel, shapes, [SMEM] + [VMEM] * 4, 10**7, 2**19, [VMEM] * 2)
+    return call(slots, terms, own, scale[None], gain[None])
+
+
+def pack_kernel(*refs):
+    at = 0
+    for piece in refs[:-1]:
+        refs[-1][at : at + piece.shape[0]] = piece[...]
+        at += piece.shape[0]
+
+
+def pack(pieces):
+    rows = sum(piece.shape[0] for piece in pieces)
+    shape = jax.ShapeDtypeStruct((rows, pieces[0].shape[1]), jnp.bfloat16)
+    return local_call(pack_kernel, shape, [VMEM] * len(pieces), 10**7, 2**22)(*pieces)
+
+
+def mlp_kernel(labels, x, weights, others, down, other_down, scales, other_scales, out):
     units = scales.shape[1]
     size = x.shape[1] // 4
     places = [pl.ds(pl.multiple_of(labels[p] * size, size), size) for p in range(4)]
@@ -204,24 +264,22 @@
     for held, scale in ((weights, scales), (others, other_scales)):
         both = jnp.zeros((x.shape[0], 2 * units), jnp.float32)
         for p, at in enumerate(places):
-            piece = held[:, p, :, : 2 * units].reshape(size, 2 * units)
+            piece = held[:, p].reshape(size, 2 * units)
             both += jnp.dot(x[:, at], piece, preferred_element_type=jnp.float32)
         gate = both[:, :units] * scale[0:1]
         up = both[:, units:] * scale[1:2]
         inner.append((gate / (1.0 + jnp.exp(-gate)) * up).astype(jnp.bfloat16))
     for p, at in enumerate(places):
-        total = 0.0
-        for held, part in zip((weights, others), inner):
-            total += dot_t(part, held[:, p, :, 2 * units :].reshape(size, units))
+        rows = slice(p * size, (p + 1) * size)
+        total = dot_t(inner[0], down[rows]) + dot_t(inner[1], other_down[rows])
         out[:, at] = total.astype(jnp.bfloat16)
 
 
-def mlp(labels, x, weights, others, scales, other_scales):
+def mlp(labels, x, *weights):
     shape = jax.ShapeDtypeStruct(x.shape, jnp.bfloat16)
-    flops = 4 * x.shape[0] * x.shape[1] * weights.shape[-1]
-    return local_call(mlp_kernel, shape, [SMEM] + [VMEM] * 5, flops, 4 * weights.size)(
-        labels, x, weights, others, scales, other_scales
-    )
+    size = sum(w.size for w in weights)
+    call = local_call(mlp_kernel, shape, [SMEM] + [VMEM] * 7, 2 * x.shape[0] * size, 2 * size)
+    return call(labels, x, *weights)
 
 
 def per_device(
@@ -251,13 +309,18 @@
     peers = lax.axis_size("y")
     heads = heads_shard(w_query, w_key, w_value, w_out, peers)
     heads = lax.all_to_all(heads, "y", 0, 0, tiled=True).reshape(-1, heads.shape[2])
-    own = ring_blocks(mlp_shard(w_gate, w_up, w_down))
-    mlp_weights = lax.all_gather(own, "y", axis=0)
-    mlp_weights = hold(mlp_weights)
-    mlp_others = swap_cores(mlp_weights)
+    own, downs = mlp_shard(w_gate, w_up, w_down, peers)
+    own = ring_blocks(own)
+    weights = lax.all_gather(own, "y", axis=0)
+    weights = hold(weights)
+    others = swap_cores(weights)
     mlp_scales = jnp.stack([scale_gate, scale_up])
     other_scales = swap_cores(mlp_scales)
-    heads = ring_pieces(heads)
+    heads = ring_halves(heads)
+    downs = lax.all_to_all(downs, "y", 0, 0, tiled=True).reshape(-1, downs.shape[2])
+    downs = ring_pieces(downs)
+    downs = pack(downs)
+    other_downs = swap_cores(downs)
     all_rows = lax.all_gather(own_rows, TP, axis=0, tiled=True)
 
     values = all_rows.astype(f32)
@@ -272,26 +335,19 @@
         decay_rate, core, product, jnp.cos(angles), jnp.sin(angles), scales, heads
     )
 
-    slots = ring_slots()
-
-    def in_order(values):
-        size = width // 4
-        return jnp.concatenate(
-            [lax.dynamic_slice_in_dim(values, slot * size, size, 1) for slot in slots], axis=1
-        )
-
     got = swap_cores(sent)
-    mixed = sum_over_chips((kept + got.astype(f32)).astype(bf16))
-    mixed = in_order(mixed) * scale_out
-    hidden = (own_rows.astype(f32) + mixed).astype(bf16)
-    values = hidden.astype(f32)
-    mlp_in = (values * inv_rms(values) * mlp_gain).astype(bf16)
-    copies = jnp.broadcast_to(mlp_in[None], (lax.axis_size("x"), rows, width))
+    chips = lax.axis_size("x")
+    both = (kept + got.astype(f32)).astype(bf16).reshape(chips, rows, width)
+    terms = lax.all_to_all(both, "x", 0, 0, tiled=True)
+    slots = jnp.stack(ring_slots()).astype(jnp.int32)
+    hidden, copies = settle(slots, terms, own_rows, scale_out, mlp_gain)
     mlp_in = lax.all_to_all(copies, "x", 0, 0, tiled=True).reshape(-1, width)
-
     labels = jnp.stack(ring_labels()).astype(jnp.int32)
-    partial = mlp(labels, mlp_in, mlp_weights, mlp_others, mlp_scales, other_scales)
-    channel = sum_over_chips(partial) * scale_down
+    partial = mlp(
+        labels, mlp_in, weights, others, downs, other_downs, mlp_scales, other_scales
+    )
+    terms = lax.all_to_all(partial.reshape(chips, rows, width), "x", 0, 0, tiled=True)
+    channel = jnp.sum(terms.astype(f32), axis=0) * scale_down
     return (hidden.astype(f32) + channel).astype(bf16)[None]
 
 
@@ -305,6 +361,4 @@
         by_rows, by_rows, by_cols, P(TP), P(TP), P(),
     )
 
-    return jax.shard_map(
-        per_device, mesh=grid, in_specs=in_specs, out_specs=P(seqs, TP, None), check_vma=False
-    )
+    return jax.shard_map(per_device, mesh=grid, in_specs=in_specs, out_specs=P(seqs, TP, None), check_vma=False)

time: 195 us -> 218 us (1.12)
  the two profiles are of different devices: /device:TPU:24 before, /device:TPU:2 now
where the time goes in v5:
time: 218 us; the launch traced here: 217 us
  starting transfers between devices  76.3 us (35%)
  waiting for transfers between devices  68.6 us (31%)
  blocking collectives  23.3 us (11%)
  between operations  14.6 us (7%)
  Pallas kernels  14.2 us (7%)
  local copies, waits for them, and re-layouts  11 us (5%)
  other arithmetic  5.06 us (2%)
  matrix products  3.79 us (2%)
    all_to_all x1, waiting for transfers between devices, per_device(): lax.all_to_all(heads, 'y', 0, 0, tiled=True).reshape(-1, heads.shape[2])  17.3 us
    all_gather x1, blocking collectives, per_device(): all_rows = lax.all_gather(own_rows, TP, axis=0, tiled=True)  13.5 us
    all_to_all x1, waiting for transfers between devices, per_device(): lax.all_to_all(downs, 'y', 0, 0, tiled=True).reshape(-1, downs.shape[2])  11.6 us
    ppermute x1, waiting for transfers between devices, ring_halves(): far_b = lax.ppermute(odd2, RING, pairs(0))  10.2 us
    unnamed x52, local copies, waits for them, and re-layouts  9.86 us
    all_to_all x1, blocking collectives, per_device(): lax.all_to_all(partial.reshape(chips, rows, width), 'x', 0, 0, tiled=True)  9.78 us
    ppermute x1, starting transfers between devices, ring_blocks(): odd = lax.ppermute(block, RING, pairs(1))  9.13 us
    ppermute x4, starting transfers between devices, swap_cores(): return lax.ppermute(array, 'core', [(0, 1), (1, 0)])  8.02 us
  transfers between devices with their start and end apart: 22, of which 11 were waited for; matrix products, arithmetic and copies ran while one was open for 4% of the time, Pallas kernels for 3%

profile of v5, /device:TPU:2, one launch (start us, length us, event | category | flops | bytes accessed | tf_op | source)
XLA Modules:
  0.0 216.9 jit_solution(9603305931985779372)
XLA Ops:
  10.0 4.3 %collective-permute-start.7 = (bf16[64,768]{1,0:T(8,128)(2,1)S(1)}, bf16[64,768]{1,0:T(8,128)(2,1)S(1)}, u32[]{:S(2)}, u32[]{:S(2)}) collective-permute-start(bf16[64,768]{1,0:T(8,128)(2,1)S(1)} %get-tuple-element.15), channel_id=1, source_target_pairs={{0,64},{64,0},{128,192},{192,128},{256,320},{320,256},{384,448},{4... | collective-permute-start | bytes 294920 | tf_op jit(solution)/shard_map/ppermute | solution.py:61
  14.3 9.1 %collective-permute-start.8 = (bf16[64,768]{1,0:T(8,128)(2,1)S(1)}, bf16[64,768]{1,0:T(8,128)(2,1)S(1)}, u32[]{:S(2)}, u32[]{:S(2)}) collective-permute-start(bf16[64,768]{1,0:T(8,128)(2,1)S(1)} %get-tuple-element.15), channel_id=1, source_target_pairs={{64,128},{128,64},{192,256},{256,192},{320,384},{384,320},{448,0},... | collective-permute-start | bytes 294920 | tf_op jit(solution)/shard_map/ppermute | solution.py:62
  26.3 7.2 %collective-permute-done.9 = bf16[64,768]{1,0:T(8,128)(2,1)S(1)} collective-permute-done((bf16[64,768]{1,0:T(8,128)(2,1)S(1)}, bf16[64,768]{1,0:T(8,128)(2,1)S(1)}, u32[]{:S(2)}, u32[]{:S(2)}) %collective-permute-start.9) | collective-permute-done | bytes 98336 | tf_op jit(solution)/shard_map/ppermute | solution.py:63
  34.3 7.1 %all-to-all-start.3 = ((bf16[8,64,384]{2,1,0:T(8,128)(2,1)}), bf16[8,64,384]{2,1,0:T(8,128)(2,1)S(1)}, u32[]{:S(2)}, u32[]{:S(2)}) async-start(bf16[8,64,384]{2,1,0:T(8,128)(2,1)} %get-tuple-element.16), calls=%async_computation.3 | async-start | bytes 786432 | tf_op jit(solution)/shard_map/all_to_all | solution.py:320
  43.4 11.6 %all-to-all-done.3 = bf16[8,64,384]{2,1,0:T(8,128)(2,1)S(1)} async-done(((bf16[8,64,384]{2,1,0:T(8,128)(2,1)}), bf16[8,64,384]{2,1,0:T(8,128)(2,1)S(1)}, u32[]{:S(2)}, u32[]{:S(2)}) %all-to-all-start.3) | async-done | bytes 393248 | tf_op jit(solution)/shard_map/all_to_all | solution.py:320
  55.0 3.6 %all-to-all-start = ((bf16[8,64,1024]{2,1,0:T(8,128)(2,1)}), bf16[8,64,1024]{2,1,0:T(8,128)(2,1)S(1)}, u32[]{:S(2)}, u32[]{:S(2)}) async-start(bf16[8,64,1024]{2,1,0:T(8,128)(2,1)} %heads_shard.1), calls=%async_computation | async-start | bytes 2097152 | tf_op jit(solution)/shard_map/all_to_all | solution.py:311
  58.6 13.5 %all-gather = bf16[1,192,2048]{2,1,0:T(8,128)(2,1)S(1)} all-gather(bf16[1,24,2048]{2,1,0:T(8,128)(2,1)S(1)} %copy-done.5), channel_id=2, replica_groups=mesh['rep'=2,'z'=4,'y'=8,'x'=4,'core'=2] {'x','core'}, dimensions={1}, use_global_device_ids=true | all-gather | bytes 884736 | tf_op jit(solution)/shard_map/all_gather | solution.py:324
  74.3 2.8 %collective-permute-start.12 = (bf16[512,384]{1,0:T(8,128)(2,1)S(1)}, bf16[512,384]{1,0:T(8,128)(2,1)S(1)}, u32[]{:S(2)}, u32[]{:S(2)}) collective-permute-start(bf16[512,384]{1,0:T(8,128)(2,1)S(1)} %bitcast.39), channel_id=1, source_target_pairs={{64,128},{128,64},{192,256},{256,192},{320,384},{384,320},{448,0},... | collective-permute-start | bytes 1179656 | tf_op jit(solution)/shard_map/ppermute | solution.py:31
  78.3 17.3 %all-to-all-done = bf16[8,64,1024]{2,1,0:T(8,128)(2,1)S(1)} async-done(((bf16[8,64,1024]{2,1,0:T(8,128)(2,1)}), bf16[8,64,1024]{2,1,0:T(8,128)(2,1)S(1)}, u32[]{:S(2)}, u32[]{:S(2)}) %all-to-all-start) | async-done | bytes 1048608 | tf_op jit(solution)/shard_map/all_to_all | solution.py:311
  96.7 5.4 %collective-permute-start.3 = (bf16[256,1024]{1,0:T(8,128)(2,1)}, bf16[256,1024]{1,0:T(8,128)(2,1)S(1)}, u32[]{:S(2)}, u32[]{:S(2)}) collective-permute-start(bf16[256,1024]{1,0:T(8,128)(2,1)} %bitcast.10), channel_id=1, source_target_pairs={{64,128},{128,64},{192,256},{256,192},{320,384},{384,320},{448,0},... | collective-permute-start | bytes 1572872 | tf_op jit(solution)/shard_map/ppermute | solution.py:41
  104.1 2.7 %collective-permute-start.14 = (bf16[256,384]{1,0:T(8,128)(2,1)S(1)}, bf16[256,384]{1,0:T(8,128)(2,1)S(1)}, u32[]{:S(2)}, u32[]{:S(2)}) collective-permute-start(bf16[256,384]{1,0:T(8,128)(2,1)S(1)} %slice.62), channel_id=1, source_target_pairs={{0,64},{64,0},{128,192},{192,128},{256,320},{320,256},{384,448},{4... | collective-permute-start | bytes 589832 | tf_op jit(solution)/shard_map/ppermute | solution.py:33
  106.8 3.1 %collective-permute-start = (bf16[256,1024]{1,0:T(8,128)(2,1)}, bf16[256,1024]{1,0:T(8,128)(2,1)}, u32[]{:S(2)}, u32[]{:S(2)}) collective-permute-start(bf16[256,1024]{1,0:T(8,128)(2,1)} %bitcast.9), channel_id=1, source_target_pairs={{0,64},{64,0},{128,192},{192,128},{256,320},{320,256},{384,448},{4... | collective-permute-start | bytes 1572872 | tf_op jit(solution)/shard_map/ppermute | solution.py:40
  111.7 4.8 %collective-permute-done.13.refs_3_ = bf16[256,384]{1,0:T(8,128)(2,1)S(1)} collective-permute-done((bf16[256,384]{1,0:T(8,128)(2,1)S(1)}, bf16[256,384]{1,0:T(8,128)(2,1)S(1)}, u32[]{:S(2)}, u32[]{:S(2)}) %collective-permute-start.13) | collective-permute-done | bytes 196640 | tf_op jit(solution)/shard_map/ppermute | solution.py:32
  123.7 4.9 %collective-permute-start.2 = (bf16[256,1024]{1,0:T(8,128)(2,1)}, bf16[256,1024]{1,0:T(8,128)(2,1)}, u32[]{:S(2)}, u32[]{:S(2)}) collective-permute-start(bf16[256,1024]{1,0:T(8,128)(2,1)} %bitcast.9), channel_id=1, source_target_pairs={{64,128},{128,64},{192,256},{256,192},{320,384},{384,320},{448,0},... | collective-permute-start | bytes 1572872 | tf_op jit(solution)/shard_map/ppermute | solution.py:43
  137.1 3.9 %collective-permute-start.5 = (bf16[256,1024]{1,0:T(8,128)(2,1)S(1)}, bf16[256,1024]{1,0:T(8,128)(2,1)S(1)}, u32[]{:S(2)}, u32[]{:S(2)}) collective-permute-start(bf16[256,1024]{1,0:T(8,128)(2,1)S(1)} %collective-permute-done.3.refs_4_), channel_id=1, source_target_pairs={{0,64},{64,0},{128,192},{192,128},{256,320},{320,256},{384,448},{4... | collective-permute-start | bytes 1572872 | tf_op jit(solution)/shard_map/ppermute | solution.py:45
  142.2 4.1 %collective-permute-start.4 = (bf16[256,1024]{1,0:T(8,128)(2,1)}, bf16[256,1024]{1,0:T(8,128)(2,1)S(1)}, u32[]{:S(2)}, u32[]{:S(2)}) collective-permute-start(bf16[256,1024]{1,0:T(8,128)(2,1)} %collective-permute-done.refs_1_), channel_id=1, source_target_pairs={{64,128},{128,64},{192,256},{256,192},{320,384},{384,320},{448,0},... | collective-permute-start | bytes 1572872 | tf_op jit(solution)/shard_map/ppermute | solution.py:44
  147.6 4.2 %collective-permute-done.1.refs_2_ = bf16[256,1024]{1,0:T(8,128)(2,1)S(1)} collective-permute-done((bf16[256,1024]{1,0:T(8,128)(2,1)}, bf16[256,1024]{1,0:T(8,128)(2,1)S(1)}, u32[]{:S(2)}, u32[]{:S(2)}) %collective-permute-start.1) | collective-permute-done | bytes 524320 | tf_op jit(solution)/shard_map/ppermute | solution.py:42
  152.1 10.2 %collective-permute-done.5.refs_6_ = bf16[256,1024]{1,0:T(8,128)(2,1)S(1)} collective-permute-done((bf16[256,1024]{1,0:T(8,128)(2,1)S(1)}, bf16[256,1024]{1,0:T(8,128)(2,1)S(1)}, u32[]{:S(2)}, u32[]{:S(2)}) %collective-permute-start.5) | collective-permute-done | bytes 524320 | tf_op jit(solution)/shard_map/ppermute | solution.py:45
  169.6 4.8 %all-to-all-start.1 = ((bf16[4,24,2048]{2,1,0:T(8,128)(2,1)}), bf16[4,24,2048]{2,1,0:T(8,128)(2,1)S(1)}, u32[]{:S(2)}, u32[]{:S(2)}) async-start(bf16[4,24,2048]{2,1,0:T(8,128)(2,1)} %bitcast.14), calls=%async_computation.1 | async-start | bytes 786432 | tf_op jit(solution)/shard_map/all_to_all | solution.py:341
  174.5 6.8 %all-to-all-done.1.terms = bf16[4,24,2048]{2,1,0:T(8,128)(2,1)S(1)} async-done(((bf16[4,24,2048]{2,1,0:T(8,128)(2,1)}), bf16[4,24,2048]{2,1,0:T(8,128)(2,1)S(1)}, u32[]{:S(2)}, u32[]{:S(2)}) %all-to-all-start.1) | async-done | bytes 393248 | tf_op jit(solution)/shard_map/all_to_all | solution.py:341
  182.8 4.9 %all-to-all-start.2 = ((bf16[4,24,2048]{2,1,0:T(8,128)(2,1)}), bf16[4,24,2048]{2,1,0:T(8,128)(2,1)S(1)}, u32[]{:S(2)}, u32[]{:S(2)}) async-start(bf16[4,24,2048]{2,1,0:T(8,128)(2,1)} %get-tuple-element.14), calls=%async_computation.2 | async-start | bytes 786432 | tf_op jit(solution)/shard_map/all_to_all | solution.py:344
  190.8 2.8 %all-to-all-done.2 = bf16[4,24,2048]{2,1,0:T(8,128)(2,1)S(1)} async-done(((bf16[4,24,2048]{2,1,0:T(8,128)(2,1)}), bf16[4,24,2048]{2,1,0:T(8,128)(2,1)S(1)}, u32[]{:S(2)}, u32[]{:S(2)}) %all-to-all-start.2) | async-done | bytes 393248 | tf_op jit(solution)/shard_map/all_to_all | solution.py:344
  193.6 5.9 %shard_map.176 = bf16[96,2048]{1,0:T(8,128)(2,1)S(1)} custom-call(s32[4]{0:T(128)S(1)} %pad_add_fusion.1.labels, bf16[96,2048]{1,0:T(8,128)(2,1)S(1)} %bitcast.41, bf16[8,4,64,768]{3,2,1,0:T(8,128)(2,1)} %hold.1.weights, bf16[8,4,64,768]{3,2,1,0:T(8,128)(2,1)} %collective-permute-done.10.others, bf16[2048,384]{1,0:T(8,128)(2,1)S(1)} %shard_map.175.down, ...), custom_call_target="tpu_custom_call" | custom-call | flops 906264576 | bytes 9440256 | tf_op jit(solution)/shard_map/pallas_call | solution.py:282
  199.5 9.8 %all_to_all.25 = bf16[4,24,2048]{2,1,0:T(8,128)(2,1)S(1)} all-to-all(bf16[4,24,2048]{2,1,0:T(8,128)(2,1)S(1)} %bitcast.42), channel_id=1, replica_groups=mesh['rep'=2,'z'=4,'y'=8,'x'=4,'core'=2] {'x'}, dimensions={0} | all-to-all | bytes 786432 | tf_op jit(solution)/shard_map/all_to_all | solution.py:349
  (106 shorter events, 47.6 us)
Async XLA Ops:
  6.5 122.1 %all-gather.4.cloned.1.call-start = ((), (), s32[]{:S(2)}) async-start(), calls=%async_computation.5 | async-start | bytes 3538944 | tf_op jit(solution)/shard_map/all_gather | solution.py:314
  10.0 15.3 %collective-permute-start.7 = (bf16[64,768]{1,0:T(8,128)(2,1)S(1)}, bf16[64,768]{1,0:T(8,128)(2,1)S(1)}, u32[]{:S(2)}, u32[]{:S(2)}) collective-permute-start(bf16[64,768]{1,0:T(8,128)(2,1)S(1)} %get-tuple-element.15), channel_id=1, source_target_pairs={{0,64},{64,0},{128,192},{192,128},{256,320},{320,256},{384,448},{4... | collective-permute-start | bytes 294920 | tf_op jit(solution)/shard_map/ppermute | solution.py:61
  14.3 12.0 %collective-permute-start.8 = (bf16[64,768]{1,0:T(8,128)(2,1)S(1)}, bf16[64,768]{1,0:T(8,128)(2,1)S(1)}, u32[]{:S(2)}, u32[]{:S(2)}) collective-permute-start(bf16[64,768]{1,0:T(8,128)(2,1)S(1)} %get-tuple-element.15), channel_id=1, source_target_pairs={{64,128},{128,64},{192,256},{256,192},{320,384},{384,320},{448,0},... | collective-permute-start | bytes 294920 | tf_op jit(solution)/shard_map/ppermute | solution.py:62
  23.4 10.0 %collective-permute-start.9 = (bf16[64,768]{1,0:T(8,128)(2,1)S(1)}, bf16[64,768]{1,0:T(8,128)(2,1)S(1)}, u32[]{:S(2)}, u32[]{:S(2)}) collective-permute-start(bf16[64,768]{1,0:T(8,128)(2,1)S(1)} %get-tuple-element.15), channel_id=1, source_target_pairs={{0,128},{64,192},{128,256},{192,320},{256,384},{320,448},{384,0},{... | collective-permute-start | bytes 294920 | tf_op jit(solution)/shard_map/ppermute | solution.py:63
  34.3 20.7 %all-to-all-start.3 = ((bf16[8,64,384]{2,1,0:T(8,128)(2,1)}), bf16[8,64,384]{2,1,0:T(8,128)(2,1)S(1)}, u32[]{:S(2)}, u32[]{:S(2)}) async-start(bf16[8,64,384]{2,1,0:T(8,128)(2,1)} %get-tuple-element.16), calls=%async_computation.3 | async-start | bytes 786432 | tf_op jit(solution)/shard_map/all_to_all | solution.py:320
  43.4 33.6 %copy-start.22 = (f32[2048]{0:T(1024)S(1)}, f32[2048]{0:T(1024)}, u32[]{:S(2)}) copy-start(f32[2048]{0:T(1024)} %param.19) | copy-start | bytes 24580
  55.0 40.6 %all-to-all-start = ((bf16[8,64,1024]{2,1,0:T(8,128)(2,1)}), bf16[8,64,1024]{2,1,0:T(8,128)(2,1)S(1)}, u32[]{:S(2)}, u32[]{:S(2)}) async-start(bf16[8,64,1024]{2,1,0:T(8,128)(2,1)} %heads_shard.1), calls=%async_computation | async-start | bytes 2097152 | tf_op jit(solution)/shard_map/all_to_all | solution.py:311
  72.3 29.7 %collective-permute-start.11 = (bf16[512,384]{1,0:T(8,128)(2,1)S(1)}, bf16[512,384]{1,0:T(8,128)(2,1)S(1)}, u32[]{:S(2)}, u32[]{:S(2)}) collective-permute-start(bf16[512,384]{1,0:T(8,128)(2,1)S(1)} %bitcast.38), channel_id=1, source_target_pairs={{0,64},{64,0},{128,192},{192,128},{256,320},{320,256},{384,448},{4... | collective-permute-start | bytes 1179656 | tf_op jit(solution)/shard_map/ppermute | solution.py:30
  74.3 29.8 %collective-permute-start.12 = (bf16[512,384]{1,0:T(8,128)(2,1)S(1)}, bf16[512,384]{1,0:T(8,128)(2,1)S(1)}, u32[]{:S(2)}, u32[]{:S(2)}) collective-permute-start(bf16[512,384]{1,0:T(8,128)(2,1)S(1)} %bitcast.39), channel_id=1, source_target_pairs={{64,128},{128,64},{192,256},{256,192},{320,384},{384,320},{448,0},... | collective-permute-start | bytes 1179656 | tf_op jit(solution)/shard_map/ppermute | solution.py:31
  96.7 38.2 %collective-permute-start.3 = (bf16[256,1024]{1,0:T(8,128)(2,1)}, bf16[256,1024]{1,0:T(8,128)(2,1)S(1)}, u32[]{:S(2)}, u32[]{:S(2)}) collective-permute-start(bf16[256,1024]{1,0:T(8,128)(2,1)} %bitcast.10), channel_id=1, source_target_pairs={{64,128},{128,64},{192,256},{256,192},{320,384},{384,320},{448,0},... | collective-permute-start | bytes 1572872 | tf_op jit(solution)/shard_map/ppermute | solution.py:41
  102.1 14.3 %collective-permute-start.13 = (bf16[256,384]{1,0:T(8,128)(2,1)S(1)}, bf16[256,384]{1,0:T(8,128)(2,1)S(1)}, u32[]{:S(2)}, u32[]{:S(2)}) collective-permute-start(bf16[256,384]{1,0:T(8,128)(2,1)S(1)} %slice.61), channel_id=1, source_target_pairs={{64,128},{128,64},{192,256},{256,192},{320,384},{384,320},{448,0},... | collective-permute-start | bytes 589832 | tf_op jit(solution)/shard_map/ppermute | solution.py:32
  104.1 13.0 %collective-permute-start.14 = (bf16[256,384]{1,0:T(8,128)(2,1)S(1)}, bf16[256,384]{1,0:T(8,128)(2,1)S(1)}, u32[]{:S(2)}, u32[]{:S(2)}) collective-permute-start(bf16[256,384]{1,0:T(8,128)(2,1)S(1)} %slice.62), channel_id=1, source_target_pairs={{0,64},{64,0},{128,192},{192,128},{256,320},{320,256},{384,448},{4... | collective-permute-start | bytes 589832 | tf_op jit(solution)/shard_map/ppermute | solution.py:33
  106.8 30.3 %collective-permute-start = (bf16[256,1024]{1,0:T(8,128)(2,1)}, bf16[256,1024]{1,0:T(8,128)(2,1)}, u32[]{:S(2)}, u32[]{:S(2)}) collective-permute-start(bf16[256,1024]{1,0:T(8,128)(2,1)} %bitcast.9), channel_id=1, source_target_pairs={{0,64},{64,0},{128,192},{192,128},{256,320},{320,256},{384,448},{4... | collective-permute-start | bytes 1572872 | tf_op jit(solution)/shard_map/ppermute | solution.py:40
  121.8 69.0 %collective-permute-start.15 = (bf16[2048,384]{1,0:T(8,128)(2,1)S(1)}, bf16[2048,384]{1,0:T(8,128)(2,1)}, u32[]{:S(2)}, u32[]{:S(2)}) collective-permute-start(bf16[2048,384]{1,0:T(8,128)(2,1)S(1)} %shard_map.175.down), channel_id=1, source_target_pairs={{0,1},{1,0},{2,3},{3,2},{4,5},{5,4},{6,7},{7,6},{8,9},{9,8},{10,11... | collective-permute-start | bytes 4718600 | tf_op jit(solution)/shard_map/ppermute | solution.py:85
  123.7 18.5 %collective-permute-start.2 = (bf16[256,1024]{1,0:T(8,128)(2,1)}, bf16[256,1024]{1,0:T(8,128)(2,1)}, u32[]{:S(2)}, u32[]{:S(2)}) collective-permute-start(bf16[256,1024]{1,0:T(8,128)(2,1)} %bitcast.9), channel_id=1, source_target_pairs={{64,128},{128,64},{192,256},{256,192},{320,384},{384,320},{448,0},... | collective-permute-start | bytes 1572872 | tf_op jit(solution)/shard_map/ppermute | solution.py:43
  132.4 61.3 %collective-permute-start.10 = (bf16[8,4,64,768]{3,2,1,0:T(8,128)(2,1)}, bf16[8,4,64,768]{3,2,1,0:T(8,128)(2,1)}, u32[]{:S(2)}, u32[]{:S(2)}) collective-permute-start(bf16[8,4,64,768]{3,2,1,0:T(8,128)(2,1)} %hold.1.weights), channel_id=1, source_target_pairs={{0,1},{1,0},{2,3},{3,2},{4,5},{5,4},{6,7},{7,6},{8,9},{9,8},{10,11... | collective-permute-start | bytes 9437192 | tf_op jit(solution)/shard_map/ppermute | solution.py:85
  134.9 16.9 %collective-permute-start.1 = (bf16[256,1024]{1,0:T(8,128)(2,1)}, bf16[256,1024]{1,0:T(8,128)(2,1)S(1)}, u32[]{:S(2)}, u32[]{:S(2)}) collective-permute-start(bf16[256,1024]{1,0:T(8,128)(2,1)} %bitcast.10), channel_id=1, source_target_pairs={{0,64},{64,0},{128,192},{192,128},{256,320},{320,256},{384,448},{4... | collective-permute-start | bytes 1572872 | tf_op jit(solution)/shard_map/ppermute | solution.py:42
  137.1 25.3 %collective-permute-start.5 = (bf16[256,1024]{1,0:T(8,128)(2,1)S(1)}, bf16[256,1024]{1,0:T(8,128)(2,1)S(1)}, u32[]{:S(2)}, u32[]{:S(2)}) collective-permute-start(bf16[256,1024]{1,0:T(8,128)(2,1)S(1)} %collective-permute-done.3.refs_4_), channel_id=1, source_target_pairs={{0,64},{64,0},{128,192},{192,128},{256,320},{320,256},{384,448},{4... | collective-permute-start | bytes 1572872 | tf_op jit(solution)/shard_map/ppermute | solution.py:45
  142.2 20.3 %collective-permute-start.4 = (bf16[256,1024]{1,0:T(8,128)(2,1)}, bf16[256,1024]{1,0:T(8,128)(2,1)S(1)}, u32[]{:S(2)}, u32[]{:S(2)}) collective-permute-start(bf16[256,1024]{1,0:T(8,128)(2,1)} %collective-permute-done.refs_1_), channel_id=1, source_target_pairs={{64,128},{128,64},{192,256},{256,192},{320,384},{384,320},{448,0},... | collective-permute-start | bytes 1572872 | tf_op jit(solution)/shard_map/ppermute | solution.py:44
  165.0 3.7 %collective-permute-start.6 = (bf16[96,2048]{1,0:T(8,128)(2,1)S(1)}, bf16[96,2048]{1,0:T(8,128)(2,1)S(1)}, u32[]{:S(2)}, u32[]{:S(2)}) collective-permute-start(bf16[96,2048]{1,0:T(8,128)(2,1)S(1)} %get-tuple-element.12), channel_id=1, source_target_pairs={{0,1},{1,0},{2,3},{3,2},{4,5},{5,4},{6,7},{7,6},{8,9},{9,8},{10,11... | collective-permute-start | bytes 1179656 | tf_op jit(solution)/shard_map/ppermute | solution.py:85
  168.7 19.0 %copy-start.25 = (f32[384]{0:T(512)S(1)}, f32[384]{0:T(512)}, u32[]{:S(2)}) copy-start(f32[384]{0:T(512)} %param.34) | copy-start | bytes 4612
  169.6 11.7 %all-to-all-start.1 = ((bf16[4,24,2048]{2,1,0:T(8,128)(2,1)}), bf16[4,24,2048]{2,1,0:T(8,128)(2,1)S(1)}, u32[]{:S(2)}, u32[]{:S(2)}) async-start(bf16[4,24,2048]{2,1,0:T(8,128)(2,1)} %bitcast.14), calls=%async_computation.1 | async-start | bytes 786432 | tf_op jit(solution)/shard_map/all_to_all | solution.py:341
  182.8 10.8 %all-to-all-start.2 = ((bf16[4,24,2048]{2,1,0:T(8,128)(2,1)}), bf16[4,24,2048]{2,1,0:T(8,128)(2,1)S(1)}, u32[]{:S(2)}, u32[]{:S(2)}) async-start(bf16[4,24,2048]{2,1,0:T(8,128)(2,1)} %get-tuple-element.14), calls=%async_computation.2 | async-start | bytes 786432 | tf_op jit(solution)/shard_map/all_to_all | solution.py:344
  187.7 3.1 %collective-permute-start.16 = (f32[2,384]{1,0:T(2,128)S(1)}, f32[2,384]{1,0:T(2,128)S(1)}, u32[]{:S(2)}, u32[]{:S(2)}) collective-permute-start(f32[2,384]{1,0:T(2,128)S(1)} %pad_maximum_fusion.1.scales), channel_id=1, source_target_pairs={{0,1},{1,0},{2,3},{3,2},{4,5},{5,4},{6,7},{7,6},{8,9},{9,8},{10,11... | collective-permute-start | bytes 9224 | tf_op jit(solution)/shard_map/ppermute | solution.py:85
  (24 other events, 195.6 us)
Sparse Core Ops, SparseCore 0:
  34.4 69.5 all-gather.3

commit v6 on v4

--- a/solution.py
+++ b/solution.py
@@ -46,10 +46,13 @@
 
 
 def ring_blocks(block):
+    half = block.shape[0] // 2
     even = lax.ppermute(block, RING, pairs(0))
     odd = lax.ppermute(block, RING, pairs(1))
-    far = lax.ppermute(block, RING, [(i, (i + 2) % 8) for i in range(8)])
-    return jnp.stack([block, even, odd, far])
+    far_a = lax.ppermute(block[:half], RING, [(i, (i + 2) % 8) for i in range(8)])
+    far_b = lax.ppermute(block[half:], RING, [(i, (i - 2) % 8) for i in range(8)])
+    blocks = jnp.concatenate([block, even, odd, far_a, far_b], axis=0)
+    return blocks.reshape(4, *block.shape)
 
 
 def ring_dot(x, pieces, columns):
@@ -72,6 +75,22 @@
 def sum_over_chips(partial):
     blocks = partial.reshape(lax.axis_size("x"), -1, partial.shape[1])
     return jnp.sum(lax.all_to_all(blocks, "x", 0, 0, tiled=True).astype(jnp.float32), axis=0)
+
+
+def sum_on_chips(partial):
+    half = partial.shape[0] // 2
+    first, second = partial[:half], partial[half:]
+
+    def swap(array, offset):
+        return lax.ppermute(array, "x", pairs(offset, 4)).astype(jnp.float32)
+
+    a = first.astype(jnp.float32) + swap(first, 0)
+    b = second.astype(jnp.float32) + swap(second, 1)
+    a, b = a.astype(jnp.bfloat16), b.astype(jnp.bfloat16)
+    return jnp.concatenate(
+        [a.astype(jnp.float32) + swap(a, 1), b.astype(jnp.float32) + swap(b, 0)],
+        axis=0,
+    )
 
 
 def swap_cores(array):
@@ -187,41 +206,51 @@
     )
 
 
-def hold_kernel(weights, out):
-    out[...] = weights[...]
-
-
-def hold(weights):
-    shape = jax.ShapeDtypeStruct(weights.shape, weights.dtype)
-    return local_call(hold_kernel, shape, [VMEM], 10**7, 4 * weights.size)(weights)
-
-
-def mlp_kernel(labels, x, weights, others, scales, other_scales, out):
+def mlp_kernel(labels, x, weights, others, scales, other_scales, out, held, sems):
     units = scales.shape[1]
     size = x.shape[1] // 4
+    copies = [
+        [pltpu.make_async_copy(w.at[:, p], held.at[i, p], sems.at[i, p]) for p in range(4)]
+        for i, w in enumerate((weights, others))
+    ]
+    for copy in copies[0] + copies[1]:
+        copy.start()
     places = [pl.ds(pl.multiple_of(labels[p] * size, size), size) for p in range(4)]
     inner = []
-    for held, scale in ((weights, scales), (others, other_scales)):
+    for i, scale in enumerate((scales, other_scales)):
         both = jnp.zeros((x.shape[0], 2 * units), jnp.float32)
         for p, at in enumerate(places):
-            piece = held[:, p, :, : 2 * units].reshape(size, 2 * units)
+            copies[i][p].wait()
+            piece = held[i, p, :, :, : 2 * units].reshape(size, 2 * units)
             both += jnp.dot(x[:, at], piece, preferred_element_type=jnp.float32)
         gate = both[:, :units] * scale[0:1]
         up = both[:, units:] * scale[1:2]
         inner.append((gate / (1.0 + jnp.exp(-gate)) * up).astype(jnp.bfloat16))
     for p, at in enumerate(places):
         total = 0.0
-        for held, part in zip((weights, others), inner):
-            total += dot_t(part, held[:, p, :, 2 * units :].reshape(size, units))
+        for i, part in enumerate(inner):
+            total += dot_t(part, held[i, p, :, :, 2 * units :].reshape(size, units))
         out[:, at] = total.astype(jnp.bfloat16)
 
 
 def mlp(labels, x, weights, others, scales, other_scales):
-    shape = jax.ShapeDtypeStruct(x.shape, jnp.bfloat16)
-    flops = 4 * x.shape[0] * x.shape[1] * weights.shape[-1]
-    return local_call(mlp_kernel, shape, [SMEM] + [VMEM] * 5, flops, 4 * weights.size)(
-        labels, x, weights, others, scales, other_scales
-    )
+    hbm = pl.BlockSpec(memory_space=pltpu.HBM)
+    peers, pieces = weights.shape[:2]
+    return pl.pallas_call(
+        mlp_kernel,
+        out_shape=jax.ShapeDtypeStruct(x.shape, jnp.bfloat16),
+        in_specs=[SMEM, VMEM, hbm, hbm, VMEM, VMEM],
+        out_specs=VMEM,
+        scratch_shapes=[
+            pltpu.VMEM((2, pieces, peers, *weights.shape[2:]), jnp.bfloat16),
+            pltpu.SemaphoreType.DMA((2, pieces)),
+        ],
+        compiler_params=pltpu.CompilerParams(vmem_limit_bytes=57 * 2**20),
+        cost_estimate=pl.CostEstimate(
+            flops=4 * x.shape[0] * weights.size, bytes_accessed=4 * weights.size, transcendentals=0
+        ),
+        name="mlp",
+    )(labels, x, weights, others, scales, other_scales)
 
 
 def per_device(
@@ -253,7 +282,6 @@
     heads = lax.all_to_all(heads, "y", 0, 0, tiled=True).reshape(-1, heads.shape[2])
     own = ring_blocks(mlp_shard(w_gate, w_up, w_down))
     mlp_weights = lax.all_gather(own, "y", axis=0)
-    mlp_weights = hold(mlp_weights)
     mlp_others = swap_cores(mlp_weights)
     mlp_scales = jnp.stack([scale_gate, scale_up])
     other_scales = swap_cores(mlp_scales)
@@ -281,14 +309,15 @@
         )
 
     got = swap_cores(sent)
-    mixed = sum_over_chips((kept + got.astype(f32)).astype(bf16))
+    mixed = sum_on_chips((kept + got.astype(f32)).astype(bf16))
     mixed = in_order(mixed) * scale_out
-    hidden = (own_rows.astype(f32) + mixed).astype(bf16)
+    chips = lax.axis_size("x")
+    core_rows = all_rows.reshape(chips, 2, rows, width)
+    core_rows = lax.dynamic_index_in_dim(core_rows, lax.axis_index("core"), 1, keepdims=False)
+    hidden = (core_rows.reshape(-1, width).astype(f32) + mixed).astype(bf16)
     values = hidden.astype(f32)
     mlp_in = (values * inv_rms(values) * mlp_gain).astype(bf16)
-    copies = jnp.broadcast_to(mlp_in[None], (lax.axis_size("x"), rows, width))
-    mlp_in = lax.all_to_all(copies, "x", 0, 0, tiled=True).reshape(-1, width)
-
+    hidden = lax.dynamic_slice_in_dim(hidden, lax.axis_index("x") * rows, rows, 0)
     labels = jnp.stack(ring_labels()).astype(jnp.int32)
     partial = mlp(labels, mlp_in, mlp_weights, mlp_others, mlp_scales, other_scales)
     channel = sum_over_chips(partial) * scale_down

time: 195 us -> 184 us (0.944)
  the two profiles are of different devices: /device:TPU:24 before, /device:TPU:2 now
where the time goes in v6:
time: 184 us; the launch traced here: 183 us
  starting transfers between devices  69.9 us (38%)
  waiting for transfers between devices  55.7 us (30%)
  between operations  14.6 us (8%)
  blocking collectives  13.5 us (7%)
  Pallas kernels  11.1 us (6%)
  local copies, waits for them, and re-layouts  7.22 us (4%)
  matrix products  5.54 us (3%)
  other arithmetic  4.97 us (3%)
    all_to_all x1, waiting for transfers between devices, per_device(): lax.all_to_all(heads, 'y', 0, 0, tiled=True).reshape(-1, heads.shape[2])  20.3 us
    ppermute x1, waiting for transfers between devices, ring_pieces(): even = lax.ppermute(block, RING, pairs(0))  14.4 us
    ppermute x4, starting transfers between devices, swap(): return lax.ppermute(array, 'x', pairs(offset, 4)).astype(jnp.float32)  14.2 us
    all_gather x1, blocking collectives, per_device(): all_rows = lax.all_gather(own_rows, TP, axis=0, tiled=True)  13.5 us
    ppermute x1, starting transfers between devices, ring_blocks(): odd = lax.ppermute(block, RING, pairs(1))  9.13 us
    pallas_call x1, Pallas kernels, mlp(): pl.pallas_call(mlp_kernel, out_shape=jax.ShapeDtypeStruct(x.shape, jnp.bf...  7.14 us
    all_to_all x1, starting transfers between devices, per_device(): lax.all_to_all(heads, 'y', 0, 0, tiled=True).reshape(-1, heads.shape[2])  7.11 us
    ppermute x4, waiting for transfers between devices, swap(): return lax.ppermute(array, 'x', pairs(offset, 4)).astype(jnp.float32)  6.65 us
  transfers between devices with their start and end apart: 18, of which 11 were waited for; matrix products, arithmetic and copies ran while one was open for 6% of the time, Pallas kernels for 2%

profile of v6, /device:TPU:2, one launch (start us, length us, event | category | flops | bytes accessed | tf_op | source)
XLA Modules:
  0.0 182.6 jit_solution(9441672948207196931)
XLA Ops:
  9.2 4.3 %collective-permute-start.9 = (bf16[64,1152]{1,0:T(8,128)(2,1)S(1)}, bf16[64,1152]{1,0:T(8,128)(2,1)S(1)}, u32[]{:S(2)}, u32[]{:S(2)}) collective-permute-start(bf16[64,1152]{1,0:T(8,128)(2,1)S(1)} %shard_map.173), channel_id=1, source_target_pairs={{0,64},{64,0},{128,192},{192,128},{256,320},{320,256},{384,448},{4... | collective-permute-start | bytes 442376 | tf_op jit(solution)/shard_map/ppermute | solution.py:50
  13.5 9.1 %collective-permute-start.10 = (bf16[64,1152]{1,0:T(8,128)(2,1)S(1)}, bf16[64,1152]{1,0:T(8,128)(2,1)S(1)}, u32[]{:S(2)}, u32[]{:S(2)}) collective-permute-start(bf16[64,1152]{1,0:T(8,128)(2,1)S(1)} %shard_map.173), channel_id=1, source_target_pairs={{64,128},{128,64},{192,256},{256,192},{320,384},{384,320},{448,0},... | collective-permute-start | bytes 442376 | tf_op jit(solution)/shard_map/ppermute | solution.py:51
  22.7 1.9 %collective-permute-start.11 = (bf16[32,1152]{1,0:T(8,128)(2,1)S(1)}, bf16[32,1152]{1,0:T(8,128)(2,1)S(1)}, u32[]{:S(2)}, u32[]{:S(2)}) collective-permute-start(bf16[32,1152]{1,0:T(8,128)(2,1)S(1)} %get-tuple-element.20), channel_id=1, source_target_pairs={{0,128},{64,192},{128,256},{192,320},{256,384},{320,448},{384,0},{... | collective-permute-start | bytes 221192 | tf_op jit(solution)/shard_map/ppermute | solution.py:52
  24.6 6.0 %collective-permute-start.12 = (bf16[32,1152]{1,0:T(8,128)(2,1)S(1)}, bf16[32,1152]{1,0:T(8,128)(2,1)S(1)}, u32[]{:S(2)}, u32[]{:S(2)}) collective-permute-start(bf16[32,1152]{1,0:T(8,128)(2,1)S(1)} %get-tuple-element.19), channel_id=1, source_target_pairs={{0,384},{64,448},{128,0},{192,64},{256,128},{320,192},{384,256},{4... | collective-permute-start | bytes 221192 | tf_op jit(solution)/shard_map/ppermute | solution.py:53
  33.5 2.0 %heads_shard.1 = bf16[8,64,1024]{2,1,0:T(8,128)(2,1)} custom-call(f32[64,256]{1,0:T(8,128)} %query.1, f32[64,256]{1,0:T(8,128)} %keyed.1, f32[64,256]{1,0:T(8,128)} %valued.1, f32[64,256]{1,0:T(8,128)} %bitcast.47), custom_call_target="tpu_custom_call" | custom-call | flops 10000000 | bytes 2097152 | tf_op jit(solution)/shard_map/heads_shard/pallas_call | solution.py:139
  35.5 7.1 %all-to-all-start = ((bf16[8,64,1024]{2,1,0:T(8,128)(2,1)}), bf16[8,64,1024]{2,1,0:T(8,128)(2,1)S(1)}, u32[]{:S(2)}, u32[]{:S(2)}) async-start(bf16[8,64,1024]{2,1,0:T(8,128)(2,1)} %heads_shard.1), calls=%async_computation | async-start | bytes 2097152 | tf_op jit(solution)/shard_map/all_to_all | solution.py:282
  43.3 13.5 %all-gather = bf16[1,192,2048]{2,1,0:T(8,128)(2,1)S(1)} all-gather(bf16[1,24,2048]{2,1,0:T(8,128)(2,1)S(1)} %copy-done.12), channel_id=2, replica_groups=mesh['rep'=2,'z'=4,'y'=8,'x'=4,'core'=2] {'x','core'}, dimensions={1}, use_global_device_ids=true | all-gather | bytes 884736 | tf_op jit(solution)/shard_map/all_gather | solution.py:289
  57.9 20.3 %all-to-all-done = bf16[8,64,1024]{2,1,0:T(8,128)(2,1)S(1)} async-done(((bf16[8,64,1024]{2,1,0:T(8,128)(2,1)}), bf16[8,64,1024]{2,1,0:T(8,128)(2,1)S(1)}, u32[]{:S(2)}, u32[]{:S(2)}) %all-to-all-start) | async-done | bytes 1048608 | tf_op jit(solution)/shard_map/all_to_all | solution.py:282
  78.3 3.5 %collective-permute-start = (bf16[512,1024]{1,0:T(8,128)(2,1)S(1)}, bf16[512,1024]{1,0:T(8,128)(2,1)S(1)}, u32[]{:S(2)}, u32[]{:S(2)}) collective-permute-start(bf16[512,1024]{1,0:T(8,128)(2,1)S(1)} %bitcast.31), channel_id=1, source_target_pairs={{0,64},{64,0},{128,192},{192,128},{256,320},{320,256},{384,448},{4... | collective-permute-start | bytes 3145736 | tf_op jit(solution)/shard_map/ppermute | solution.py:30
  81.8 5.0 %collective-permute-start.1 = (bf16[512,1024]{1,0:T(8,128)(2,1)S(1)}, bf16[512,1024]{1,0:T(8,128)(2,1)S(1)}, u32[]{:S(2)}, u32[]{:S(2)}) collective-permute-start(bf16[512,1024]{1,0:T(8,128)(2,1)S(1)} %bitcast.32), channel_id=1, source_target_pairs={{64,128},{128,64},{192,256},{256,192},{320,384},{384,320},{448,0},... | collective-permute-start | bytes 3145736 | tf_op jit(solution)/shard_map/ppermute | solution.py:31
  88.6 14.4 %collective-permute-done.even = bf16[512,1024]{1,0:T(8,128)(2,1)S(1)} collective-permute-done((bf16[512,1024]{1,0:T(8,128)(2,1)S(1)}, bf16[512,1024]{1,0:T(8,128)(2,1)S(1)}, u32[]{:S(2)}, u32[]{:S(2)}) %collective-permute-start) | collective-permute-done | bytes 1048608 | tf_op jit(solution)/shard_map/ppermute | solution.py:30
  103.1 4.1 %collective-permute-start.2 = (bf16[256,1024]{1,0:T(8,128)(2,1)S(1)}, bf16[256,1024]{1,0:T(8,128)(2,1)S(1)}, u32[]{:S(2)}, u32[]{:S(2)}) collective-permute-start(bf16[256,1024]{1,0:T(8,128)(2,1)S(1)} %slice.47), channel_id=1, source_target_pairs={{64,128},{128,64},{192,256},{256,192},{320,384},{384,320},{448,0},... | collective-permute-start | bytes 1572872 | tf_op jit(solution)/shard_map/ppermute | solution.py:32
  109.2 3.4 %collective-permute-start.3 = (bf16[256,1024]{1,0:T(8,128)(2,1)}, bf16[256,1024]{1,0:T(8,128)(2,1)}, u32[]{:S(2)}, u32[]{:S(2)}) collective-permute-start(bf16[256,1024]{1,0:T(8,128)(2,1)} %slice.49), channel_id=1, source_target_pairs={{0,64},{64,0},{128,192},{192,128},{256,320},{320,256},{384,448},{4... | collective-permute-start | bytes 1572872 | tf_op jit(solution)/shard_map/ppermute | solution.py:33
  114.1 4.0 %collective-permute-done.2.far_a = bf16[256,1024]{1,0:T(8,128)(2,1)S(1)} collective-permute-done((bf16[256,1024]{1,0:T(8,128)(2,1)S(1)}, bf16[256,1024]{1,0:T(8,128)(2,1)S(1)}, u32[]{:S(2)}, u32[]{:S(2)}) %collective-permute-start.2) | collective-permute-done | bytes 524320 | tf_op jit(solution)/shard_map/ppermute | solution.py:32
  126.9 2.4 %collective-permute-start.4 = (bf16[96,2048]{1,0:T(8,128)(2,1)S(1)}, bf16[96,2048]{1,0:T(8,128)(2,1)S(1)}, u32[]{:S(2)}, u32[]{:S(2)}) collective-permute-start(bf16[96,2048]{1,0:T(8,128)(2,1)S(1)} %get-tuple-element.8), channel_id=1, source_target_pairs={{0,1},{1,0},{2,3},{3,2},{4,5},{5,4},{6,7},{7,6},{8,9},{9,8},{10,11... | collective-permute-start | bytes 1179656 | tf_op jit(solution)/shard_map/ppermute | solution.py:97
  130.8 2.6 %collective-permute-start.5 = (bf16[48,2048]{1,0:T(8,128)(2,1)S(1)}, bf16[48,2048]{1,0:T(8,128)(2,1)S(1)}, u32[]{:S(2)}, u32[]{:S(2)}) collective-permute-start(bf16[48,2048]{1,0:T(8,128)(2,1)S(1)} %get-tuple-element.18), channel_id=1, source_target_pairs={{0,2},{2,0},{4,6},{6,4},{1,3},{3,1},{5,7},{7,5},{8,10},{10,8},{12,... | collective-permute-start | bytes 589832 | tf_op jit(solution)/shard_map/ppermute | solution.py:85
  133.4 4.1 %collective-permute-start.7 = (bf16[48,2048]{1,0:T(8,128)(2,1)S(1)}, bf16[48,2048]{1,0:T(8,128)(2,1)S(1)}, u32[]{:S(2)}, u32[]{:S(2)}) collective-permute-start(bf16[48,2048]{1,0:T(8,128)(2,1)S(1)} %get-tuple-element.17), channel_id=1, source_target_pairs={{2,4},{4,2},{6,0},{0,6},{3,5},{5,3},{7,1},{1,7},{10,12},{12,10},{1... | collective-permute-start | bytes 589832 | tf_op jit(solution)/shard_map/ppermute | solution.py:85
  140.2 2.5 %collective-permute-done.7 = bf16[48,2048]{1,0:T(8,128)(2,1)S(1)} collective-permute-done((bf16[48,2048]{1,0:T(8,128)(2,1)S(1)}, bf16[48,2048]{1,0:T(8,128)(2,1)S(1)}, u32[]{:S(2)}, u32[]{:S(2)}) %collective-permute-start.7) | collective-permute-done | bytes 196640 | tf_op jit(solution)/shard_map/ppermute | solution.py:85
  142.7 4.2 %collective-permute-start.8 = (bf16[48,2048]{1,0:T(8,128)(2,1)S(1)}, bf16[48,2048]{1,0:T(8,128)(2,1)S(1)}, u32[]{:S(2)}, u32[]{:S(2)}) collective-permute-start(bf16[48,2048]{1,0:T(8,128)(2,1)S(1)} %get-tuple-element.15), channel_id=1, source_target_pairs={{0,2},{2,0},{4,6},{6,4},{1,3},{3,1},{5,7},{7,5},{8,10},{10,8},{12,... | collective-permute-start | bytes 589832 | tf_op jit(solution)/shard_map/ppermute | solution.py:85
  147.0 3.4 %collective-permute-start.6 = (bf16[48,2048]{1,0:T(8,128)(2,1)S(1)}, bf16[48,2048]{1,0:T(8,128)(2,1)S(1)}, u32[]{:S(2)}, u32[]{:S(2)}) collective-permute-start(bf16[48,2048]{1,0:T(8,128)(2,1)S(1)} %get-tuple-element.16), channel_id=1, source_target_pairs={{2,4},{4,2},{6,0},{0,6},{3,5},{5,3},{7,1},{1,7},{10,12},{12,10},{1... | collective-permute-start | bytes 589832 | tf_op jit(solution)/shard_map/ppermute | solution.py:85
  151.3 3.4 %collective-permute-done.6 = bf16[48,2048]{1,0:T(8,128)(2,1)S(1)} collective-permute-done((bf16[48,2048]{1,0:T(8,128)(2,1)S(1)}, bf16[48,2048]{1,0:T(8,128)(2,1)S(1)}, u32[]{:S(2)}, u32[]{:S(2)}) %collective-permute-start.6) | collective-permute-done | bytes 196640 | tf_op jit(solution)/shard_map/ppermute | solution.py:85
  156.9 7.1 %mlp.1 = bf16[96,2048]{1,0:T(8,128)(2,1)} custom-call(s32[4]{0:T(128)} %pad_add_fusion.labels, bf16[96,2048]{1,0:T(8,128)(2,1)} %get-tuple-element.9.x, bf16[8,4,64,1152]{3,2,1,0:T(8,128)(2,1)} %all-gather.3.cloned.1.call-done.weights, bf16[8,4,64,1152]{3,2,1,0:T(8,128)(2,1)} %collective-permute-done.13.others, f32[2,384]{1,0:T(2,128)} %copy-done.14, ...), custom_call_target="tpu_custom_call" | custom-call | flops 905969664 | bytes 9437184 | tf_op jit(solution)/shard_map/mlp/pallas_call | solution.py:239
  164.1 4.9 %all-to-all-start.1 = ((bf16[4,24,2048]{2,1,0:T(8,128)(2,1)}), bf16[4,24,2048]{2,1,0:T(8,128)(2,1)S(1)}, u32[]{:S(2)}, u32[]{:S(2)}) async-start(bf16[4,24,2048]{2,1,0:T(8,128)(2,1)} %bitcast.45), calls=%async_computation.1 | async-start | bytes 786432 | tf_op jit(solution)/shard_map/all_to_all | solution.py:77
  169.0 5.9 %all-to-all-done.1 = bf16[4,24,2048]{2,1,0:T(8,128)(2,1)S(1)} async-done(((bf16[4,24,2048]{2,1,0:T(8,128)(2,1)}), bf16[4,24,2048]{2,1,0:T(8,128)(2,1)S(1)}, u32[]{:S(2)}, u32[]{:S(2)}) %all-to-all-start.1) | async-done | bytes 393248 | tf_op jit(solution)/shard_map/all_to_all | solution.py:77
  (95 shorter events, 28.6 us)
Async XLA Ops:
  6.5 113.5 %all-gather.3.cloned.1.call-start = ((), (), s32[]{:S(2)}) async-start(), calls=%async_computation.2 | async-start | bytes 5308416 | tf_op jit(solution)/shard_map/all_gather | solution.py:284
  9.2 21.4 %collective-permute-start.9 = (bf16[64,1152]{1,0:T(8,128)(2,1)S(1)}, bf16[64,1152]{1,0:T(8,128)(2,1)S(1)}, u32[]{:S(2)}, u32[]{:S(2)}) collective-permute-start(bf16[64,1152]{1,0:T(8,128)(2,1)S(1)} %shard_map.173), channel_id=1, source_target_pairs={{0,64},{64,0},{128,192},{192,128},{256,320},{320,256},{384,448},{4... | collective-permute-start | bytes 442376 | tf_op jit(solution)/shard_map/ppermute | solution.py:50
  13.5 17.2 %collective-permute-start.10 = (bf16[64,1152]{1,0:T(8,128)(2,1)S(1)}, bf16[64,1152]{1,0:T(8,128)(2,1)S(1)}, u32[]{:S(2)}, u32[]{:S(2)}) collective-permute-start(bf16[64,1152]{1,0:T(8,128)(2,1)S(1)} %shard_map.173), channel_id=1, source_target_pairs={{64,128},{128,64},{192,256},{256,192},{320,384},{384,320},{448,0},... | collective-permute-start | bytes 442376 | tf_op jit(solution)/shard_map/ppermute | solution.py:51
  22.7 9.1 %collective-permute-start.11 = (bf16[32,1152]{1,0:T(8,128)(2,1)S(1)}, bf16[32,1152]{1,0:T(8,128)(2,1)S(1)}, u32[]{:S(2)}, u32[]{:S(2)}) collective-permute-start(bf16[32,1152]{1,0:T(8,128)(2,1)S(1)} %get-tuple-element.20), channel_id=1, source_target_pairs={{0,128},{64,192},{128,256},{192,320},{256,384},{320,448},{384,0},{... | collective-permute-start | bytes 221192 | tf_op jit(solution)/shard_map/ppermute | solution.py:52
  24.6 8.0 %collective-permute-start.12 = (bf16[32,1152]{1,0:T(8,128)(2,1)S(1)}, bf16[32,1152]{1,0:T(8,128)(2,1)S(1)}, u32[]{:S(2)}, u32[]{:S(2)}) collective-permute-start(bf16[32,1152]{1,0:T(8,128)(2,1)S(1)} %get-tuple-element.19), channel_id=1, source_target_pairs={{0,384},{64,448},{128,0},{192,64},{256,128},{320,192},{384,256},{4... | collective-permute-start | bytes 221192 | tf_op jit(solution)/shard_map/ppermute | solution.py:53
  33.5 9.9 %copy-start.12 = (bf16[1,24,2048]{2,1,0:T(8,128)(2,1)S(1)}, bf16[1,24,2048]{2,1,0:T(8,128)(2,1)}, u32[]{:S(2)}) copy-start(bf16[1,24,2048]{2,1,0:T(8,128)(2,1)} %param.18) | copy-start | bytes 294916
  35.5 51.7 %copy-start.15 = (f32[2048]{0:T(1024)S(1)}, f32[2048]{0:T(1024)}, u32[]{:S(2)}) copy-start(f32[2048]{0:T(1024)} %param.19) | copy-start | bytes 24580
  35.5 42.7 %all-to-all-start = ((bf16[8,64,1024]{2,1,0:T(8,128)(2,1)}), bf16[8,64,1024]{2,1,0:T(8,128)(2,1)S(1)}, u32[]{:S(2)}, u32[]{:S(2)}) async-start(bf16[8,64,1024]{2,1,0:T(8,128)(2,1)} %heads_shard.1), calls=%async_computation | async-start | bytes 2097152 | tf_op jit(solution)/shard_map/all_to_all | solution.py:282
  78.3 24.8 %collective-permute-start = (bf16[512,1024]{1,0:T(8,128)(2,1)S(1)}, bf16[512,1024]{1,0:T(8,128)(2,1)S(1)}, u32[]{:S(2)}, u32[]{:S(2)}) collective-permute-start(bf16[512,1024]{1,0:T(8,128)(2,1)S(1)} %bitcast.31), channel_id=1, source_target_pairs={{0,64},{64,0},{128,192},{192,128},{256,320},{320,256},{384,448},{4... | collective-permute-start | bytes 3145736 | tf_op jit(solution)/shard_map/ppermute | solution.py:30
  81.8 26.6 %collective-permute-start.1 = (bf16[512,1024]{1,0:T(8,128)(2,1)S(1)}, bf16[512,1024]{1,0:T(8,128)(2,1)S(1)}, u32[]{:S(2)}, u32[]{:S(2)}) collective-permute-start(bf16[512,1024]{1,0:T(8,128)(2,1)S(1)} %bitcast.32), channel_id=1, source_target_pairs={{64,128},{128,64},{192,256},{256,192},{320,384},{384,320},{448,0},... | collective-permute-start | bytes 3145736 | tf_op jit(solution)/shard_map/ppermute | solution.py:31
  88.6 29.5 %copy-start.10 = (bf16[192,2048]{1,0:T(8,128)(2,1)}, bf16[192,2048]{1,0:T(8,128)(2,1)S(1)}, u32[]{:S(2)}) copy-start(bf16[192,2048]{1,0:T(8,128)(2,1)S(1)} %fusion.2) | copy-start | bytes 2359300
  103.1 15.1 %collective-permute-start.2 = (bf16[256,1024]{1,0:T(8,128)(2,1)S(1)}, bf16[256,1024]{1,0:T(8,128)(2,1)S(1)}, u32[]{:S(2)}, u32[]{:S(2)}) collective-permute-start(bf16[256,1024]{1,0:T(8,128)(2,1)S(1)} %slice.47), channel_id=1, source_target_pairs={{64,128},{128,64},{192,256},{256,192},{320,384},{384,320},{448,0},... | collective-permute-start | bytes 1572872 | tf_op jit(solution)/shard_map/ppermute | solution.py:32
  109.2 12.7 %collective-permute-start.3 = (bf16[256,1024]{1,0:T(8,128)(2,1)}, bf16[256,1024]{1,0:T(8,128)(2,1)}, u32[]{:S(2)}, u32[]{:S(2)}) collective-permute-start(bf16[256,1024]{1,0:T(8,128)(2,1)} %slice.49), channel_id=1, source_target_pairs={{0,64},{64,0},{128,192},{192,128},{256,320},{320,256},{384,448},{4... | collective-permute-start | bytes 1572872 | tf_op jit(solution)/shard_map/ppermute | solution.py:33
  120.0 36.3 %collective-permute-start.13 = (bf16[8,4,64,1152]{3,2,1,0:T(8,128)(2,1)}, bf16[8,4,64,1152]{3,2,1,0:T(8,128)(2,1)}, u32[]{:S(2)}, u32[]{:S(2)}) collective-permute-start(bf16[8,4,64,1152]{3,2,1,0:T(8,128)(2,1)} %all-gather.3.cloned.1.call-done.weights), channel_id=1, source_target_pairs={{0,1},{1,0},{2,3},{3,2},{4,5},{5,4},{6,7},{7,6},{8,9},{9,8},{10,11... | collective-permute-start | bytes 14155784 | tf_op jit(solution)/shard_map/ppermute | solution.py:97
  126.9 3.7 %collective-permute-start.4 = (bf16[96,2048]{1,0:T(8,128)(2,1)S(1)}, bf16[96,2048]{1,0:T(8,128)(2,1)S(1)}, u32[]{:S(2)}, u32[]{:S(2)}) collective-permute-start(bf16[96,2048]{1,0:T(8,128)(2,1)S(1)} %get-tuple-element.8), channel_id=1, source_target_pairs={{0,1},{1,0},{2,3},{3,2},{4,5},{5,4},{6,7},{7,6},{8,9},{9,8},{10,11... | collective-permute-start | bytes 1179656 | tf_op jit(solution)/shard_map/ppermute | solution.py:97
  130.7 16.2 %copy-start.9 = (bf16[1,192,2048]{2,1,0:T(8,128)(2,1)S(1)}, bf16[1,192,2048]{2,1,0:T(8,128)(2,1)}, u32[]{:S(2)}) copy-start(bf16[1,192,2048]{2,1,0:T(8,128)(2,1)} %copy-done.8) | copy-start | bytes 2359300
  130.8 9.4 %collective-permute-start.5 = (bf16[48,2048]{1,0:T(8,128)(2,1)S(1)}, bf16[48,2048]{1,0:T(8,128)(2,1)S(1)}, u32[]{:S(2)}, u32[]{:S(2)}) collective-permute-start(bf16[48,2048]{1,0:T(8,128)(2,1)S(1)} %get-tuple-element.18), channel_id=1, source_target_pairs={{0,2},{2,0},{4,6},{6,4},{1,3},{3,1},{5,7},{7,5},{8,10},{10,8},{12,... | collective-permute-start | bytes 589832 | tf_op jit(solution)/shard_map/ppermute | solution.py:85
  133.4 9.3 %collective-permute-start.7 = (bf16[48,2048]{1,0:T(8,128)(2,1)S(1)}, bf16[48,2048]{1,0:T(8,128)(2,1)S(1)}, u32[]{:S(2)}, u32[]{:S(2)}) collective-permute-start(bf16[48,2048]{1,0:T(8,128)(2,1)S(1)} %get-tuple-element.17), channel_id=1, source_target_pairs={{2,4},{4,2},{6,0},{0,6},{3,5},{5,3},{7,1},{1,7},{10,12},{12,10},{1... | collective-permute-start | bytes 589832 | tf_op jit(solution)/shard_map/ppermute | solution.py:85
  137.5 13.8 %copy-start.14 = (f32[2,384]{1,0:T(2,128)}, f32[2,384]{1,0:T(2,128)S(1)}, u32[]{:S(2)}) copy-start(f32[2,384]{1,0:T(2,128)S(1)} %pad_maximum_fusion.scales) | copy-start | bytes 9220
  137.5 18.8 %collective-permute-start.14 = (f32[2,384]{1,0:T(2,128)S(1)}, f32[2,384]{1,0:T(2,128)S(1)}, u32[]{:S(2)}, u32[]{:S(2)}) collective-permute-start(f32[2,384]{1,0:T(2,128)S(1)} %pad_maximum_fusion.scales), channel_id=1, source_target_pairs={{0,1},{1,0},{2,3},{3,2},{4,5},{5,4},{6,7},{7,6},{8,9},{9,8},{10,11... | collective-permute-start | bytes 9224 | tf_op jit(solution)/shard_map/ppermute | solution.py:97
  142.7 8.5 %collective-permute-start.8 = (bf16[48,2048]{1,0:T(8,128)(2,1)S(1)}, bf16[48,2048]{1,0:T(8,128)(2,1)S(1)}, u32[]{:S(2)}, u32[]{:S(2)}) collective-permute-start(bf16[48,2048]{1,0:T(8,128)(2,1)S(1)} %get-tuple-element.15), channel_id=1, source_target_pairs={{0,2},{2,0},{4,6},{6,4},{1,3},{3,1},{5,7},{7,5},{8,10},{10,8},{12,... | collective-permute-start | bytes 589832 | tf_op jit(solution)/shard_map/ppermute | solution.py:85
  147.0 7.7 %collective-permute-start.6 = (bf16[48,2048]{1,0:T(8,128)(2,1)S(1)}, bf16[48,2048]{1,0:T(8,128)(2,1)S(1)}, u32[]{:S(2)}, u32[]{:S(2)}) collective-permute-start(bf16[48,2048]{1,0:T(8,128)(2,1)S(1)} %get-tuple-element.16), channel_id=1, source_target_pairs={{2,4},{4,2},{6,0},{0,6},{3,5},{5,3},{7,1},{1,7},{10,12},{12,10},{1... | collective-permute-start | bytes 589832 | tf_op jit(solution)/shard_map/ppermute | solution.py:85
  156.9 18.1 %copy-start.17 = (f32[2048]{0:T(1024)S(1)}, f32[2048]{0:T(1024)}, u32[]{:S(2)}) copy-start(f32[2048]{0:T(1024)} %param.35) | copy-start | bytes 24580
  164.1 10.9 %all-to-all-start.1 = ((bf16[4,24,2048]{2,1,0:T(8,128)(2,1)}), bf16[4,24,2048]{2,1,0:T(8,128)(2,1)S(1)}, u32[]{:S(2)}, u32[]{:S(2)}) async-start(bf16[4,24,2048]{2,1,0:T(8,128)(2,1)} %bitcast.45), calls=%async_computation.1 | async-start | bytes 786432 | tf_op jit(solution)/shard_map/all_to_all | solution.py:77
  (15 other events, 29.9 us)
Sparse Core Ops, SparseCore 0:
  33.6 78.2 all-gather.2

commit v7 on v4

--- a/solution.py
+++ b/solution.py
@@ -45,13 +45,6 @@
     return [jnp.where(z == j, 0, jnp.where(even == j, 1, jnp.where(odd == j, 2, 3))) for j in range(4)]
 
 
-def ring_blocks(block):
-    even = lax.ppermute(block, RING, pairs(0))
-    odd = lax.ppermute(block, RING, pairs(1))
-    far = lax.ppermute(block, RING, [(i, (i + 2) % 8) for i in range(8)])
-    return jnp.stack([block, even, odd, far])
-
-
 def ring_dot(x, pieces, columns):
     size = pieces[0].shape[0]
     half = size // 2
@@ -62,7 +55,8 @@
         cut = lax.dynamic_slice_in_dim(x, start, piece.shape[0], 1)
         return jnp.dot(cut, piece[:, :columns], preferred_element_type=jnp.float32)
 
-    return sum(term(start, piece) for start, piece in zip(starts, pieces))
+    total = sum(term(start, piece) for start, piece in zip(starts[:3], pieces[:3]))
+    return total + term(starts[3], pieces[3]) + term(starts[4], pieces[4])
 
 
 def dot_t(a, b):
@@ -134,15 +128,16 @@
 
 def mlp_shard_kernel(gate, up, down, out):
     units = gate.shape[1]
-    out[:, :units] = gate[...].astype(jnp.bfloat16)
-    out[:, units : 2 * units] = up[...].astype(jnp.bfloat16)
-    out[:, 2 * units :] = down[...].astype(jnp.bfloat16)
-
-
-def mlp_shard(w_gate, w_up, w_down):
+    for i, ref in enumerate((gate, up, down)):
+        part = ref[...].astype(jnp.bfloat16)
+        for peer in range(out.shape[0]):
+            out[peer, :, i * units : (i + 1) * units] = part
+
+
+def mlp_shard(w_gate, w_up, w_down, peers):
     rows, units = w_gate.shape
-    shape = jax.ShapeDtypeStruct((rows, 3 * units), jnp.bfloat16)
-    return local_call(mlp_shard_kernel, shape, [VMEM] * 3, 10**7, 2**20)(w_gate, w_up, w_down.T)
+    shape = jax.ShapeDtypeStruct((peers, rows, 3 * units), jnp.bfloat16)
+    return local_call(mlp_shard_kernel, shape, [VMEM] * 3, 10**7, 2**21)(w_gate, w_up, w_down.T)
 
 
 def retain_kernel(rate, core, product, cosine, sine, sq, sk, sv, own, even, odd, far_a, far_b, kept, sent):
@@ -187,41 +182,58 @@
     )
 
 
-def hold_kernel(weights, out):
-    out[...] = weights[...]
-
-
-def hold(weights):
-    shape = jax.ShapeDtypeStruct(weights.shape, weights.dtype)
-    return local_call(hold_kernel, shape, [VMEM], 10**7, 4 * weights.size)(weights)
-
-
-def mlp_kernel(labels, x, weights, others, scales, other_scales, out):
+def near_kernel(places, x, own, even, odd, out):
+    size = own.shape[0]
+    wide = out.shape[1]
+    total = 0.0
+    for i, piece in enumerate((own, even, odd)):
+        at = pl.ds(pl.multiple_of(places[i] * size, size), size)
+        total += jnp.dot(x[:, at], piece[:, :wide], preferred_element_type=jnp.float32)
+    out[...] = total
+
+
+def near(places, x, pieces, wide):
+    shape = jax.ShapeDtypeStruct((x.shape[0], wide), jnp.float32)
+    specs = [SMEM] + [VMEM] * 4
+    return local_call(near_kernel, shape, specs, 4 * 10**8, 2**22)(places, x, *pieces)
+
+
+def mlp_kernel(places, core, x, both, scales, own, even, odd, far_a, far_b, kept, sent, inner):
     units = scales.shape[1]
-    size = x.shape[1] // 4
-    places = [pl.ds(pl.multiple_of(labels[p] * size, size), size) for p in range(4)]
-    inner = []
-    for held, scale in ((weights, scales), (others, other_scales)):
-        both = jnp.zeros((x.shape[0], 2 * units), jnp.float32)
-        for p, at in enumerate(places):
-            piece = held[:, p, :, : 2 * units].reshape(size, 2 * units)
-            both += jnp.dot(x[:, at], piece, preferred_element_type=jnp.float32)
-        gate = both[:, :units] * scale[0:1]
-        up = both[:, units:] * scale[1:2]
-        inner.append((gate / (1.0 + jnp.exp(-gate)) * up).astype(jnp.bfloat16))
-    for p, at in enumerate(places):
-        total = 0.0
-        for held, part in zip((weights, others), inner):
-            total += dot_t(part, held[:, p, :, 2 * units :].reshape(size, units))
-        out[:, at] = total.astype(jnp.bfloat16)
-
-
-def mlp(labels, x, weights, others, scales, other_scales):
-    shape = jax.ShapeDtypeStruct(x.shape, jnp.bfloat16)
-    flops = 4 * x.shape[0] * x.shape[1] * weights.shape[-1]
-    return local_call(mlp_kernel, shape, [SMEM] + [VMEM] * 5, flops, 4 * weights.size)(
-        labels, x, weights, others, scales, other_scales
-    )
+    size = own.shape[0]
+    half = size // 2
+    far = pl.multiple_of(places[3] * size, size)
+    total = both[...]
+    for i, piece in enumerate((far_a, far_b)):
+        at = pl.ds(far + i * half, half)
+        total += jnp.dot(x[:, at], piece[:, : 2 * units], preferred_element_type=jnp.float32)
+    gate = total[:, :units] * scales[0:1]
+    up = total[:, units:] * scales[1:2]
+    inner[...] = (gate / (1.0 + jnp.exp(-gate)) * up).astype(jnp.bfloat16)
+    rows = x.shape[0] // 2
+    mine = inner[pl.ds(pl.multiple_of(core[0] * rows, rows), rows), :]
+    other = inner[pl.ds(pl.multiple_of((1 - core[0]) * rows, rows), rows), :]
+    attended = jnp.concatenate([mine, other], axis=0)
+    starts = [pl.multiple_of(places[i] * size, size) for i in range(3)] + [far, far + half]
+    for start, piece in zip(starts, (own, even, odd, far_a, far_b)):
+        term = dot_t(attended, piece[:, 2 * units :])
+        at = pl.ds(start, piece.shape[0])
+        kept[:, at] = term[:rows]
+        sent[:, at] = term[rows:].astype(jnp.bfloat16)
+
+
+def mlp(places, core, x, both, scales, pieces):
+    half = (x.shape[0] // 2, x.shape[1])
+    return pl.pallas_call(
+        mlp_kernel,
+        out_shape=[jax.ShapeDtypeStruct(half, kind) for kind in (jnp.float32, jnp.bfloat16)],
+        in_specs=[SMEM] * 2 + [VMEM] * 8,
+        out_specs=[VMEM] * 2,
+        scratch_shapes=[pltpu.VMEM((x.shape[0], scales.shape[1]), jnp.bfloat16)],
+        compiler_params=pltpu.CompilerParams(vmem_limit_bytes=24 * 2**20),
+        cost_estimate=pl.CostEstimate(flops=5 * 10**8, bytes_accessed=2**23, transcendentals=0),
+        name="mlp",
+    )(places, core, x, both, scales, *pieces)
 
 
 def per_device(
@@ -251,13 +263,10 @@
     peers = lax.axis_size("y")
     heads = heads_shard(w_query, w_key, w_value, w_out, peers)
     heads = lax.all_to_all(heads, "y", 0, 0, tiled=True).reshape(-1, heads.shape[2])
-    own = ring_blocks(mlp_shard(w_gate, w_up, w_down))
-    mlp_weights = lax.all_gather(own, "y", axis=0)
-    mlp_weights = hold(mlp_weights)
-    mlp_others = swap_cores(mlp_weights)
-    mlp_scales = jnp.stack([scale_gate, scale_up])
-    other_scales = swap_cores(mlp_scales)
+    weights = mlp_shard(w_gate, w_up, w_down, peers)
+    weights = lax.all_to_all(weights, "y", 0, 0, tiled=True).reshape(-1, weights.shape[2])
     heads = ring_pieces(heads)
+    weights = ring_pieces(weights)
     all_rows = lax.all_gather(own_rows, TP, axis=0, tiled=True)
 
     values = all_rows.astype(f32)
@@ -288,10 +297,14 @@
     mlp_in = (values * inv_rms(values) * mlp_gain).astype(bf16)
     copies = jnp.broadcast_to(mlp_in[None], (lax.axis_size("x"), rows, width))
     mlp_in = lax.all_to_all(copies, "x", 0, 0, tiled=True).reshape(-1, width)
-
-    labels = jnp.stack(ring_labels()).astype(jnp.int32)
-    partial = mlp(labels, mlp_in, mlp_weights, mlp_others, mlp_scales, other_scales)
-    channel = sum_over_chips(partial) * scale_down
+    mlp_in = lax.all_gather(mlp_in, "core", axis=0, tiled=True)
+
+    places = jnp.stack(ring_labels()).astype(jnp.int32)
+    scales = jnp.stack([scale_gate, scale_up])
+    both = near(places, mlp_in, weights[:3], 2 * w_gate.shape[1])
+    kept, sent = mlp(places, core, mlp_in, both, scales, weights)
+    got = swap_cores(sent)
+    channel = sum_over_chips((kept + got.astype(f32)).astype(bf16)) * scale_down
     return (hidden.astype(f32) + channel).astype(bf16)[None]
 
 

time: 195 us -> 183 us (0.938)
  the two profiles are of different devices: /device:TPU:24 before, /device:TPU:8 now
where the time goes in v7:
time: 183 us; the launch traced here: 182 us
  waiting for transfers between devices  71.3 us (39%)
  starting transfers between devices  56.9 us (31%)
  blocking collectives  27.1 us (15%)
  Pallas kernels  9.54 us (5%)
  local copies, waits for them, and re-layouts  6.35 us (3%)
  matrix products  5.67 us (3%)
  other arithmetic  4.14 us (2%)
    ppermute x2, waiting for transfers between devices, ring_pieces(): odd = lax.ppermute(block, RING, pairs(1))  31.2 us
    all_to_all x1, waiting for transfers between devices, per_device(): lax.all_to_all(heads, 'y', 0, 0, tiled=True).reshape(-1, heads.shape[2])  24.4 us
    ppermute x2, starting transfers between devices, ring_pieces(): odd = lax.ppermute(block, RING, pairs(1))  13.8 us
    all_gather x1, blocking collectives, per_device(): all_rows = lax.all_gather(own_rows, TP, axis=0, tiled=True)  13.7 us
    all_to_all x1, blocking collectives, sum_over_chips(): lax.all_to_all(blocks, 'x', 0, 0, tiled=True).astype(jnp.float32)  11.1 us
    all_to_all x1, starting transfers between devices, per_device(): lax.all_to_all(heads, 'y', 0, 0, tiled=True).reshape(-1, heads.shape[2])  9.4 us
    ppermute x2, starting transfers between devices, ring_pieces(): far_a = lax.ppermute(even[:half], RING, pairs(1))  8.88 us
    all_to_all x1, waiting for transfers between devices, per_device(): mlp_in = lax.all_to_all(copies, 'x', 0, 0, tiled=True).reshape(-1, width)  7.27 us
  transfers between devices with their start and end apart: 14, of which 9 were waited for; matrix products, arithmetic and copies ran while one was open for 8% of the time, Pallas kernels for 3%

profile of v7, /device:TPU:8, one launch (start us, length us, event | category | flops | bytes accessed | tf_op | source)
XLA Modules:
  0.0 182.1 jit_solution(11159633239224750776)
XLA Ops:
  0.0 2.0 %heads_shard.1 = bf16[8,64,1024]{2,1,0:T(8,128)(2,1)} custom-call(f32[64,256]{1,0:T(8,128)} %query.1, f32[64,256]{1,0:T(8,128)} %keyed.1, f32[64,256]{1,0:T(8,128)} %valued.1, f32[64,256]{1,0:T(8,128)} %bitcast.55), custom_call_target="tpu_custom_call" | custom-call | flops 10000000 | bytes 2097152 | tf_op jit(solution)/shard_map/heads_shard/pallas_call | solution.py:114
  2.0 9.4 %all-to-all-start = ((bf16[8,64,1024]{2,1,0:T(8,128)(2,1)}), bf16[8,64,1024]{2,1,0:T(8,128)(2,1)S(1)}, u32[]{:S(2)}, u32[]{:S(2)}) async-start(bf16[8,64,1024]{2,1,0:T(8,128)(2,1)} %heads_shard.1), calls=%async_computation | async-start | bytes 2097152 | tf_op jit(solution)/shard_map/all_to_all | solution.py:265
  12.6 24.4 %all-to-all-done = bf16[8,64,1024]{2,1,0:T(8,128)(2,1)S(1)} async-done(((bf16[8,64,1024]{2,1,0:T(8,128)(2,1)}), bf16[8,64,1024]{2,1,0:T(8,128)(2,1)S(1)}, u32[]{:S(2)}, u32[]{:S(2)}) %all-to-all-start) | async-done | bytes 1048608 | tf_op jit(solution)/shard_map/all_to_all | solution.py:265
  37.0 4.9 %all-to-all-start.3 = ((bf16[8,64,1152]{2,1,0:T(8,128)(2,1)}), bf16[8,64,1152]{2,1,0:T(8,128)(2,1)S(1)}, u32[]{:S(2)}, u32[]{:S(2)}) async-start(bf16[8,64,1152]{2,1,0:T(8,128)(2,1)} %shard_map.173), calls=%async_computation.3 | async-start | bytes 2359296 | tf_op jit(solution)/shard_map/all_to_all | solution.py:267
  42.6 13.7 %all-gather = bf16[1,192,2048]{2,1,0:T(8,128)(2,1)S(1)} all-gather(bf16[1,24,2048]{2,1,0:T(8,128)(2,1)S(1)} %copy-done.13), channel_id=2, replica_groups=mesh['rep'=2,'z'=4,'y'=8,'x'=4,'core'=2] {'x','core'}, dimensions={1}, use_global_device_ids=true | all-gather | bytes 884736 | tf_op jit(solution)/shard_map/all_gather | solution.py:270
  56.6 10.9 %collective-permute-start.1 = (bf16[512,1024]{1,0:T(8,128)(2,1)S(1)}, bf16[512,1024]{1,0:T(8,128)(2,1)S(1)}, u32[]{:S(2)}, u32[]{:S(2)}) collective-permute-start(bf16[512,1024]{1,0:T(8,128)(2,1)S(1)} %bitcast.41), channel_id=1, source_target_pairs={{64,128},{128,64},{192,256},{256,192},{320,384},{384,320},{448,0},... | collective-permute-start | bytes 3145736 | tf_op jit(solution)/shard_map/ppermute | solution.py:31
  67.5 1.9 %collective-permute-start = (bf16[512,1024]{1,0:T(8,128)(2,1)S(1)}, bf16[512,1024]{1,0:T(8,128)(2,1)S(1)}, u32[]{:S(2)}, u32[]{:S(2)}) collective-permute-start(bf16[512,1024]{1,0:T(8,128)(2,1)S(1)} %bitcast.42), channel_id=1, source_target_pairs={{0,64},{64,0},{128,192},{192,128},{256,320},{320,256},{384,448},{4... | collective-permute-start | bytes 3145736 | tf_op jit(solution)/shard_map/ppermute | solution.py:30
  70.8 20.4 %collective-permute-done.1.odd = bf16[512,1024]{1,0:T(8,128)(2,1)S(1)} collective-permute-done((bf16[512,1024]{1,0:T(8,128)(2,1)S(1)}, bf16[512,1024]{1,0:T(8,128)(2,1)S(1)}, u32[]{:S(2)}, u32[]{:S(2)}) %collective-permute-start.1) | collective-permute-done | bytes 1048608 | tf_op jit(solution)/shard_map/ppermute | solution.py:31
  95.4 4.3 %collective-permute-start.2 = (bf16[256,1024]{1,0:T(8,128)(2,1)}, bf16[256,1024]{1,0:T(8,128)(2,1)}, u32[]{:S(2)}, u32[]{:S(2)}) collective-permute-start(bf16[256,1024]{1,0:T(8,128)(2,1)} %slice.39), channel_id=1, source_target_pairs={{64,128},{128,64},{192,256},{256,192},{320,384},{384,320},{448,0},... | collective-permute-start | bytes 1572872 | tf_op jit(solution)/shard_map/ppermute | solution.py:32
  101.0 2.9 %collective-permute-start.6 = (bf16[512,1152]{1,0:T(8,128)(2,1)S(1)}, bf16[512,1152]{1,0:T(8,128)(2,1)S(1)}, u32[]{:S(2)}, u32[]{:S(2)}) collective-permute-start(bf16[512,1152]{1,0:T(8,128)(2,1)S(1)} %bitcast.37), channel_id=1, source_target_pairs={{64,128},{128,64},{192,256},{256,192},{320,384},{384,320},{448,0},... | collective-permute-start | bytes 3538952 | tf_op jit(solution)/shard_map/ppermute | solution.py:31
  103.8 2.2 %collective-permute-start.5 = (bf16[512,1152]{1,0:T(8,128)(2,1)S(1)}, bf16[512,1152]{1,0:T(8,128)(2,1)}, u32[]{:S(2)}, u32[]{:S(2)}) collective-permute-start(bf16[512,1152]{1,0:T(8,128)(2,1)S(1)} %bitcast.38), channel_id=1, source_target_pairs={{0,64},{64,0},{128,192},{192,128},{256,320},{320,256},{384,448},{4... | collective-permute-start | bytes 3538952 | tf_op jit(solution)/shard_map/ppermute | solution.py:30
  109.9 3.8 %collective-permute-done.2.far_a = bf16[256,1024]{1,0:T(8,128)(2,1)} collective-permute-done((bf16[256,1024]{1,0:T(8,128)(2,1)}, bf16[256,1024]{1,0:T(8,128)(2,1)}, u32[]{:S(2)}, u32[]{:S(2)}) %collective-permute-start.2) | collective-permute-done | bytes 524320 | tf_op jit(solution)/shard_map/ppermute | solution.py:32
  116.1 2.0 %shard_map.172 = (f32[96,2048]{1,0:T(8,128)S(1)}, bf16[96,2048]{1,0:T(8,128)(2,1)S(1)}) custom-call(f32[1]{0:T(128)S(6)} %copy.19.rate, s32[1]{0:T(128)} %bitcast.core, f32[192,768]{1,0:T(8,128)S(1)} %fusion.4.product, f32[192,128]{1,0:T(8,128)S(1)} %copy-done.4, f32[192,128]{1,0:T(8,128)S(1)} %get-tuple-element.19.sine, f32[1,256]{1,0:T(1,128)S(1)} %bitcast.46, ...), custom_call_target="tpu_custom_call" | custom-call | flops 300000000 | bytes 2097152 | tf_op jit(solution)/shard_map/pallas_call | solution.py:180
  122.6 3.7 %all-to-all-start.1 = ((bf16[4,24,2048]{2,1,0:T(8,128)(2,1)}), bf16[4,24,2048]{2,1,0:T(8,128)(2,1)S(1)}, u32[]{:S(2)}, u32[]{:S(2)}) async-start(bf16[4,24,2048]{2,1,0:T(8,128)(2,1)} %bitcast.8), calls=%async_computation.1 | async-start | bytes 786432 | tf_op jit(solution)/shard_map/all_to_all | solution.py:68
  126.3 10.8 %collective-permute-done.6.odd = bf16[512,1152]{1,0:T(8,128)(2,1)S(1)} collective-permute-done((bf16[512,1152]{1,0:T(8,128)(2,1)S(1)}, bf16[512,1152]{1,0:T(8,128)(2,1)S(1)}, u32[]{:S(2)}, u32[]{:S(2)}) %collective-permute-start.6) | collective-permute-done | bytes 1179680 | tf_op jit(solution)/shard_map/ppermute | solution.py:31
  138.0 2.6 %collective-permute-start.8 = (bf16[256,1152]{1,0:T(8,128)(2,1)}, bf16[256,1152]{1,0:T(8,128)(2,1)S(1)}, u32[]{:S(2)}, u32[]{:S(2)}) collective-permute-start(bf16[256,1152]{1,0:T(8,128)(2,1)} %slice.44), channel_id=1, source_target_pairs={{0,64},{64,0},{128,192},{192,128},{256,320},{320,256},{384,448},{4... | collective-permute-start | bytes 1769480 | tf_op jit(solution)/shard_map/ppermute | solution.py:33
  140.5 1.9 %slice.43 = bf16[256,1152]{1,0:T(8,128)(2,1)} slice(bf16[512,1152]{1,0:T(8,128)(2,1)} %collective-permute-done.5.even), slice={[0:256], [0:1152]} | slice | bytes 1179648 | tf_op jit(solution)/shard_map/slice | solution.py:32
  142.5 4.6 %collective-permute-start.7 = (bf16[256,1152]{1,0:T(8,128)(2,1)}, bf16[256,1152]{1,0:T(8,128)(2,1)}, u32[]{:S(2)}, u32[]{:S(2)}) collective-permute-start(bf16[256,1152]{1,0:T(8,128)(2,1)} %slice.43), channel_id=1, source_target_pairs={{64,128},{128,64},{192,256},{256,192},{320,384},{384,320},{448,0},... | collective-permute-start | bytes 1769480 | tf_op jit(solution)/shard_map/ppermute | solution.py:32
  148.8 3.7 %all-to-all-start.2 = ((bf16[4,24,2048]{2,1,0:T(8,128)(2,1)}), bf16[4,24,2048]{2,1,0:T(8,128)(2,1)S(1)}, u32[]{:S(2)}, u32[]{:S(2)}) async-start(bf16[4,24,2048]{2,1,0:T(8,128)(2,1)} %broadcast_in_dim.34), calls=%async_computation.2 | async-start | bytes 786432 | tf_op jit(solution)/shard_map/all_to_all | solution.py:299
  152.6 7.3 %all-to-all-done.2 = bf16[4,24,2048]{2,1,0:T(8,128)(2,1)S(1)} async-done(((bf16[4,24,2048]{2,1,0:T(8,128)(2,1)}), bf16[4,24,2048]{2,1,0:T(8,128)(2,1)S(1)}, u32[]{:S(2)}, u32[]{:S(2)}) %all-to-all-start.2) | async-done | bytes 393248 | tf_op jit(solution)/shard_map/all_to_all | solution.py:299
  159.9 2.4 %all_gather.7.x = bf16[192,2048]{1,0:T(8,128)(2,1)S(1)} all-gather(bf16[96,2048]{1,0:T(8,128)(2,1)S(1)} %bitcast.49), channel_id=1, replica_groups=mesh['rep'=2,'z'=4,'y'=8,'x'=4,'core'=2] {'core'}, dimensions={0}, use_global_device_ids=true | all-gather | bytes 1179648 | tf_op jit(solution)/shard_map/all_gather | solution.py:300
  164.2 2.4 %mlp.1 = (f32[96,2048]{1,0:T(8,128)S(1)}, bf16[96,2048]{1,0:T(8,128)(2,1)S(1)}) custom-call(s32[4]{0:T(128)S(1)} %pad_add_fusion.places, s32[1]{0:T(128)} %bitcast.core, bf16[192,2048]{1,0:T(8,128)(2,1)S(1)} %all_gather.7.x, f32[192,768]{1,0:T(8,128)S(1)} %shard_map.174.both, f32[2,384]{1,0:T(2,128)S(1)} %pad_maximum_fusion.scales, ...), custom_call_target="tpu_custom_call" | custom-call | flops 500000000 | bytes 8388608 | tf_op jit(solution)/shard_map/mlp/pallas_call | solution.py:227
  166.6 2.1 %collective-permute-start.9 = (bf16[96,2048]{1,0:T(8,128)(2,1)S(1)}, bf16[96,2048]{1,0:T(8,128)(2,1)S(1)}, u32[]{:S(2)}, u32[]{:S(2)}) collective-permute-start(bf16[96,2048]{1,0:T(8,128)(2,1)S(1)} %get-tuple-element.12), channel_id=1, source_target_pairs={{0,1},{1,0},{2,3},{3,2},{4,5},{5,4},{6,7},{7,6},{8,9},{9,8},{10,11... | collective-permute-start | bytes 1179656 | tf_op jit(solution)/shard_map/ppermute | solution.py:72
  170.3 11.1 %all_to_all.25 = bf16[4,24,2048]{2,1,0:T(8,128)(2,1)S(1)} all-to-all(bf16[4,24,2048]{2,1,0:T(8,128)(2,1)S(1)} %bitcast.50), channel_id=1, replica_groups=mesh['rep'=2,'z'=4,'y'=8,'x'=4,'core'=2] {'x'}, dimensions={0} | all-to-all | bytes 786432 | tf_op jit(solution)/shard_map/all_to_all | solution.py:68
  (84 shorter events, 25.9 us)
Async XLA Ops:
  2.0 9.4 %copy-start.5 = (f32[64,384]{1,0:T(8,128)S(1)}, f32[64,384]{1,0:T(8,128)}, u32[]{:S(2)}) copy-start(f32[64,384]{1,0:T(8,128)} %gate.1) | copy-start | bytes 294916
  2.0 9.4 %copy-start.6 = (f32[64,384]{1,0:T(8,128)S(1)}, f32[64,384]{1,0:T(8,128)}, u32[]{:S(2)}) copy-start(f32[64,384]{1,0:T(8,128)} %up.1) | copy-start | bytes 294916
  2.0 9.4 %copy-start.7 = (f32[384,64]{0,1:T(8,128)S(1)}, f32[384,64]{0,1:T(8,128)}, u32[]{:S(2)}) copy-start(f32[384,64]{0,1:T(8,128)} %param.32) | copy-start | bytes 294916
  2.0 35.0 %all-to-all-start = ((bf16[8,64,1024]{2,1,0:T(8,128)(2,1)}), bf16[8,64,1024]{2,1,0:T(8,128)(2,1)S(1)}, u32[]{:S(2)}, u32[]{:S(2)}) async-start(bf16[8,64,1024]{2,1,0:T(8,128)(2,1)} %heads_shard.1), calls=%async_computation | async-start | bytes 2097152 | tf_op jit(solution)/shard_map/all_to_all | solution.py:265
  12.6 30.0 %copy-start.13 = (bf16[1,24,2048]{2,1,0:T(8,128)(2,1)S(1)}, bf16[1,24,2048]{2,1,0:T(8,128)(2,1)}, u32[]{:S(2)}) copy-start(bf16[1,24,2048]{2,1,0:T(8,128)(2,1)} %param.18) | copy-start | bytes 294916
  37.0 64.0 %all-to-all-start.3 = ((bf16[8,64,1152]{2,1,0:T(8,128)(2,1)}), bf16[8,64,1152]{2,1,0:T(8,128)(2,1)S(1)}, u32[]{:S(2)}, u32[]{:S(2)}) async-start(bf16[8,64,1152]{2,1,0:T(8,128)(2,1)} %shard_map.173), calls=%async_computation.3 | async-start | bytes 2359296 | tf_op jit(solution)/shard_map/all_to_all | solution.py:267
  41.9 28.6 %copy-start.17 = (f32[2048]{0:T(1024)S(1)}, f32[2048]{0:T(1024)}, u32[]{:S(2)}) copy-start(f32[2048]{0:T(1024)} %param.19) | copy-start | bytes 24580
  56.6 34.6 %collective-permute-start.1 = (bf16[512,1024]{1,0:T(8,128)(2,1)S(1)}, bf16[512,1024]{1,0:T(8,128)(2,1)S(1)}, u32[]{:S(2)}, u32[]{:S(2)}) collective-permute-start(bf16[512,1024]{1,0:T(8,128)(2,1)S(1)} %bitcast.41), channel_id=1, source_target_pairs={{64,128},{128,64},{192,256},{256,192},{320,384},{384,320},{448,0},... | collective-permute-start | bytes 3145736 | tf_op jit(solution)/shard_map/ppermute | solution.py:31
  67.5 27.0 %collective-permute-start = (bf16[512,1024]{1,0:T(8,128)(2,1)S(1)}, bf16[512,1024]{1,0:T(8,128)(2,1)S(1)}, u32[]{:S(2)}, u32[]{:S(2)}) collective-permute-start(bf16[512,1024]{1,0:T(8,128)(2,1)S(1)} %bitcast.42), channel_id=1, source_target_pairs={{0,64},{64,0},{128,192},{192,128},{256,320},{320,256},{384,448},{4... | collective-permute-start | bytes 3145736 | tf_op jit(solution)/shard_map/ppermute | solution.py:30
  70.8 29.0 %copy-start.11 = (bf16[192,2048]{1,0:T(8,128)(2,1)}, bf16[192,2048]{1,0:T(8,128)(2,1)S(1)}, u32[]{:S(2)}) copy-start(bf16[192,2048]{1,0:T(8,128)(2,1)S(1)} %fusion.2) | copy-start | bytes 2359300
  92.1 16.6 %collective-permute-start.3 = (bf16[256,1024]{1,0:T(8,128)(2,1)}, bf16[256,1024]{1,0:T(8,128)(2,1)}, u32[]{:S(2)}, u32[]{:S(2)}) collective-permute-start(bf16[256,1024]{1,0:T(8,128)(2,1)} %slice.41), channel_id=1, source_target_pairs={{0,64},{64,0},{128,192},{192,128},{256,320},{320,256},{384,448},{4... | collective-permute-start | bytes 1572872 | tf_op jit(solution)/shard_map/ppermute | solution.py:33
  95.4 18.2 %collective-permute-start.2 = (bf16[256,1024]{1,0:T(8,128)(2,1)}, bf16[256,1024]{1,0:T(8,128)(2,1)}, u32[]{:S(2)}, u32[]{:S(2)}) collective-permute-start(bf16[256,1024]{1,0:T(8,128)(2,1)} %slice.39), channel_id=1, source_target_pairs={{64,128},{128,64},{192,256},{256,192},{320,384},{384,320},{448,0},... | collective-permute-start | bytes 1572872 | tf_op jit(solution)/shard_map/ppermute | solution.py:32
  101.0 36.1 %collective-permute-start.6 = (bf16[512,1152]{1,0:T(8,128)(2,1)S(1)}, bf16[512,1152]{1,0:T(8,128)(2,1)S(1)}, u32[]{:S(2)}, u32[]{:S(2)}) collective-permute-start(bf16[512,1152]{1,0:T(8,128)(2,1)S(1)} %bitcast.37), channel_id=1, source_target_pairs={{64,128},{128,64},{192,256},{256,192},{320,384},{384,320},{448,0},... | collective-permute-start | bytes 3538952 | tf_op jit(solution)/shard_map/ppermute | solution.py:31
  103.8 36.7 %collective-permute-start.5 = (bf16[512,1152]{1,0:T(8,128)(2,1)S(1)}, bf16[512,1152]{1,0:T(8,128)(2,1)}, u32[]{:S(2)}, u32[]{:S(2)}) collective-permute-start(bf16[512,1152]{1,0:T(8,128)(2,1)S(1)} %bitcast.38), channel_id=1, source_target_pairs={{0,64},{64,0},{128,192},{192,128},{256,320},{320,256},{384,448},{4... | collective-permute-start | bytes 3538952 | tf_op jit(solution)/shard_map/ppermute | solution.py:30
  118.2 3.6 %collective-permute-start.4 = (bf16[96,2048]{1,0:T(8,128)(2,1)S(1)}, bf16[96,2048]{1,0:T(8,128)(2,1)S(1)}, u32[]{:S(2)}, u32[]{:S(2)}) collective-permute-start(bf16[96,2048]{1,0:T(8,128)(2,1)S(1)} %get-tuple-element.10), channel_id=1, source_target_pairs={{0,1},{1,0},{2,3},{3,2},{4,5},{5,4},{6,7},{7,6},{8,9},{9,8},{10,11... | collective-permute-start | bytes 1179656 | tf_op jit(solution)/shard_map/ppermute | solution.py:72
  122.6 24.4 %all-to-all-start.1 = ((bf16[4,24,2048]{2,1,0:T(8,128)(2,1)}), bf16[4,24,2048]{2,1,0:T(8,128)(2,1)S(1)}, u32[]{:S(2)}, u32[]{:S(2)}) async-start(bf16[4,24,2048]{2,1,0:T(8,128)(2,1)} %bitcast.8), calls=%async_computation.1 | async-start | bytes 786432 | tf_op jit(solution)/shard_map/all_to_all | solution.py:68
  138.0 9.2 %copy-start.16 = (f32[2048]{0:T(1024)S(1)}, f32[2048]{0:T(1024)}, u32[]{:S(2)}) copy-start(f32[2048]{0:T(1024)} %param.27) | copy-start | bytes 24580
  138.0 9.4 %copy-start.18 = (f32[2048]{0:T(1024)S(1)}, f32[2048]{0:T(1024)}, u32[]{:S(2)}) copy-start(f32[2048]{0:T(1024)} %param.29) | copy-start | bytes 24580
  138.0 26.2 %collective-permute-start.8 = (bf16[256,1152]{1,0:T(8,128)(2,1)}, bf16[256,1152]{1,0:T(8,128)(2,1)S(1)}, u32[]{:S(2)}, u32[]{:S(2)}) collective-permute-start(bf16[256,1152]{1,0:T(8,128)(2,1)} %slice.44), channel_id=1, source_target_pairs={{0,64},{64,0},{128,192},{192,128},{256,320},{320,256},{384,448},{4... | collective-permute-start | bytes 1769480 | tf_op jit(solution)/shard_map/ppermute | solution.py:33
  142.5 21.7 %collective-permute-start.7 = (bf16[256,1152]{1,0:T(8,128)(2,1)}, bf16[256,1152]{1,0:T(8,128)(2,1)}, u32[]{:S(2)}, u32[]{:S(2)}) collective-permute-start(bf16[256,1152]{1,0:T(8,128)(2,1)} %slice.43), channel_id=1, source_target_pairs={{64,128},{128,64},{192,256},{256,192},{320,384},{384,320},{448,0},... | collective-permute-start | bytes 1769480 | tf_op jit(solution)/shard_map/ppermute | solution.py:32
  148.8 11.1 %all-to-all-start.2 = ((bf16[4,24,2048]{2,1,0:T(8,128)(2,1)}), bf16[4,24,2048]{2,1,0:T(8,128)(2,1)S(1)}, u32[]{:S(2)}, u32[]{:S(2)}) async-start(bf16[4,24,2048]{2,1,0:T(8,128)(2,1)} %broadcast_in_dim.34), calls=%async_computation.2 | async-start | bytes 786432 | tf_op jit(solution)/shard_map/all_to_all | solution.py:299
  166.6 3.6 %collective-permute-start.9 = (bf16[96,2048]{1,0:T(8,128)(2,1)S(1)}, bf16[96,2048]{1,0:T(8,128)(2,1)S(1)}, u32[]{:S(2)}, u32[]{:S(2)}) collective-permute-start(bf16[96,2048]{1,0:T(8,128)(2,1)S(1)} %get-tuple-element.12), channel_id=1, source_target_pairs={{0,1},{1,0},{2,3},{3,2},{4,5},{5,4},{6,7},{7,6},{8,9},{9,8},{10,11... | collective-permute-start | bytes 1179656 | tf_op jit(solution)/shard_map/ppermute | solution.py:72
  170.3 11.2 %copy-start.15 = (bf16[1,24,2048]{2,1,0:T(8,128)(2,1)S(1)}, bf16[1,24,2048]{2,1,0:T(8,128)(2,1)}, u32[]{:S(2)}) copy-start(bf16[1,24,2048]{2,1,0:T(8,128)(2,1)} %get-tuple-element.14) | copy-start | bytes 294916
  170.3 11.2 %copy-start.19 = (f32[2048]{0:T(1024)S(1)}, f32[2048]{0:T(1024)}, u32[]{:S(2)}) copy-start(f32[2048]{0:T(1024)} %param.35) | copy-start | bytes 24580
  (12 other events, 54.8 us)

commit v8 on v4

--- a/solution.py
+++ b/solution.py
@@ -91,13 +91,13 @@
 SMEM = pl.BlockSpec(memory_space=pltpu.SMEM)
 
 
-def local_call(kernel, out_shape, specs, flops, moved, out_specs=VMEM):
+def local_call(kernel, out_shape, specs, flops, moved, out_specs=VMEM, grant=24):
     return pl.pallas_call(
         kernel,
         out_shape=out_shape,
         in_specs=specs,
         out_specs=out_specs,
-        compiler_params=pltpu.CompilerParams(vmem_limit_bytes=24 * 2**20),
+        compiler_params=pltpu.CompilerParams(vmem_limit_bytes=grant * 2**20),
         cost_estimate=pl.CostEstimate(flops=flops, bytes_accessed=moved, transcendentals=0),
     )
 
@@ -187,15 +187,6 @@
     )
 
 
-def hold_kernel(weights, out):
-    out[...] = weights[...]
-
-
-def hold(weights):
-    shape = jax.ShapeDtypeStruct(weights.shape, weights.dtype)
-    return local_call(hold_kernel, shape, [VMEM], 10**7, 4 * weights.size)(weights)
-
-
 def mlp_kernel(labels, x, weights, others, scales, other_scales, out):
     units = scales.shape[1]
     size = x.shape[1] // 4
@@ -219,9 +210,9 @@
 def mlp(labels, x, weights, others, scales, other_scales):
     shape = jax.ShapeDtypeStruct(x.shape, jnp.bfloat16)
     flops = 4 * x.shape[0] * x.shape[1] * weights.shape[-1]
-    return local_call(mlp_kernel, shape, [SMEM] + [VMEM] * 5, flops, 4 * weights.size)(
-        labels, x, weights, others, scales, other_scales
-    )
+    moved = 4 * weights.size
+    call = local_call(mlp_kernel, shape, [SMEM] + [VMEM] * 5, flops, moved, grant=57)
+    return call(labels, x, weights, others, scales, other_scales)
 
 
 def per_device(
@@ -253,7 +244,6 @@
     heads = lax.all_to_all(heads, "y", 0, 0, tiled=True).reshape(-1, heads.shape[2])
     own = ring_blocks(mlp_shard(w_gate, w_up, w_down))
     mlp_weights = lax.all_gather(own, "y", axis=0)
-    mlp_weights = hold(mlp_weights)
     mlp_others = swap_cores(mlp_weights)
     mlp_scales = jnp.stack([scale_gate, scale_up])
     other_scales = swap_cores(mlp_scales)

time: 195 us -> 194 us (level)
    unnamed x32 -> x34, local copies, waits for them, and re-layouts: 6.25 us -> 4.67 us
    pallas_call x2 -> x1, Pallas kernels: 8.84 us -> 7.27 us  [mlp(): return call(labels, x, weights, others, scales, other_scales)]
  transfers between devices with their start and end apart: 14 -> 14, of which waited for: 9 -> 9; matrix products, arithmetic and copies ran while one was open for 2% -> 3% of each run, Pallas kernels for 3% -> 2%
where the time goes in v8:
time: 194 us; the launch traced here: 193 us
  waiting for transfers between devices  82.2 us (42%)
  starting transfers between devices  48.9 us (25%)
  blocking collectives  24.5 us (13%)
  between operations  14.4 us (7%)
  Pallas kernels  10.2 us (5%)
  local copies, waits for them, and re-layouts  5.56 us (3%)
  other arithmetic  5.48 us (3%)
    all_gather x1, waiting for transfers between devices, per_device(): mlp_weights = lax.all_gather(own, 'y', axis=0)  30.4 us
    all_to_all x1, waiting for transfers between devices, per_device(): lax.all_to_all(heads, 'y', 0, 0, tiled=True).reshape(-1, heads.shape[2])  19.3 us
    all_gather x1, blocking collectives, per_device(): all_rows = lax.all_gather(own_rows, TP, axis=0, tiled=True)  13.7 us
    all_to_all x1, blocking collectives, sum_over_chips(): lax.all_to_all(blocks, 'x', 0, 0, tiled=True).astype(jnp.float32)  10.8 us
    ppermute x1, waiting for transfers between devices, ring_pieces(): far_b = lax.ppermute(odd[half:], RING, pairs(0))  8.47 us
    all_to_all x1, waiting for transfers between devices, sum_over_chips(): lax.all_to_all(blocks, 'x', 0, 0, tiled=True).astype(jnp.float32)  8.37 us
    all_to_all x1, starting transfers between devices, per_device(): lax.all_to_all(heads, 'y', 0, 0, tiled=True).reshape(-1, heads.shape[2])  7.33 us
    pallas_call x1, Pallas kernels, mlp(): return call(labels, x, weights, others, scales, other_scales)  7.27 us
  transfers between devices with their start and end apart: 14, of which 9 were waited for; matrix products, arithmetic and copies ran while one was open for 3% of the time, Pallas kernels for 2%

profile of v8, /device:TPU:24, one launch (start us, length us, event | category | flops | bytes accessed | tf_op | source)
XLA Modules:
  0.0 192.8 jit_solution(647455530750112141)
XLA Ops:
  9.2 6.1 %collective-permute-start.7 = (bf16[64,1152]{1,0:T(8,128)(2,1)S(1)}, bf16[64,1152]{1,0:T(8,128)(2,1)S(1)}, u32[]{:S(2)}, u32[]{:S(2)}) collective-permute-start(bf16[64,1152]{1,0:T(8,128)(2,1)S(1)} %shard_map.173), channel_id=1, source_target_pairs={{0,128},{64,192},{128,256},{192,320},{256,384},{320,448},{384,0},{... | collective-permute-start | bytes 442376 | tf_op jit(solution)/shard_map/ppermute | solution.py:51
  15.3 6.8 %collective-permute-start.6 = (bf16[64,1152]{1,0:T(8,128)(2,1)S(1)}, bf16[64,1152]{1,0:T(8,128)(2,1)S(1)}, u32[]{:S(2)}, u32[]{:S(2)}) collective-permute-start(bf16[64,1152]{1,0:T(8,128)(2,1)S(1)} %shard_map.173), channel_id=1, source_target_pairs={{64,128},{128,64},{192,256},{256,192},{320,384},{384,320},{448,0},... | collective-permute-start | bytes 442376 | tf_op jit(solution)/shard_map/ppermute | solution.py:50
  22.1 3.0 %collective-permute-start.5 = (bf16[64,1152]{1,0:T(8,128)(2,1)S(1)}, bf16[64,1152]{1,0:T(8,128)(2,1)S(1)}, u32[]{:S(2)}, u32[]{:S(2)}) collective-permute-start(bf16[64,1152]{1,0:T(8,128)(2,1)S(1)} %shard_map.173), channel_id=1, source_target_pairs={{0,64},{64,0},{128,192},{192,128},{256,320},{320,256},{384,448},{4... | collective-permute-start | bytes 442376 | tf_op jit(solution)/shard_map/ppermute | solution.py:49
  25.1 5.2 %collective-permute-done.6 = bf16[64,1152]{1,0:T(8,128)(2,1)S(1)} collective-permute-done((bf16[64,1152]{1,0:T(8,128)(2,1)S(1)}, bf16[64,1152]{1,0:T(8,128)(2,1)S(1)}, u32[]{:S(2)}, u32[]{:S(2)}) %collective-permute-start.6) | collective-permute-done | bytes 147488 | tf_op jit(solution)/shard_map/ppermute | solution.py:50
  31.3 2.1 %heads_shard.1 = bf16[8,64,1024]{2,1,0:T(8,128)(2,1)} custom-call(f32[64,256]{1,0:T(8,128)} %query.1, f32[64,256]{1,0:T(8,128)} %keyed.1, f32[64,256]{1,0:T(8,128)} %valued.1, f32[64,256]{1,0:T(8,128)} %bitcast.61), custom_call_target="tpu_custom_call" | custom-call | flops 10000000 | bytes 2097152 | tf_op jit(solution)/shard_map/heads_shard/pallas_call | solution.py:120
  33.4 7.3 %all-to-all-start = ((bf16[8,64,1024]{2,1,0:T(8,128)(2,1)}), bf16[8,64,1024]{2,1,0:T(8,128)(2,1)S(1)}, u32[]{:S(2)}, u32[]{:S(2)}) async-start(bf16[8,64,1024]{2,1,0:T(8,128)(2,1)} %heads_shard.1), calls=%async_computation | async-start | bytes 2097152 | tf_op jit(solution)/shard_map/all_to_all | solution.py:244
  41.4 13.7 %all-gather = bf16[1,192,2048]{2,1,0:T(8,128)(2,1)S(1)} all-gather(bf16[1,24,2048]{2,1,0:T(8,128)(2,1)S(1)} %copy-done.8), channel_id=2, replica_groups=mesh['rep'=2,'z'=4,'y'=8,'x'=4,'core'=2] {'x','core'}, dimensions={1}, use_global_device_ids=true | all-gather | bytes 884736 | tf_op jit(solution)/shard_map/all_gather | solution.py:251
  56.2 19.3 %all-to-all-done = bf16[8,64,1024]{2,1,0:T(8,128)(2,1)S(1)} async-done(((bf16[8,64,1024]{2,1,0:T(8,128)(2,1)}), bf16[8,64,1024]{2,1,0:T(8,128)(2,1)S(1)}, u32[]{:S(2)}, u32[]{:S(2)}) %all-to-all-start) | async-done | bytes 1048608 | tf_op jit(solution)/shard_map/all_to_all | solution.py:244
  75.6 1.9 collective-permute-start.1
  77.5 3.3 %collective-permute-start = (bf16[512,1024]{1,0:T(8,128)(2,1)S(1)}, bf16[512,1024]{1,0:T(8,128)(2,1)S(1)}, u32[]{:S(2)}, u32[]{:S(2)}) collective-permute-start(bf16[512,1024]{1,0:T(8,128)(2,1)S(1)} %bitcast.42), channel_id=1, source_target_pairs={{0,64},{64,0},{128,192},{192,128},{256,320},{320,256},{384,448},{4... | collective-permute-start | bytes 3145736 | tf_op jit(solution)/shard_map/ppermute | solution.py:30
  80.8 30.4 %all-gather.4.cloned.1.call-done = bf16[32,64,1152]{2,1,0:T(8,128)(2,1)} async-done(((bf16[4,64,1152]{2,1,0:T(8,128)(2,1)}), bf16[32,64,1152]{2,1,0:T(8,128)(2,1)}) %all-gather.4.cloned.1.call-update) | async-done | bytes 4718608 | tf_op jit(solution)/shard_map/all_gather | solution.py:246
  111.2 1.9 collective-permute-start.8
  114.9 3.4 %collective-permute-start.3 = (bf16[256,1024]{1,0:T(8,128)(2,1)S(1)}, bf16[256,1024]{1,0:T(8,128)(2,1)S(1)}, u32[]{:S(2)}, u32[]{:S(2)}) collective-permute-start(bf16[256,1024]{1,0:T(8,128)(2,1)S(1)} %slice.33), channel_id=1, source_target_pairs={{0,64},{64,0},{128,192},{192,128},{256,320},{320,256},{384,448},{4... | collective-permute-start | bytes 1572872 | tf_op jit(solution)/shard_map/ppermute | solution.py:33
  118.4 3.6 %collective-permute-start.2 = (bf16[256,1024]{1,0:T(8,128)(2,1)S(1)}, bf16[256,1024]{1,0:T(8,128)(2,1)S(1)}, u32[]{:S(2)}, u32[]{:S(2)}) collective-permute-start(bf16[256,1024]{1,0:T(8,128)(2,1)S(1)} %slice.31), channel_id=1, source_target_pairs={{64,128},{128,64},{192,256},{256,192},{320,384},{384,320},{448,0},... | collective-permute-start | bytes 1572872 | tf_op jit(solution)/shard_map/ppermute | solution.py:32
  122.7 8.5 %collective-permute-done.3.far_b = bf16[256,1024]{1,0:T(8,128)(2,1)S(1)} collective-permute-done((bf16[256,1024]{1,0:T(8,128)(2,1)S(1)}, bf16[256,1024]{1,0:T(8,128)(2,1)S(1)}, u32[]{:S(2)}, u32[]{:S(2)}) %collective-permute-start.3) | collective-permute-done | bytes 524320 | tf_op jit(solution)/shard_map/ppermute | solution.py:33
  131.4 4.1 %collective-permute-done.2.far_a = bf16[256,1024]{1,0:T(8,128)(2,1)S(1)} collective-permute-done((bf16[256,1024]{1,0:T(8,128)(2,1)S(1)}, bf16[256,1024]{1,0:T(8,128)(2,1)S(1)}, u32[]{:S(2)}, u32[]{:S(2)}) %collective-permute-start.2) | collective-permute-done | bytes 524320 | tf_op jit(solution)/shard_map/ppermute | solution.py:32
  137.3 1.9 collective-permute-start.4
  141.8 4.3 %all-to-all-start.1 = ((bf16[4,24,2048]{2,1,0:T(8,128)(2,1)}), bf16[4,24,2048]{2,1,0:T(8,128)(2,1)S(1)}, u32[]{:S(2)}, u32[]{:S(2)}) async-start(bf16[4,24,2048]{2,1,0:T(8,128)(2,1)} %bitcast.8), calls=%async_computation.1 | async-start | bytes 786432 | tf_op jit(solution)/shard_map/all_to_all | solution.py:74
  146.1 8.4 %all-to-all-done.1 = bf16[4,24,2048]{2,1,0:T(8,128)(2,1)S(1)} async-done(((bf16[4,24,2048]{2,1,0:T(8,128)(2,1)}), bf16[4,24,2048]{2,1,0:T(8,128)(2,1)S(1)}, u32[]{:S(2)}, u32[]{:S(2)}) %all-to-all-start.1) | async-done | bytes 393248 | tf_op jit(solution)/shard_map/all_to_all | solution.py:74
  155.6 3.5 %all-to-all-start.2 = ((bf16[4,24,2048]{2,1,0:T(8,128)(2,1)}), bf16[4,24,2048]{2,1,0:T(8,128)(2,1)S(1)}, u32[]{:S(2)}, u32[]{:S(2)}) async-start(bf16[4,24,2048]{2,1,0:T(8,128)(2,1)} %broadcast_in_dim.34), calls=%async_computation.2 | async-start | bytes 786432 | tf_op jit(solution)/shard_map/all_to_all | solution.py:280
  159.1 1.9 collective-permute-start.9
  162.2 4.2 %all-to-all-done.2 = bf16[4,24,2048]{2,1,0:T(8,128)(2,1)S(1)} async-done(((bf16[4,24,2048]{2,1,0:T(8,128)(2,1)}), bf16[4,24,2048]{2,1,0:T(8,128)(2,1)S(1)}, u32[]{:S(2)}, u32[]{:S(2)}) %all-to-all-start.2) | async-done | bytes 393248 | tf_op jit(solution)/shard_map/all_to_all | solution.py:280
  167.1 7.3 %shard_map.174 = bf16[96,2048]{1,0:T(8,128)(2,1)} custom-call(s32[4]{0:T(128)} %pad_add_fusion.labels, bf16[96,2048]{1,0:T(8,128)(2,1)} %bitcast.52, bf16[8,4,64,1152]{3,2,1,0:T(8,128)(2,1)} %bitcast.51, bf16[8,4,64,1152]{3,2,1,0:T(8,128)(2,1)} %collective-permute-done.8.others, f32[2,384]{1,0:T(2,128)} %copy-done.10, f32[2,384]{1,0:T(2,128)} %copy-done.14), custom_call_target="tpu_custom_call" | custom-call | flops 905969664 | bytes 9437184 | tf_op jit(solution)/shard_map/pallas_call | solution.py:215
  174.4 10.8 %all_to_all.20 = bf16[4,24,2048]{2,1,0:T(8,128)(2,1)S(1)} all-to-all(bf16[4,24,2048]{2,1,0:T(8,128)(2,1)} %bitcast.53), channel_id=1, replica_groups=mesh['rep'=2,'z'=4,'y'=8,'x'=4,'core'=2] {'x'}, dimensions={0} | all-to-all | bytes 786432 | tf_op jit(solution)/shard_map/all_to_all | solution.py:74
  (71 shorter events, 15.6 us)
Async XLA Ops:
  6.5 104.6 %all-gather.4.cloned.1.call-start = ((), (), s32[]{:S(2)}) async-start(), calls=%async_computation.4 | async-start | bytes 5308416 | tf_op jit(solution)/shard_map/all_gather | solution.py:246
  6.5 0.9 copy-start
  9.2 15.9 %collective-permute-start.7 = (bf16[64,1152]{1,0:T(8,128)(2,1)S(1)}, bf16[64,1152]{1,0:T(8,128)(2,1)S(1)}, u32[]{:S(2)}, u32[]{:S(2)}) collective-permute-start(bf16[64,1152]{1,0:T(8,128)(2,1)S(1)} %shard_map.173), channel_id=1, source_target_pairs={{0,128},{64,192},{128,256},{192,320},{256,384},{320,448},{384,0},{... | collective-permute-start | bytes 442376 | tf_op jit(solution)/shard_map/ppermute | solution.py:51
  15.3 15.0 %collective-permute-start.6 = (bf16[64,1152]{1,0:T(8,128)(2,1)S(1)}, bf16[64,1152]{1,0:T(8,128)(2,1)S(1)}, u32[]{:S(2)}, u32[]{:S(2)}) collective-permute-start(bf16[64,1152]{1,0:T(8,128)(2,1)S(1)} %shard_map.173), channel_id=1, source_target_pairs={{64,128},{128,64},{192,256},{256,192},{320,384},{384,320},{448,0},... | collective-permute-start | bytes 442376 | tf_op jit(solution)/shard_map/ppermute | solution.py:50
  22.1 8.2 %collective-permute-start.5 = (bf16[64,1152]{1,0:T(8,128)(2,1)S(1)}, bf16[64,1152]{1,0:T(8,128)(2,1)S(1)}, u32[]{:S(2)}, u32[]{:S(2)}) collective-permute-start(bf16[64,1152]{1,0:T(8,128)(2,1)S(1)} %shard_map.173), channel_id=1, source_target_pairs={{0,64},{64,0},{128,192},{192,128},{256,320},{320,256},{384,448},{4... | collective-permute-start | bytes 442376 | tf_op jit(solution)/shard_map/ppermute | solution.py:49
  31.3 10.1 %copy-start.8 = (bf16[1,24,2048]{2,1,0:T(8,128)(2,1)S(1)}, bf16[1,24,2048]{2,1,0:T(8,128)(2,1)}, u32[]{:S(2)}) copy-start(bf16[1,24,2048]{2,1,0:T(8,128)(2,1)} %param.18) | copy-start | bytes 294916
  33.4 80.1 %copy-start.11 = (f32[2048]{0:T(1024)S(1)}, f32[2048]{0:T(1024)}, u32[]{:S(2)}) copy-start(f32[2048]{0:T(1024)} %param.19) | copy-start | bytes 24580
  33.4 42.2 %all-to-all-start = ((bf16[8,64,1024]{2,1,0:T(8,128)(2,1)}), bf16[8,64,1024]{2,1,0:T(8,128)(2,1)S(1)}, u32[]{:S(2)}, u32[]{:S(2)}) async-start(bf16[8,64,1024]{2,1,0:T(8,128)(2,1)} %heads_shard.1), calls=%async_computation | async-start | bytes 2097152 | tf_op jit(solution)/shard_map/all_to_all | solution.py:244
  75.6 39.3 %collective-permute-start.1 = (bf16[512,1024]{1,0:T(8,128)(2,1)S(1)}, bf16[512,1024]{1,0:T(8,128)(2,1)S(1)}, u32[]{:S(2)}, u32[]{:S(2)}) collective-permute-start(bf16[512,1024]{1,0:T(8,128)(2,1)S(1)} %bitcast.41), channel_id=1, source_target_pairs={{64,128},{128,64},{192,256},{256,192},{320,384},{384,320},{448,0},... | collective-permute-start | bytes 3145736 | tf_op jit(solution)/shard_map/ppermute | solution.py:31
  77.5 40.8 %collective-permute-start = (bf16[512,1024]{1,0:T(8,128)(2,1)S(1)}, bf16[512,1024]{1,0:T(8,128)(2,1)S(1)}, u32[]{:S(2)}, u32[]{:S(2)}) collective-permute-start(bf16[512,1024]{1,0:T(8,128)(2,1)S(1)} %bitcast.42), channel_id=1, source_target_pairs={{0,64},{64,0},{128,192},{192,128},{256,320},{320,256},{384,448},{4... | collective-permute-start | bytes 3145736 | tf_op jit(solution)/shard_map/ppermute | solution.py:30
  111.2 55.2 %collective-permute-start.8 = (bf16[8,4,64,1152]{3,2,1,0:T(8,128)(2,1)}, bf16[8,4,64,1152]{3,2,1,0:T(8,128)(2,1)}, u32[]{:S(2)}, u32[]{:S(2)}) collective-permute-start(bf16[8,4,64,1152]{3,2,1,0:T(8,128)(2,1)} %bitcast.50), channel_id=1, source_target_pairs={{0,1},{1,0},{2,3},{3,2},{4,5},{5,4},{6,7},{7,6},{8,9},{9,8},{10,11... | collective-permute-start | bytes 14155784 | tf_op jit(solution)/shard_map/ppermute | solution.py:78
  114.9 16.2 %collective-permute-start.3 = (bf16[256,1024]{1,0:T(8,128)(2,1)S(1)}, bf16[256,1024]{1,0:T(8,128)(2,1)S(1)}, u32[]{:S(2)}, u32[]{:S(2)}) collective-permute-start(bf16[256,1024]{1,0:T(8,128)(2,1)S(1)} %slice.33), channel_id=1, source_target_pairs={{0,64},{64,0},{128,192},{192,128},{256,320},{320,256},{384,448},{4... | collective-permute-start | bytes 1572872 | tf_op jit(solution)/shard_map/ppermute | solution.py:33
  118.4 17.2 %collective-permute-start.2 = (bf16[256,1024]{1,0:T(8,128)(2,1)S(1)}, bf16[256,1024]{1,0:T(8,128)(2,1)S(1)}, u32[]{:S(2)}, u32[]{:S(2)}) collective-permute-start(bf16[256,1024]{1,0:T(8,128)(2,1)S(1)} %slice.31), channel_id=1, source_target_pairs={{64,128},{128,64},{192,256},{256,192},{320,384},{384,320},{448,0},... | collective-permute-start | bytes 1572872 | tf_op jit(solution)/shard_map/ppermute | solution.py:32
  137.3 3.6 %collective-permute-start.4 = (bf16[96,2048]{1,0:T(8,128)(2,1)S(1)}, bf16[96,2048]{1,0:T(8,128)(2,1)S(1)}, u32[]{:S(2)}, u32[]{:S(2)}) collective-permute-start(bf16[96,2048]{1,0:T(8,128)(2,1)S(1)} %get-tuple-element.8), channel_id=1, source_target_pairs={{0,1},{1,0},{2,3},{3,2},{4,5},{5,4},{6,7},{7,6},{8,9},{9,8},{10,11... | collective-permute-start | bytes 1179656 | tf_op jit(solution)/shard_map/ppermute | solution.py:78
  140.9 13.6 %copy-start.9 = (f32[2048]{0:T(1024)S(1)}, f32[2048]{0:T(1024)}, u32[]{:S(2)}) copy-start(f32[2048]{0:T(1024)} %param.27) | copy-start | bytes 24580
  140.9 13.8 %copy-start.12 = (f32[2048]{0:T(1024)S(1)}, f32[2048]{0:T(1024)}, u32[]{:S(2)}) copy-start(f32[2048]{0:T(1024)} %param.29) | copy-start | bytes 24580
  141.8 12.7 %all-to-all-start.1 = ((bf16[4,24,2048]{2,1,0:T(8,128)(2,1)}), bf16[4,24,2048]{2,1,0:T(8,128)(2,1)S(1)}, u32[]{:S(2)}, u32[]{:S(2)}) async-start(bf16[4,24,2048]{2,1,0:T(8,128)(2,1)} %bitcast.8), calls=%async_computation.1 | async-start | bytes 786432 | tf_op jit(solution)/shard_map/all_to_all | solution.py:74
  146.1 13.0 %copy-start.15 = (f32[384]{0:T(512)S(1)}, f32[384]{0:T(512)}, u32[]{:S(2)}) copy-start(f32[384]{0:T(512)} %param.34) | copy-start | bytes 4612
  146.1 13.0 %copy-start.16 = (f32[384]{0:T(512)S(1)}, f32[384]{0:T(512)}, u32[]{:S(2)}) copy-start(f32[384]{0:T(512)} %param.33) | copy-start | bytes 4612
  155.6 10.8 %all-to-all-start.2 = ((bf16[4,24,2048]{2,1,0:T(8,128)(2,1)}), bf16[4,24,2048]{2,1,0:T(8,128)(2,1)S(1)}, u32[]{:S(2)}, u32[]{:S(2)}) async-start(bf16[4,24,2048]{2,1,0:T(8,128)(2,1)} %broadcast_in_dim.34), calls=%async_computation.2 | async-start | bytes 786432 | tf_op jit(solution)/shard_map/all_to_all | solution.py:280
  159.1 7.3 %copy-start.10 = (f32[2,384]{1,0:T(2,128)}, f32[2,384]{1,0:T(2,128)S(1)}, u32[]{:S(2)}) copy-start(f32[2,384]{1,0:T(2,128)S(1)} %pad_maximum_fusion.1.scales) | copy-start | bytes 9220
  159.1 3.1 %collective-permute-start.9 = (f32[2,384]{1,0:T(2,128)S(1)}, f32[2,384]{1,0:T(2,128)S(1)}, u32[]{:S(2)}, u32[]{:S(2)}) collective-permute-start(f32[2,384]{1,0:T(2,128)S(1)} %pad_maximum_fusion.1.scales), channel_id=1, source_target_pairs={{0,1},{1,0},{2,3},{3,2},{4,5},{5,4},{6,7},{7,6},{8,9},{9,8},{10,11... | collective-permute-start | bytes 9224 | tf_op jit(solution)/shard_map/ppermute | solution.py:78
  162.2 4.2 %copy-start.14 = (f32[2,384]{1,0:T(2,128)}, f32[2,384]{1,0:T(2,128)S(1)}, u32[]{:S(2)}) copy-start(f32[2,384]{1,0:T(2,128)S(1)} %collective-permute-done.9.other_scales) | copy-start | bytes 9220
  167.1 18.1 %copy-start.13 = (f32[2048]{0:T(1024)S(1)}, f32[2048]{0:T(1024)}, u32[]{:S(2)}) copy-start(f32[2048]{0:T(1024)} %param.35) | copy-start | bytes 24580
  (7 other events, 5.5 us)
Sparse Core Ops, SparseCore 0:
  31.4 79.7 all-gather.3

commit v9 on v4

--- a/solution.py
+++ b/solution.py
@@ -25,13 +25,16 @@
     return out
 
 
-def ring_pieces(block):
+def ring_halves(block):
     half = block.shape[0] // 2
-    even = lax.ppermute(block, RING, pairs(0))
-    odd = lax.ppermute(block, RING, pairs(1))
-    far_a = lax.ppermute(even[:half], RING, pairs(1))
-    far_b = lax.ppermute(odd[half:], RING, pairs(0))
-    return block, even, odd, far_a, far_b
+    low, high = block[:half], block[half:]
+    even1 = lax.ppermute(low, RING, pairs(0))
+    odd2 = lax.ppermute(high, RING, pairs(1))
+    even2 = lax.ppermute(high, RING, pairs(0))
+    odd1 = lax.ppermute(low, RING, pairs(1))
+    far_a = lax.ppermute(even1, RING, pairs(1))
+    far_b = lax.ppermute(odd2, RING, pairs(0))
+    return block, even1, even2, odd1, odd2, far_a, far_b
 
 
 def ring_labels():
@@ -55,8 +58,8 @@
 def ring_dot(x, pieces, columns):
     size = pieces[0].shape[0]
     half = size // 2
-    own_at, even_at, odd_at, far_at = ring_labels()
-    starts = (own_at * size, even_at * size, odd_at * size, far_at * size, far_at * size + half)
+    own_at, even_at, odd_at, far_at = [label * size for label in ring_labels()]
+    starts = (own_at, even_at, even_at + half, odd_at, odd_at + half, far_at, far_at + half)
 
     def term(start, piece):
         cut = lax.dynamic_slice_in_dim(x, start, piece.shape[0], 1)
@@ -145,7 +148,8 @@
     return local_call(mlp_shard_kernel, shape, [VMEM] * 3, 10**7, 2**20)(w_gate, w_up, w_down.T)
 
 
-def retain_kernel(rate, core, product, cosine, sine, sq, sk, sv, own, even, odd, far_a, far_b, kept, sent):
+def retain_kernel(rate, core, product, cosine, sine, sq, sk, sv, *refs):
+    pieces, (kept, sent) = refs[:-2], refs[-2:]
     width = sq.shape[1]
     cos, sin = cosine[...], sine[...]
     query = rotary(product[:, :width] * sq[...], cos, sin).astype(jnp.bfloat16)
@@ -168,7 +172,7 @@
     attended = jnp.concatenate(mine + other, axis=0).astype(jnp.bfloat16)
     half = length // 2
     at = 0
-    for piece in (own, even, odd, far_a, far_b):
+    for piece in pieces:
         to = at + piece.shape[0]
         term = dot_t(attended, piece[:, 3 * width :])
         kept[:, at:to] = term[:half]
@@ -185,15 +189,6 @@
     return local_call(retain_kernel, shapes, specs, 3 * 10**8, 2**21, [VMEM] * 2)(
         rate, core, product, cosine, sine, *scales, *pieces
     )
-
-
-def hold_kernel(weights, out):
-    out[...] = weights[...]
-
-
-def hold(weights):
-    shape = jax.ShapeDtypeStruct(weights.shape, weights.dtype)
-    return local_call(hold_kernel, shape, [VMEM], 10**7, 4 * weights.size)(weights)
 
 
 def mlp_kernel(labels, x, weights, others, scales, other_scales, out):
@@ -253,11 +248,10 @@
     heads = lax.all_to_all(heads, "y", 0, 0, tiled=True).reshape(-1, heads.shape[2])
     own = ring_blocks(mlp_shard(w_gate, w_up, w_down))
     mlp_weights = lax.all_gather(own, "y", axis=0)
-    mlp_weights = hold(mlp_weights)
     mlp_others = swap_cores(mlp_weights)
     mlp_scales = jnp.stack([scale_gate, scale_up])
     other_scales = swap_cores(mlp_scales)
-    heads = ring_pieces(heads)
+    heads = ring_halves(heads)
     all_rows = lax.all_gather(own_rows, TP, axis=0, tiled=True)
 
     values = all_rows.astype(f32)

time: 195 us -> 208 us (1.067)
  waiting for transfers between devices: 82.9 us -> 94.2 us
  starting transfers between devices: 48.9 us -> 54.5 us
  Pallas kernels: 11.7 us -> 7.86 us
    ppermute x4 -> x6, waiting for transfers between devices: 12.6 us -> 20.5 us  [the longest x1 10.5 us: ring_halves(): far_b = lax.ppermute(odd2, RING, pairs(0))]
    ppermute x4 -> x6, starting transfers between devices: 12.2 us -> 17.8 us  [the longest x1 3.93 us: ring_halves(): far_b = lax.ppermute(odd2, RING, pairs(0))]
    pallas_call x1 -> x0, Pallas kernels: 2.48 us -> none  [hold(): local_call(hold_kernel, shape, [VMEM], 10 ** 7, 4 * weights.size)(weights)]
    all_gather x1, waiting for transfers between devices: 30.4 us -> 32.6 us  [per_device(): mlp_weights = lax.all_gather(own, 'y', axis=0)]
    unnamed x32 -> x28, local copies, waits for them, and re-layouts: 6.25 us -> 5.06 us
  transfers between devices with their start and end apart: 14 -> 16, of which waited for: 9 -> 11; matrix products, arithmetic and copies ran while one was open for 2% -> 3% of each run, Pallas kernels for 3% -> 1%
where the time goes in v9:
time: 208 us; the launch traced here: 207 us
  waiting for transfers between devices  94.2 us (45%)
  starting transfers between devices  54.5 us (26%)
  blocking collectives  23.5 us (11%)
  between operations  14.5 us (7%)
  Pallas kernels  7.86 us (4%)
  local copies, waits for them, and re-layouts  7 us (3%)
  other arithmetic  3.76 us (2%)
    all_gather x1, waiting for transfers between devices, per_device(): mlp_weights = lax.all_gather(own, 'y', axis=0)  32.6 us
    all_to_all x1, waiting for transfers between devices, per_device(): lax.all_to_all(heads, 'y', 0, 0, tiled=True).reshape(-1, heads.shape[2])  20.6 us
    all_gather x1, blocking collectives, per_device(): all_rows = lax.all_gather(own_rows, TP, axis=0, tiled=True)  13.7 us
    ppermute x1, waiting for transfers between devices, ring_halves(): far_b = lax.ppermute(odd2, RING, pairs(0))  10.5 us
    all_to_all x1, blocking collectives, sum_over_chips(): lax.all_to_all(blocks, 'x', 0, 0, tiled=True).astype(jnp.float32)  9.77 us
    all_to_all x1, waiting for transfers between devices, sum_over_chips(): lax.all_to_all(blocks, 'x', 0, 0, tiled=True).astype(jnp.float32)  8.37 us
    all_to_all x1, starting transfers between devices, per_device(): lax.all_to_all(heads, 'y', 0, 0, tiled=True).reshape(-1, heads.shape[2])  7.33 us
    ppermute x1, starting transfers between devices, ring_blocks(): odd = lax.ppermute(block, RING, pairs(1))  6.78 us
  transfers between devices with their start and end apart: 16, of which 11 were waited for; matrix products, arithmetic and copies ran while one was open for 3% of the time, Pallas kernels for 1%

profile of v9, /device:TPU:24, one launch (start us, length us, event | category | flops | bytes accessed | tf_op | source)
XLA Modules:
  0.0 207.1 jit_solution(5598762048797570822)
XLA Ops:
  9.2 6.1 %collective-permute-start.9 = (bf16[64,1152]{1,0:T(8,128)(2,1)S(1)}, bf16[64,1152]{1,0:T(8,128)(2,1)S(1)}, u32[]{:S(2)}, u32[]{:S(2)}) collective-permute-start(bf16[64,1152]{1,0:T(8,128)(2,1)S(1)} %shard_map.173), channel_id=1, source_target_pairs={{0,128},{64,192},{128,256},{192,320},{256,384},{320,448},{384,0},{... | collective-permute-start | bytes 442376 | tf_op jit(solution)/shard_map/ppermute | solution.py:54
  15.3 6.8 %collective-permute-start.8 = (bf16[64,1152]{1,0:T(8,128)(2,1)S(1)}, bf16[64,1152]{1,0:T(8,128)(2,1)S(1)}, u32[]{:S(2)}, u32[]{:S(2)}) collective-permute-start(bf16[64,1152]{1,0:T(8,128)(2,1)S(1)} %shard_map.173), channel_id=1, source_target_pairs={{64,128},{128,64},{192,256},{256,192},{320,384},{384,320},{448,0},... | collective-permute-start | bytes 442376 | tf_op jit(solution)/shard_map/ppermute | solution.py:53
  22.1 3.0 %collective-permute-start.7 = (bf16[64,1152]{1,0:T(8,128)(2,1)S(1)}, bf16[64,1152]{1,0:T(8,128)(2,1)S(1)}, u32[]{:S(2)}, u32[]{:S(2)}) collective-permute-start(bf16[64,1152]{1,0:T(8,128)(2,1)S(1)} %shard_map.173), channel_id=1, source_target_pairs={{0,64},{64,0},{128,192},{192,128},{256,320},{320,256},{384,448},{4... | collective-permute-start | bytes 442376 | tf_op jit(solution)/shard_map/ppermute | solution.py:52
  25.1 5.2 %collective-permute-done.8 = bf16[64,1152]{1,0:T(8,128)(2,1)S(1)} collective-permute-done((bf16[64,1152]{1,0:T(8,128)(2,1)S(1)}, bf16[64,1152]{1,0:T(8,128)(2,1)S(1)}, u32[]{:S(2)}, u32[]{:S(2)}) %collective-permute-start.8) | collective-permute-done | bytes 147488 | tf_op jit(solution)/shard_map/ppermute | solution.py:53
  31.3 2.1 heads_shard.1
  33.4 7.3 %all-to-all-start = ((bf16[8,64,1024]{2,1,0:T(8,128)(2,1)}), bf16[8,64,1024]{2,1,0:T(8,128)(2,1)S(1)}, u32[]{:S(2)}, u32[]{:S(2)}) async-start(bf16[8,64,1024]{2,1,0:T(8,128)(2,1)} %heads_shard.1), calls=%async_computation | async-start | bytes 2097152 | tf_op jit(solution)/shard_map/all_to_all | solution.py:248
  40.7 13.7 %all-gather = bf16[1,192,2048]{2,1,0:T(8,128)(2,1)S(1)} all-gather(bf16[1,24,2048]{2,1,0:T(8,128)(2,1)S(1)} %copy-done.7), channel_id=2, replica_groups=mesh['rep'=2,'z'=4,'y'=8,'x'=4,'core'=2] {'x','core'}, dimensions={1}, use_global_device_ids=true | all-gather | bytes 884736 | tf_op jit(solution)/shard_map/all_gather | solution.py:255
  54.9 20.6 %all-to-all-done = bf16[8,64,1024]{2,1,0:T(8,128)(2,1)S(1)} async-done(((bf16[8,64,1024]{2,1,0:T(8,128)(2,1)}), bf16[8,64,1024]{2,1,0:T(8,128)(2,1)S(1)}, u32[]{:S(2)}, u32[]{:S(2)}) %all-to-all-start) | async-done | bytes 1048608 | tf_op jit(solution)/shard_map/all_to_all | solution.py:248
  78.6 32.6 %all-gather.4.cloned.1.call-done = bf16[32,64,1152]{2,1,0:T(8,128)(2,1)} async-done(((bf16[4,64,1152]{2,1,0:T(8,128)(2,1)}), bf16[32,64,1152]{2,1,0:T(8,128)(2,1)}) %all-gather.4.cloned.1.call-update) | async-done | bytes 4718608 | tf_op jit(solution)/shard_map/all_gather | solution.py:250
  113.1 3.3 %collective-permute-start = (bf16[256,1024]{1,0:T(8,128)(2,1)}, bf16[256,1024]{1,0:T(8,128)(2,1)S(1)}, u32[]{:S(2)}, u32[]{:S(2)}) collective-permute-start(bf16[256,1024]{1,0:T(8,128)(2,1)} %bitcast.5), channel_id=1, source_target_pairs={{0,64},{64,0},{128,192},{192,128},{256,320},{320,256},{384,448},{4... | collective-permute-start | bytes 1572872 | tf_op jit(solution)/shard_map/ppermute | solution.py:31
  117.6 3.6 %collective-permute-start.2 = (bf16[256,1024]{1,0:T(8,128)(2,1)}, bf16[256,1024]{1,0:T(8,128)(2,1)S(1)}, u32[]{:S(2)}, u32[]{:S(2)}) collective-permute-start(bf16[256,1024]{1,0:T(8,128)(2,1)} %bitcast.5), channel_id=1, source_target_pairs={{64,128},{128,64},{192,256},{256,192},{320,384},{384,320},{448,0},... | collective-permute-start | bytes 1572872 | tf_op jit(solution)/shard_map/ppermute | solution.py:34
  123.5 3.9 %collective-permute-start.5 = (bf16[256,1024]{1,0:T(8,128)(2,1)S(1)}, bf16[256,1024]{1,0:T(8,128)(2,1)S(1)}, u32[]{:S(2)}, u32[]{:S(2)}) collective-permute-start(bf16[256,1024]{1,0:T(8,128)(2,1)S(1)} %collective-permute-done.3.refs_4_), channel_id=1, source_target_pairs={{0,64},{64,0},{128,192},{192,128},{256,320},{320,256},{384,448},{4... | collective-permute-start | bytes 1572872 | tf_op jit(solution)/shard_map/ppermute | solution.py:36
  127.7 2.3 %collective-permute-done.refs_1_ = bf16[256,1024]{1,0:T(8,128)(2,1)S(1)} collective-permute-done((bf16[256,1024]{1,0:T(8,128)(2,1)}, bf16[256,1024]{1,0:T(8,128)(2,1)S(1)}, u32[]{:S(2)}, u32[]{:S(2)}) %collective-permute-start) | collective-permute-done | bytes 524320 | tf_op jit(solution)/shard_map/ppermute | solution.py:31
  130.0 3.1 %collective-permute-start.4 = (bf16[256,1024]{1,0:T(8,128)(2,1)S(1)}, bf16[256,1024]{1,0:T(8,128)(2,1)S(1)}, u32[]{:S(2)}, u32[]{:S(2)}) collective-permute-start(bf16[256,1024]{1,0:T(8,128)(2,1)S(1)} %collective-permute-done.refs_1_), channel_id=1, source_target_pairs={{64,128},{128,64},{192,256},{256,192},{320,384},{384,320},{448,0},... | collective-permute-start | bytes 1572872 | tf_op jit(solution)/shard_map/ppermute | solution.py:35
  135.3 6.0 %collective-permute-done.1.refs_2_ = bf16[256,1024]{1,0:T(8,128)(2,1)S(1)} collective-permute-done((bf16[256,1024]{1,0:T(8,128)(2,1)}, bf16[256,1024]{1,0:T(8,128)(2,1)S(1)}, u32[]{:S(2)}, u32[]{:S(2)}) %collective-permute-start.1) | collective-permute-done | bytes 524320 | tf_op jit(solution)/shard_map/ppermute | solution.py:33
  141.5 10.5 %collective-permute-done.5.refs_6_ = bf16[256,1024]{1,0:T(8,128)(2,1)S(1)} collective-permute-done((bf16[256,1024]{1,0:T(8,128)(2,1)S(1)}, bf16[256,1024]{1,0:T(8,128)(2,1)S(1)}, u32[]{:S(2)}, u32[]{:S(2)}) %collective-permute-start.5) | collective-permute-done | bytes 524320 | tf_op jit(solution)/shard_map/ppermute | solution.py:36
  157.9 4.3 %all-to-all-start.1 = ((bf16[4,24,2048]{2,1,0:T(8,128)(2,1)}), bf16[4,24,2048]{2,1,0:T(8,128)(2,1)S(1)}, u32[]{:S(2)}, u32[]{:S(2)}) async-start(bf16[4,24,2048]{2,1,0:T(8,128)(2,1)} %bitcast.10), calls=%async_computation.1 | async-start | bytes 786432 | tf_op jit(solution)/shard_map/all_to_all | solution.py:77
  162.2 8.4 %all-to-all-done.1 = bf16[4,24,2048]{2,1,0:T(8,128)(2,1)S(1)} async-done(((bf16[4,24,2048]{2,1,0:T(8,128)(2,1)}), bf16[4,24,2048]{2,1,0:T(8,128)(2,1)S(1)}, u32[]{:S(2)}, u32[]{:S(2)}) %all-to-all-start.1) | async-done | bytes 393248 | tf_op jit(solution)/shard_map/all_to_all | solution.py:77
  171.7 3.5 %all-to-all-start.2 = ((bf16[4,24,2048]{2,1,0:T(8,128)(2,1)}), bf16[4,24,2048]{2,1,0:T(8,128)(2,1)S(1)}, u32[]{:S(2)}, u32[]{:S(2)}) async-start(bf16[4,24,2048]{2,1,0:T(8,128)(2,1)} %broadcast_in_dim.34), calls=%async_computation.2 | async-start | bytes 786432 | tf_op jit(solution)/shard_map/all_to_all | solution.py:284
  175.2 1.9 collective-permute-start.11
  178.3 4.2 %all-to-all-done.2 = bf16[4,24,2048]{2,1,0:T(8,128)(2,1)S(1)} async-done(((bf16[4,24,2048]{2,1,0:T(8,128)(2,1)}), bf16[4,24,2048]{2,1,0:T(8,128)(2,1)S(1)}, u32[]{:S(2)}, u32[]{:S(2)}) %all-to-all-start.2) | async-done | bytes 393248 | tf_op jit(solution)/shard_map/all_to_all | solution.py:284
  182.5 2.3 %copy-done = bf16[32,64,1152]{2,1,0:T(8,128)(2,1)S(1)} copy-done((bf16[32,64,1152]{2,1,0:T(8,128)(2,1)S(1)}, bf16[32,64,1152]{2,1,0:T(8,128)(2,1)}, u32[]{:S(2)}) %copy-start) | copy-done | bytes 4718616
  184.8 4.9 %shard_map.174 = bf16[96,2048]{1,0:T(8,128)(2,1)S(1)} custom-call(s32[4]{0:T(128)S(1)} %pad_add_fusion.labels, bf16[96,2048]{1,0:T(8,128)(2,1)S(1)} %bitcast.47, bf16[8,4,64,1152]{3,2,1,0:T(8,128)(2,1)S(1)} %bitcast.46, bf16[8,4,64,1152]{3,2,1,0:T(8,128)(2,1)} %collective-permute-done.10.others, f32[2,384]{1,0:T(2,128)S(1)} %pad_maximum_fusion.1.scales, ...), custom_call_target="tpu_custom_call" | custom-call | flops 905969664 | bytes 9437184 | tf_op jit(solution)/shard_map/pallas_call | solution.py:217
  189.8 9.8 %all_to_all.20 = bf16[4,24,2048]{2,1,0:T(8,128)(2,1)S(1)} all-to-all(bf16[4,24,2048]{2,1,0:T(8,128)(2,1)S(1)} %bitcast.48), channel_id=1, replica_groups=mesh['rep'=2,'z'=4,'y'=8,'x'=4,'core'=2] {'x'}, dimensions={0} | all-to-all | bytes 786432 | tf_op jit(solution)/shard_map/all_to_all | solution.py:77
  (70 shorter events, 23.2 us)
Async XLA Ops:
  6.5 104.6 %all-gather.4.cloned.1.call-start = ((), (), s32[]{:S(2)}) async-start(), calls=%async_computation.4 | async-start | bytes 5308416 | tf_op jit(solution)/shard_map/all_gather | solution.py:250
  9.2 15.9 %collective-permute-start.9 = (bf16[64,1152]{1,0:T(8,128)(2,1)S(1)}, bf16[64,1152]{1,0:T(8,128)(2,1)S(1)}, u32[]{:S(2)}, u32[]{:S(2)}) collective-permute-start(bf16[64,1152]{1,0:T(8,128)(2,1)S(1)} %shard_map.173), channel_id=1, source_target_pairs={{0,128},{64,192},{128,256},{192,320},{256,384},{320,448},{384,0},{... | collective-permute-start | bytes 442376 | tf_op jit(solution)/shard_map/ppermute | solution.py:54
  15.3 15.0 %collective-permute-start.8 = (bf16[64,1152]{1,0:T(8,128)(2,1)S(1)}, bf16[64,1152]{1,0:T(8,128)(2,1)S(1)}, u32[]{:S(2)}, u32[]{:S(2)}) collective-permute-start(bf16[64,1152]{1,0:T(8,128)(2,1)S(1)} %shard_map.173), channel_id=1, source_target_pairs={{64,128},{128,64},{192,256},{256,192},{320,384},{384,320},{448,0},... | collective-permute-start | bytes 442376 | tf_op jit(solution)/shard_map/ppermute | solution.py:53
  22.1 8.2 %collective-permute-start.7 = (bf16[64,1152]{1,0:T(8,128)(2,1)S(1)}, bf16[64,1152]{1,0:T(8,128)(2,1)S(1)}, u32[]{:S(2)}, u32[]{:S(2)}) collective-permute-start(bf16[64,1152]{1,0:T(8,128)(2,1)S(1)} %shard_map.173), channel_id=1, source_target_pairs={{0,64},{64,0},{128,192},{192,128},{256,320},{320,256},{384,448},{4... | collective-permute-start | bytes 442376 | tf_op jit(solution)/shard_map/ppermute | solution.py:52
  33.4 21.3 %copy-start.9 = (f32[2048]{0:T(1024)S(1)}, f32[2048]{0:T(1024)}, u32[]{:S(2)}) copy-start(f32[2048]{0:T(1024)} %param.19) | copy-start | bytes 24580
  33.4 42.2 %all-to-all-start = ((bf16[8,64,1024]{2,1,0:T(8,128)(2,1)}), bf16[8,64,1024]{2,1,0:T(8,128)(2,1)S(1)}, u32[]{:S(2)}, u32[]{:S(2)}) async-start(bf16[8,64,1024]{2,1,0:T(8,128)(2,1)} %heads_shard.1), calls=%async_computation | async-start | bytes 2097152 | tf_op jit(solution)/shard_map/all_to_all | solution.py:248
  76.7 46.8 %collective-permute-start.3 = (bf16[256,1024]{1,0:T(8,128)(2,1)}, bf16[256,1024]{1,0:T(8,128)(2,1)S(1)}, u32[]{:S(2)}, u32[]{:S(2)}) collective-permute-start(bf16[256,1024]{1,0:T(8,128)(2,1)} %bitcast.6), channel_id=1, source_target_pairs={{64,128},{128,64},{192,256},{256,192},{320,384},{384,320},{448,0},... | collective-permute-start | bytes 1572872 | tf_op jit(solution)/shard_map/ppermute | solution.py:32
  111.2 71.3 %collective-permute-start.10 = (bf16[8,4,64,1152]{3,2,1,0:T(8,128)(2,1)}, bf16[8,4,64,1152]{3,2,1,0:T(8,128)(2,1)}, u32[]{:S(2)}, u32[]{:S(2)}) collective-permute-start(bf16[8,4,64,1152]{3,2,1,0:T(8,128)(2,1)} %bitcast.45), channel_id=1, source_target_pairs={{0,1},{1,0},{2,3},{3,2},{4,5},{5,4},{6,7},{7,6},{8,9},{9,8},{10,11... | collective-permute-start | bytes 14155784 | tf_op jit(solution)/shard_map/ppermute | solution.py:81
  113.1 16.9 %collective-permute-start = (bf16[256,1024]{1,0:T(8,128)(2,1)}, bf16[256,1024]{1,0:T(8,128)(2,1)S(1)}, u32[]{:S(2)}, u32[]{:S(2)}) collective-permute-start(bf16[256,1024]{1,0:T(8,128)(2,1)} %bitcast.5), channel_id=1, source_target_pairs={{0,64},{64,0},{128,192},{192,128},{256,320},{320,256},{384,448},{4... | collective-permute-start | bytes 1572872 | tf_op jit(solution)/shard_map/ppermute | solution.py:31
  117.6 17.4 %collective-permute-start.2 = (bf16[256,1024]{1,0:T(8,128)(2,1)}, bf16[256,1024]{1,0:T(8,128)(2,1)S(1)}, u32[]{:S(2)}, u32[]{:S(2)}) collective-permute-start(bf16[256,1024]{1,0:T(8,128)(2,1)} %bitcast.5), channel_id=1, source_target_pairs={{64,128},{128,64},{192,256},{256,192},{320,384},{384,320},{448,0},... | collective-permute-start | bytes 1572872 | tf_op jit(solution)/shard_map/ppermute | solution.py:34
  121.2 20.0 %collective-permute-start.1 = (bf16[256,1024]{1,0:T(8,128)(2,1)}, bf16[256,1024]{1,0:T(8,128)(2,1)S(1)}, u32[]{:S(2)}, u32[]{:S(2)}) collective-permute-start(bf16[256,1024]{1,0:T(8,128)(2,1)} %bitcast.6), channel_id=1, source_target_pairs={{0,64},{64,0},{128,192},{192,128},{256,320},{320,256},{384,448},{4... | collective-permute-start | bytes 1572872 | tf_op jit(solution)/shard_map/ppermute | solution.py:33
  123.5 28.5 %collective-permute-start.5 = (bf16[256,1024]{1,0:T(8,128)(2,1)S(1)}, bf16[256,1024]{1,0:T(8,128)(2,1)S(1)}, u32[]{:S(2)}, u32[]{:S(2)}) collective-permute-start(bf16[256,1024]{1,0:T(8,128)(2,1)S(1)} %collective-permute-done.3.refs_4_), channel_id=1, source_target_pairs={{0,64},{64,0},{128,192},{192,128},{256,320},{320,256},{384,448},{4... | collective-permute-start | bytes 1572872 | tf_op jit(solution)/shard_map/ppermute | solution.py:36
  130.0 22.2 %collective-permute-start.4 = (bf16[256,1024]{1,0:T(8,128)(2,1)S(1)}, bf16[256,1024]{1,0:T(8,128)(2,1)S(1)}, u32[]{:S(2)}, u32[]{:S(2)}) collective-permute-start(bf16[256,1024]{1,0:T(8,128)(2,1)S(1)} %collective-permute-done.refs_1_), channel_id=1, source_target_pairs={{64,128},{128,64},{192,256},{256,192},{320,384},{384,320},{448,0},... | collective-permute-start | bytes 1572872 | tf_op jit(solution)/shard_map/ppermute | solution.py:35
  141.5 11.0 %copy-start.4 = (f32[256]{0:T(256)S(1)}, f32[256]{0:T(256)}, u32[]{:S(2)}) copy-start(f32[256]{0:T(256)} %param.24) | copy-start | bytes 3076
  141.5 11.0 %copy-start.5 = (f32[256]{0:T(256)S(1)}, f32[256]{0:T(256)}, u32[]{:S(2)}) copy-start(f32[256]{0:T(256)} %param.25) | copy-start | bytes 3076
  153.4 3.6 %collective-permute-start.6 = (bf16[96,2048]{1,0:T(8,128)(2,1)S(1)}, bf16[96,2048]{1,0:T(8,128)(2,1)S(1)}, u32[]{:S(2)}, u32[]{:S(2)}) collective-permute-start(bf16[96,2048]{1,0:T(8,128)(2,1)S(1)} %get-tuple-element.8), channel_id=1, source_target_pairs={{0,1},{1,0},{2,3},{3,2},{4,5},{5,4},{6,7},{7,6},{8,9},{9,8},{10,11... | collective-permute-start | bytes 1179656 | tf_op jit(solution)/shard_map/ppermute | solution.py:81
  157.0 13.6 %copy-start.8 = (f32[2048]{0:T(1024)S(1)}, f32[2048]{0:T(1024)}, u32[]{:S(2)}) copy-start(f32[2048]{0:T(1024)} %param.27) | copy-start | bytes 24580
  157.0 13.8 %copy-start.10 = (f32[2048]{0:T(1024)S(1)}, f32[2048]{0:T(1024)}, u32[]{:S(2)}) copy-start(f32[2048]{0:T(1024)} %param.29) | copy-start | bytes 24580
  157.9 12.7 %all-to-all-start.1 = ((bf16[4,24,2048]{2,1,0:T(8,128)(2,1)}), bf16[4,24,2048]{2,1,0:T(8,128)(2,1)S(1)}, u32[]{:S(2)}, u32[]{:S(2)}) async-start(bf16[4,24,2048]{2,1,0:T(8,128)(2,1)} %bitcast.10), calls=%async_computation.1 | async-start | bytes 786432 | tf_op jit(solution)/shard_map/all_to_all | solution.py:77
  162.2 13.0 %copy-start.12 = (f32[384]{0:T(512)S(1)}, f32[384]{0:T(512)}, u32[]{:S(2)}) copy-start(f32[384]{0:T(512)} %param.34) | copy-start | bytes 4612
  162.2 13.0 %copy-start.13 = (f32[384]{0:T(512)S(1)}, f32[384]{0:T(512)}, u32[]{:S(2)}) copy-start(f32[384]{0:T(512)} %param.33) | copy-start | bytes 4612
  171.7 10.8 %all-to-all-start.2 = ((bf16[4,24,2048]{2,1,0:T(8,128)(2,1)}), bf16[4,24,2048]{2,1,0:T(8,128)(2,1)S(1)}, u32[]{:S(2)}, u32[]{:S(2)}) async-start(bf16[4,24,2048]{2,1,0:T(8,128)(2,1)} %broadcast_in_dim.34), calls=%async_computation.2 | async-start | bytes 786432 | tf_op jit(solution)/shard_map/all_to_all | solution.py:284
  175.2 3.1 %collective-permute-start.11 = (f32[2,384]{1,0:T(2,128)S(1)}, f32[2,384]{1,0:T(2,128)S(1)}, u32[]{:S(2)}, u32[]{:S(2)}) collective-permute-start(f32[2,384]{1,0:T(2,128)S(1)} %pad_maximum_fusion.1.scales), channel_id=1, source_target_pairs={{0,1},{1,0},{2,3},{3,2},{4,5},{5,4},{6,7},{7,6},{8,9},{9,8},{10,11... | collective-permute-start | bytes 9224 | tf_op jit(solution)/shard_map/ppermute | solution.py:81
  184.8 14.8 %copy-start.11 = (f32[2048]{0:T(1024)S(1)}, f32[2048]{0:T(1024)}, u32[]{:S(2)}) copy-start(f32[2048]{0:T(1024)} %param.35) | copy-start | bytes 24580
  (6 other events, 25.5 us)
Sparse Core Ops, SparseCore 0:
  31.4 79.7 all-gather.3

commit v10 on v9

--- a/solution.py
+++ b/solution.py
@@ -191,31 +191,54 @@
     )
 
 
-def mlp_kernel(labels, x, weights, others, scales, other_scales, out):
+def hold_kernel(weights, out, sem):
+    copy = pltpu.make_async_copy(weights.at[:, : out.shape[1]], out, sem)
+    copy.start()
+    copy.wait()
+
+
+def hold(weights, count):
+    shape = (weights.shape[0], count, *weights.shape[2:])
+    return pl.pallas_call(
+        hold_kernel,
+        out_shape=jax.ShapeDtypeStruct(shape, weights.dtype),
+        in_specs=[pl.BlockSpec(memory_space=pltpu.HBM)],
+        out_specs=VMEM,
+        scratch_shapes=[pltpu.SemaphoreType.DMA],
+        compiler_params=pltpu.CompilerParams(vmem_limit_bytes=8 * 2**20),
+        cost_estimate=pl.CostEstimate(flops=10**7, bytes_accessed=2**22, transcendentals=0),
+        name="hold",
+    )(weights)
+
+
+def mlp_kernel(labels, x, early, late, others, scales, other_scales, out):
     units = scales.shape[1]
     size = x.shape[1] // 4
     places = [pl.ds(pl.multiple_of(labels[p] * size, size), size) for p in range(4)]
+    first = early.shape[1]
+    mine = [early[:, p] if p < first else late[:, p - first] for p in range(4)]
+    theirs = [others[:, p] for p in range(4)]
     inner = []
-    for held, scale in ((weights, scales), (others, other_scales)):
+    for held, scale in ((mine, scales), (theirs, other_scales)):
         both = jnp.zeros((x.shape[0], 2 * units), jnp.float32)
         for p, at in enumerate(places):
-            piece = held[:, p, :, : 2 * units].reshape(size, 2 * units)
+            piece = held[p][:, :, : 2 * units].reshape(size, 2 * units)
             both += jnp.dot(x[:, at], piece, preferred_element_type=jnp.float32)
         gate = both[:, :units] * scale[0:1]
         up = both[:, units:] * scale[1:2]
         inner.append((gate / (1.0 + jnp.exp(-gate)) * up).astype(jnp.bfloat16))
     for p, at in enumerate(places):
         total = 0.0
-        for held, part in zip((weights, others), inner):
-            total += dot_t(part, held[:, p, :, 2 * units :].reshape(size, units))
+        for held, part in zip((mine, theirs), inner):
+            total += dot_t(part, held[p][:, :, 2 * units :].reshape(size, units))
         out[:, at] = total.astype(jnp.bfloat16)
 
 
-def mlp(labels, x, weights, others, scales, other_scales):
+def mlp(labels, x, early, late, others, scales, other_scales):
     shape = jax.ShapeDtypeStruct(x.shape, jnp.bfloat16)
-    flops = 4 * x.shape[0] * x.shape[1] * weights.shape[-1]
-    return local_call(mlp_kernel, shape, [SMEM] + [VMEM] * 5, flops, 4 * weights.size)(
-        labels, x, weights, others, scales, other_scales
+    flops = 4 * x.shape[0] * x.shape[1] * others.shape[-1]
+    return local_call(mlp_kernel, shape, [SMEM] + [VMEM] * 6, flops, 4 * others.size)(
+        labels, x, early, late, others, scales, other_scales
     )
 
 
@@ -249,6 +272,7 @@
     own = ring_blocks(mlp_shard(w_gate, w_up, w_down))
     mlp_weights = lax.all_gather(own, "y", axis=0)
     mlp_others = swap_cores(mlp_weights)
+    early = hold(mlp_weights, 2)
     mlp_scales = jnp.stack([scale_gate, scale_up])
     other_scales = swap_cores(mlp_scales)
     heads = ring_halves(heads)
@@ -284,7 +308,7 @@
     mlp_in = lax.all_to_all(copies, "x", 0, 0, tiled=True).reshape(-1, width)
 
     labels = jnp.stack(ring_labels()).astype(jnp.int32)
-    partial = mlp(labels, mlp_in, mlp_weights, mlp_others, mlp_scales, other_scales)
+    partial = mlp(labels, mlp_in, early, mlp_weights[:, 2:], mlp_others, mlp_scales, other_scales)
     channel = sum_over_chips(partial) * scale_down
     return (hidden.astype(f32) + channel).astype(bf16)[None]
 

time: 208 us -> 212 us (1.019)
  the two profiles are of different devices: /device:TPU:24 before, /device:TPU:1 now
where the time goes in v10:
time: 212 us; the launch traced here: 211 us
  waiting for transfers between devices  75.3 us (36%)
  starting transfers between devices  66.7 us (31%)
  blocking collectives  28.9 us (14%)
  between operations  14.5 us (7%)
  local copies, waits for them, and re-layouts  11.9 us (6%)
  Pallas kernels  8.01 us (4%)
  other arithmetic  3.74 us (2%)
    all_gather x1, waiting for transfers between devices, per_device(): mlp_weights = lax.all_gather(own, 'y', axis=0)  26.5 us
    all_to_all x1, waiting for transfers between devices, per_device(): lax.all_to_all(heads, 'y', 0, 0, tiled=True).reshape(-1, heads.shape[2])  17 us
    all_gather x1, blocking collectives, per_device(): all_rows = lax.all_gather(own_rows, TP, axis=0, tiled=True)  16.7 us
    all_to_all x1, blocking collectives, sum_over_chips(): lax.all_to_all(blocks, 'x', 0, 0, tiled=True).astype(jnp.float32)  12.1 us
    ppermute x1, waiting for transfers between devices, ring_halves(): far_b = lax.ppermute(odd2, RING, pairs(0))  10.9 us
    ppermute x1, starting transfers between devices, ring_halves(): odd2 = lax.ppermute(high, RING, pairs(1))  9.31 us
    ppermute x3, starting transfers between devices, swap_cores(): return lax.ppermute(array, 'core', [(0, 1), (1, 0)])  8.95 us
    ppermute x1, starting transfers between devices, ring_blocks(): odd = lax.ppermute(block, RING, pairs(1))  8.85 us
  transfers between devices with their start and end apart: 16, of which 9 were waited for; matrix products, arithmetic and copies ran while one was open for 4% of the time, Pallas kernels for 1%

profile of v10, /device:TPU:1, one launch (start us, length us, event | category | flops | bytes accessed | tf_op | source)
XLA Modules:
  0.0 210.9 jit_solution(2581500864534300646)
XLA Ops:
  9.2 4.8 %collective-permute-start.7 = (bf16[64,1152]{1,0:T(8,128)(2,1)S(1)}, bf16[64,1152]{1,0:T(8,128)(2,1)S(1)}, u32[]{:S(2)}, u32[]{:S(2)}) collective-permute-start(bf16[64,1152]{1,0:T(8,128)(2,1)S(1)} %shard_map.173), channel_id=1, source_target_pairs={{0,64},{64,0},{128,192},{192,128},{256,320},{320,256},{384,448},{4... | collective-permute-start | bytes 442376 | tf_op jit(solution)/shard_map/ppermute | solution.py:52
  14.1 8.8 %collective-permute-start.8 = (bf16[64,1152]{1,0:T(8,128)(2,1)S(1)}, bf16[64,1152]{1,0:T(8,128)(2,1)S(1)}, u32[]{:S(2)}, u32[]{:S(2)}) collective-permute-start(bf16[64,1152]{1,0:T(8,128)(2,1)S(1)} %shard_map.173), channel_id=1, source_target_pairs={{64,128},{128,64},{192,256},{256,192},{320,384},{384,320},{448,0},... | collective-permute-start | bytes 442376 | tf_op jit(solution)/shard_map/ppermute | solution.py:53
  26.2 4.8 %collective-permute-done.9 = bf16[64,1152]{1,0:T(8,128)(2,1)S(1)} collective-permute-done((bf16[64,1152]{1,0:T(8,128)(2,1)S(1)}, bf16[64,1152]{1,0:T(8,128)(2,1)S(1)}, u32[]{:S(2)}, u32[]{:S(2)}) %collective-permute-start.9) | collective-permute-done | bytes 147488 | tf_op jit(solution)/shard_map/ppermute | solution.py:54
  34.0 6.8 %all-to-all-start = ((bf16[8,64,1024]{2,1,0:T(8,128)(2,1)}), bf16[8,64,1024]{2,1,0:T(8,128)(2,1)S(1)}, u32[]{:S(2)}, u32[]{:S(2)}) async-start(bf16[8,64,1024]{2,1,0:T(8,128)(2,1)} %heads_shard.1), calls=%async_computation | async-start | bytes 2097152 | tf_op jit(solution)/shard_map/all_to_all | solution.py:271
  40.9 16.7 %all-gather = bf16[1,192,2048]{2,1,0:T(8,128)(2,1)S(1)} all-gather(bf16[1,24,2048]{2,1,0:T(8,128)(2,1)S(1)} %copy-done.8), channel_id=2, replica_groups=mesh['rep'=2,'z'=4,'y'=8,'x'=4,'core'=2] {'x','core'}, dimensions={1}, use_global_device_ids=true | all-gather | bytes 884736 | tf_op jit(solution)/shard_map/all_gather | solution.py:279
  58.1 17.0 %all-to-all-done = bf16[8,64,1024]{2,1,0:T(8,128)(2,1)S(1)} async-done(((bf16[8,64,1024]{2,1,0:T(8,128)(2,1)}), bf16[8,64,1024]{2,1,0:T(8,128)(2,1)S(1)}, u32[]{:S(2)}, u32[]{:S(2)}) %all-to-all-start) | async-done | bytes 1048608 | tf_op jit(solution)/shard_map/all_to_all | solution.py:271
  76.3 9.3 %collective-permute-start.3 = (bf16[256,1024]{1,0:T(8,128)(2,1)}, bf16[256,1024]{1,0:T(8,128)(2,1)S(1)}, u32[]{:S(2)}, u32[]{:S(2)}) collective-permute-start(bf16[256,1024]{1,0:T(8,128)(2,1)} %bitcast.6), channel_id=1, source_target_pairs={{64,128},{128,64},{192,256},{256,192},{320,384},{384,320},{448,0},... | collective-permute-start | bytes 1572872 | tf_op jit(solution)/shard_map/ppermute | solution.py:32
  85.6 26.5 %all-gather.4.cloned.1.call-done = bf16[32,64,1152]{2,1,0:T(8,128)(2,1)} async-done(((bf16[4,64,1152]{2,1,0:T(8,128)(2,1)}), bf16[32,64,1152]{2,1,0:T(8,128)(2,1)}) %all-gather.4.cloned.1.call-update) | async-done | bytes 4718608 | tf_op jit(solution)/shard_map/all_gather | solution.py:273
  112.1 2.5 %collective-permute-start.10 = (bf16[8,4,64,1152]{3,2,1,0:T(8,128)(2,1)}, bf16[8,4,64,1152]{3,2,1,0:T(8,128)(2,1)}, u32[]{:S(2)}, u32[]{:S(2)}) collective-permute-start(bf16[8,4,64,1152]{3,2,1,0:T(8,128)(2,1)} %bitcast.45), channel_id=1, source_target_pairs={{0,1},{1,0},{2,3},{3,2},{4,5},{5,4},{6,7},{7,6},{8,9},{9,8},{10,11... | collective-permute-start | bytes 14155784 | tf_op jit(solution)/shard_map/ppermute | solution.py:81
  117.6 5.7 %collective-permute-start.2 = (bf16[256,1024]{1,0:T(8,128)(2,1)}, bf16[256,1024]{1,0:T(8,128)(2,1)S(1)}, u32[]{:S(2)}, u32[]{:S(2)}) collective-permute-start(bf16[256,1024]{1,0:T(8,128)(2,1)} %bitcast.5), channel_id=1, source_target_pairs={{64,128},{128,64},{192,256},{256,192},{320,384},{384,320},{448,0},... | collective-permute-start | bytes 1572872 | tf_op jit(solution)/shard_map/ppermute | solution.py:34
  123.3 2.6 %collective-permute-start.1 = (bf16[256,1024]{1,0:T(8,128)(2,1)}, bf16[256,1024]{1,0:T(8,128)(2,1)S(1)}, u32[]{:S(2)}, u32[]{:S(2)}) collective-permute-start(bf16[256,1024]{1,0:T(8,128)(2,1)} %bitcast.6), channel_id=1, source_target_pairs={{0,64},{64,0},{128,192},{192,128},{256,320},{320,256},{384,448},{4... | collective-permute-start | bytes 1572872 | tf_op jit(solution)/shard_map/ppermute | solution.py:33
  126.3 2.7 %collective-permute-start.5 = (bf16[256,1024]{1,0:T(8,128)(2,1)S(1)}, bf16[256,1024]{1,0:T(8,128)(2,1)S(1)}, u32[]{:S(2)}, u32[]{:S(2)}) collective-permute-start(bf16[256,1024]{1,0:T(8,128)(2,1)S(1)} %collective-permute-done.3.refs_4_), channel_id=1, source_target_pairs={{0,64},{64,0},{128,192},{192,128},{256,320},{320,256},{384,448},{4... | collective-permute-start | bytes 1572872 | tf_op jit(solution)/shard_map/ppermute | solution.py:36
  130.2 5.6 %collective-permute-start.4 = (bf16[256,1024]{1,0:T(8,128)(2,1)S(1)}, bf16[256,1024]{1,0:T(8,128)(2,1)S(1)}, u32[]{:S(2)}, u32[]{:S(2)}) collective-permute-start(bf16[256,1024]{1,0:T(8,128)(2,1)S(1)} %collective-permute-done.refs_1_), channel_id=1, source_target_pairs={{64,128},{128,64},{192,256},{256,192},{320,384},{384,320},{448,0},... | collective-permute-start | bytes 1572872 | tf_op jit(solution)/shard_map/ppermute | solution.py:35
  136.4 5.0 %collective-permute-done.1.refs_2_ = bf16[256,1024]{1,0:T(8,128)(2,1)S(1)} collective-permute-done((bf16[256,1024]{1,0:T(8,128)(2,1)}, bf16[256,1024]{1,0:T(8,128)(2,1)S(1)}, u32[]{:S(2)}, u32[]{:S(2)}) %collective-permute-start.1) | collective-permute-done | bytes 524320 | tf_op jit(solution)/shard_map/ppermute | solution.py:33
  141.7 10.9 %collective-permute-done.5.refs_6_ = bf16[256,1024]{1,0:T(8,128)(2,1)S(1)} collective-permute-done((bf16[256,1024]{1,0:T(8,128)(2,1)S(1)}, bf16[256,1024]{1,0:T(8,128)(2,1)S(1)}, u32[]{:S(2)}, u32[]{:S(2)}) %collective-permute-start.5) | collective-permute-done | bytes 524320 | tf_op jit(solution)/shard_map/ppermute | solution.py:36
  154.1 2.8 %collective-permute-start.6 = (bf16[96,2048]{1,0:T(8,128)(2,1)S(1)}, bf16[96,2048]{1,0:T(8,128)(2,1)S(1)}, u32[]{:S(2)}, u32[]{:S(2)}) collective-permute-start(bf16[96,2048]{1,0:T(8,128)(2,1)S(1)} %get-tuple-element.8), channel_id=1, source_target_pairs={{0,1},{1,0},{2,3},{3,2},{4,5},{5,4},{6,7},{7,6},{8,9},{9,8},{10,11... | collective-permute-start | bytes 1179656 | tf_op jit(solution)/shard_map/ppermute | solution.py:81
  159.0 4.0 %all-to-all-start.1 = ((bf16[4,24,2048]{2,1,0:T(8,128)(2,1)}), bf16[4,24,2048]{2,1,0:T(8,128)(2,1)S(1)}, u32[]{:S(2)}, u32[]{:S(2)}) async-start(bf16[4,24,2048]{2,1,0:T(8,128)(2,1)} %bitcast.10), calls=%async_computation.1 | async-start | bytes 786432 | tf_op jit(solution)/shard_map/all_to_all | solution.py:77
  163.0 7.2 %all-to-all-done.1 = bf16[4,24,2048]{2,1,0:T(8,128)(2,1)S(1)} async-done(((bf16[4,24,2048]{2,1,0:T(8,128)(2,1)}), bf16[4,24,2048]{2,1,0:T(8,128)(2,1)S(1)}, u32[]{:S(2)}, u32[]{:S(2)}) %all-to-all-start.1) | async-done | bytes 393248 | tf_op jit(solution)/shard_map/all_to_all | solution.py:77
  171.4 3.5 %all-to-all-start.2 = ((bf16[4,24,2048]{2,1,0:T(8,128)(2,1)}), bf16[4,24,2048]{2,1,0:T(8,128)(2,1)S(1)}, u32[]{:S(2)}, u32[]{:S(2)}) async-start(bf16[4,24,2048]{2,1,0:T(8,128)(2,1)} %broadcast_in_dim.34), calls=%async_computation.2 | async-start | bytes 786432 | tf_op jit(solution)/shard_map/all_to_all | solution.py:308
  174.9 3.7 %collective-permute-start.11 = (f32[2,384]{1,0:T(2,128)S(1)}, f32[2,384]{1,0:T(2,128)S(1)}, u32[]{:S(2)}, u32[]{:S(2)}) collective-permute-start(f32[2,384]{1,0:T(2,128)S(1)} %pad_maximum_fusion.1.scales), channel_id=1, source_target_pairs={{0,1},{1,0},{2,3},{3,2},{4,5},{5,4},{6,7},{7,6},{8,9},{9,8},{10,11... | collective-permute-start | bytes 9224 | tf_op jit(solution)/shard_map/ppermute | solution.py:81
  178.7 3.3 %slice.57.late = bf16[8,2,64,1152]{3,2,1,0:T(8,128)(2,1)} slice(bf16[8,4,64,1152]{3,2,1,0:T(8,128)(2,1)} %bitcast.46), slice={[0:8], [2:4], [0:64], [0:1152]} | slice | bytes 4718592 | tf_op jit(solution)/shard_map/slice | solution.py:311
  182.0 2.3 %copy-done = bf16[32,64,1152]{2,1,0:T(8,128)(2,1)S(1)} copy-done((bf16[32,64,1152]{2,1,0:T(8,128)(2,1)S(1)}, bf16[32,64,1152]{2,1,0:T(8,128)(2,1)}, u32[]{:S(2)}) %copy-start) | copy-done | bytes 4718616
  186.2 4.9 %shard_map.174 = bf16[96,2048]{1,0:T(8,128)(2,1)S(1)} custom-call(s32[4]{0:T(128)S(1)} %pad_add_fusion.labels, bf16[96,2048]{1,0:T(8,128)(2,1)S(1)} %bitcast.48, bf16[8,2,64,1152]{3,2,1,0:T(8,128)(2,1)S(1)} %hold.1.early, bf16[8,2,64,1152]{3,2,1,0:T(8,128)(2,1)S(1)} %copy-done.1, bf16[8,4,64,1152]{3,2,1,0:T(8,128)(2,1)} %collective-permute-done.10.others, ...), custom_call_target="tpu_custom_call" | custom-call | flops 905969664 | bytes 9437184 | tf_op jit(solution)/shard_map/pallas_call | solution.py:240
  191.2 12.1 %all_to_all.20 = bf16[4,24,2048]{2,1,0:T(8,128)(2,1)S(1)} all-to-all(bf16[4,24,2048]{2,1,0:T(8,128)(2,1)S(1)} %bitcast.49), channel_id=1, replica_groups=mesh['rep'=2,'z'=4,'y'=8,'x'=4,'core'=2] {'x'}, dimensions={0} | all-to-all | bytes 786432 | tf_op jit(solution)/shard_map/all_to_all | solution.py:77
  (74 shorter events, 22.5 us)
Async XLA Ops:
  6.5 105.6 %all-gather.4.cloned.1.call-start = ((), (), s32[]{:S(2)}) async-start(), calls=%async_computation.4 | async-start | bytes 5308416 | tf_op jit(solution)/shard_map/all_gather | solution.py:273
  9.2 15.6 %collective-permute-start.7 = (bf16[64,1152]{1,0:T(8,128)(2,1)S(1)}, bf16[64,1152]{1,0:T(8,128)(2,1)S(1)}, u32[]{:S(2)}, u32[]{:S(2)}) collective-permute-start(bf16[64,1152]{1,0:T(8,128)(2,1)S(1)} %shard_map.173), channel_id=1, source_target_pairs={{0,64},{64,0},{128,192},{192,128},{256,320},{320,256},{384,448},{4... | collective-permute-start | bytes 442376 | tf_op jit(solution)/shard_map/ppermute | solution.py:52
  14.1 12.1 %collective-permute-start.8 = (bf16[64,1152]{1,0:T(8,128)(2,1)S(1)}, bf16[64,1152]{1,0:T(8,128)(2,1)S(1)}, u32[]{:S(2)}, u32[]{:S(2)}) collective-permute-start(bf16[64,1152]{1,0:T(8,128)(2,1)S(1)} %shard_map.173), channel_id=1, source_target_pairs={{64,128},{128,64},{192,256},{256,192},{320,384},{384,320},{448,0},... | collective-permute-start | bytes 442376 | tf_op jit(solution)/shard_map/ppermute | solution.py:53
  22.9 8.1 %collective-permute-start.9 = (bf16[64,1152]{1,0:T(8,128)(2,1)S(1)}, bf16[64,1152]{1,0:T(8,128)(2,1)S(1)}, u32[]{:S(2)}, u32[]{:S(2)}) collective-permute-start(bf16[64,1152]{1,0:T(8,128)(2,1)S(1)} %shard_map.173), channel_id=1, source_target_pairs={{0,128},{64,192},{128,256},{192,320},{256,384},{320,448},{384,0},{... | collective-permute-start | bytes 442376 | tf_op jit(solution)/shard_map/ppermute | solution.py:54
  34.0 23.8 %copy-start.10 = (f32[2048]{0:T(1024)S(1)}, f32[2048]{0:T(1024)}, u32[]{:S(2)}) copy-start(f32[2048]{0:T(1024)} %param.19) | copy-start | bytes 24580
  34.0 41.1 %all-to-all-start = ((bf16[8,64,1024]{2,1,0:T(8,128)(2,1)}), bf16[8,64,1024]{2,1,0:T(8,128)(2,1)S(1)}, u32[]{:S(2)}, u32[]{:S(2)}) async-start(bf16[8,64,1024]{2,1,0:T(8,128)(2,1)} %heads_shard.1), calls=%async_computation | async-start | bytes 2097152 | tf_op jit(solution)/shard_map/all_to_all | solution.py:271
  76.3 50.0 %collective-permute-start.3 = (bf16[256,1024]{1,0:T(8,128)(2,1)}, bf16[256,1024]{1,0:T(8,128)(2,1)S(1)}, u32[]{:S(2)}, u32[]{:S(2)}) collective-permute-start(bf16[256,1024]{1,0:T(8,128)(2,1)} %bitcast.6), channel_id=1, source_target_pairs={{64,128},{128,64},{192,256},{256,192},{320,384},{384,320},{448,0},... | collective-permute-start | bytes 1572872 | tf_op jit(solution)/shard_map/ppermute | solution.py:32
  112.1 72.4 %collective-permute-start.10 = (bf16[8,4,64,1152]{3,2,1,0:T(8,128)(2,1)}, bf16[8,4,64,1152]{3,2,1,0:T(8,128)(2,1)}, u32[]{:S(2)}, u32[]{:S(2)}) collective-permute-start(bf16[8,4,64,1152]{3,2,1,0:T(8,128)(2,1)} %bitcast.45), channel_id=1, source_target_pairs={{0,1},{1,0},{2,3},{3,2},{4,5},{5,4},{6,7},{7,6},{8,9},{9,8},{10,11... | collective-permute-start | bytes 14155784 | tf_op jit(solution)/shard_map/ppermute | solution.py:81
  114.6 15.6 %collective-permute-start = (bf16[256,1024]{1,0:T(8,128)(2,1)}, bf16[256,1024]{1,0:T(8,128)(2,1)S(1)}, u32[]{:S(2)}, u32[]{:S(2)}) collective-permute-start(bf16[256,1024]{1,0:T(8,128)(2,1)} %bitcast.5), channel_id=1, source_target_pairs={{0,64},{64,0},{128,192},{192,128},{256,320},{320,256},{384,448},{4... | collective-permute-start | bytes 1572872 | tf_op jit(solution)/shard_map/ppermute | solution.py:31
  117.6 18.5 %collective-permute-start.2 = (bf16[256,1024]{1,0:T(8,128)(2,1)}, bf16[256,1024]{1,0:T(8,128)(2,1)S(1)}, u32[]{:S(2)}, u32[]{:S(2)}) collective-permute-start(bf16[256,1024]{1,0:T(8,128)(2,1)} %bitcast.5), channel_id=1, source_target_pairs={{64,128},{128,64},{192,256},{256,192},{320,384},{384,320},{448,0},... | collective-permute-start | bytes 1572872 | tf_op jit(solution)/shard_map/ppermute | solution.py:34
  123.3 18.1 %collective-permute-start.1 = (bf16[256,1024]{1,0:T(8,128)(2,1)}, bf16[256,1024]{1,0:T(8,128)(2,1)S(1)}, u32[]{:S(2)}, u32[]{:S(2)}) collective-permute-start(bf16[256,1024]{1,0:T(8,128)(2,1)} %bitcast.6), channel_id=1, source_target_pairs={{0,64},{64,0},{128,192},{192,128},{256,320},{320,256},{384,448},{4... | collective-permute-start | bytes 1572872 | tf_op jit(solution)/shard_map/ppermute | solution.py:33
  126.3 26.4 %collective-permute-start.5 = (bf16[256,1024]{1,0:T(8,128)(2,1)S(1)}, bf16[256,1024]{1,0:T(8,128)(2,1)S(1)}, u32[]{:S(2)}, u32[]{:S(2)}) collective-permute-start(bf16[256,1024]{1,0:T(8,128)(2,1)S(1)} %collective-permute-done.3.refs_4_), channel_id=1, source_target_pairs={{0,64},{64,0},{128,192},{192,128},{256,320},{320,256},{384,448},{4... | collective-permute-start | bytes 1572872 | tf_op jit(solution)/shard_map/ppermute | solution.py:36
  130.2 22.7 %collective-permute-start.4 = (bf16[256,1024]{1,0:T(8,128)(2,1)S(1)}, bf16[256,1024]{1,0:T(8,128)(2,1)S(1)}, u32[]{:S(2)}, u32[]{:S(2)}) collective-permute-start(bf16[256,1024]{1,0:T(8,128)(2,1)S(1)} %collective-permute-done.refs_1_), channel_id=1, source_target_pairs={{64,128},{128,64},{192,256},{256,192},{320,384},{384,320},{448,0},... | collective-permute-start | bytes 1572872 | tf_op jit(solution)/shard_map/ppermute | solution.py:35
  141.7 11.5 %copy-start.5 = (f32[256]{0:T(256)S(1)}, f32[256]{0:T(256)}, u32[]{:S(2)}) copy-start(f32[256]{0:T(256)} %param.24) | copy-start | bytes 3076
  141.7 11.5 %copy-start.6 = (f32[256]{0:T(256)S(1)}, f32[256]{0:T(256)}, u32[]{:S(2)}) copy-start(f32[256]{0:T(256)} %param.25) | copy-start | bytes 3076
  154.1 4.1 %collective-permute-start.6 = (bf16[96,2048]{1,0:T(8,128)(2,1)S(1)}, bf16[96,2048]{1,0:T(8,128)(2,1)S(1)}, u32[]{:S(2)}, u32[]{:S(2)}) collective-permute-start(bf16[96,2048]{1,0:T(8,128)(2,1)S(1)} %get-tuple-element.8), channel_id=1, source_target_pairs={{0,1},{1,0},{2,3},{3,2},{4,5},{5,4},{6,7},{7,6},{8,9},{9,8},{10,11... | collective-permute-start | bytes 1179656 | tf_op jit(solution)/shard_map/ppermute | solution.py:81
  158.2 12.1 %copy-start.9 = (f32[2048]{0:T(1024)S(1)}, f32[2048]{0:T(1024)}, u32[]{:S(2)}) copy-start(f32[2048]{0:T(1024)} %param.27) | copy-start | bytes 24580
  158.2 12.3 %copy-start.11 = (f32[2048]{0:T(1024)S(1)}, f32[2048]{0:T(1024)}, u32[]{:S(2)}) copy-start(f32[2048]{0:T(1024)} %param.29) | copy-start | bytes 24580
  159.0 11.2 %all-to-all-start.1 = ((bf16[4,24,2048]{2,1,0:T(8,128)(2,1)}), bf16[4,24,2048]{2,1,0:T(8,128)(2,1)S(1)}, u32[]{:S(2)}, u32[]{:S(2)}) async-start(bf16[4,24,2048]{2,1,0:T(8,128)(2,1)} %bitcast.10), calls=%async_computation.1 | async-start | bytes 786432 | tf_op jit(solution)/shard_map/all_to_all | solution.py:77
  163.0 11.8 %copy-start.13 = (f32[384]{0:T(512)S(1)}, f32[384]{0:T(512)}, u32[]{:S(2)}) copy-start(f32[384]{0:T(512)} %param.33) | copy-start | bytes 4612
  163.0 11.9 %copy-start.14 = (f32[384]{0:T(512)S(1)}, f32[384]{0:T(512)}, u32[]{:S(2)}) copy-start(f32[384]{0:T(512)} %param.34) | copy-start | bytes 4612
  171.4 13.1 %all-to-all-start.2 = ((bf16[4,24,2048]{2,1,0:T(8,128)(2,1)}), bf16[4,24,2048]{2,1,0:T(8,128)(2,1)S(1)}, u32[]{:S(2)}, u32[]{:S(2)}) async-start(bf16[4,24,2048]{2,1,0:T(8,128)(2,1)} %broadcast_in_dim.34), calls=%async_computation.2 | async-start | bytes 786432 | tf_op jit(solution)/shard_map/all_to_all | solution.py:308
  174.9 9.6 %collective-permute-start.11 = (f32[2,384]{1,0:T(2,128)S(1)}, f32[2,384]{1,0:T(2,128)S(1)}, u32[]{:S(2)}, u32[]{:S(2)}) collective-permute-start(f32[2,384]{1,0:T(2,128)S(1)} %pad_maximum_fusion.1.scales), channel_id=1, source_target_pairs={{0,1},{1,0},{2,3},{3,2},{4,5},{5,4},{6,7},{7,6},{8,9},{9,8},{10,11... | collective-permute-start | bytes 9224 | tf_op jit(solution)/shard_map/ppermute | solution.py:81
  186.2 17.1 %copy-start.12 = (f32[2048]{0:T(1024)S(1)}, f32[2048]{0:T(1024)}, u32[]{:S(2)}) copy-start(f32[2048]{0:T(1024)} %param.35) | copy-start | bytes 24580
  (7 other events, 27.1 us)
Sparse Core Ops, SparseCore 0:
  32.1 80.0 all-gather.3
